TPU v7x, 128 devices: a whole 4x4x4 slice. The times are simulated.
128 devices in a mesh: fs: 16 (over z, y), tp: 8 (over x, core).
Axes of the slice: x: 4, y: 4, z: 4, core: 2. Of those that a mesh axis runs over, the one named last changes fastest.
Arguments:
- weights_in: float32 [2, 2048, 5632], P(None, 'fs', 'tp'), may hold values from -6 to 6
- weights_mix: float32 [2048, 2048], P('fs', 'tp'), may hold values from -6 to 6
- momentum_in: float32 [2, 2048, 5632], P(None, 'fs', 'tp'), may hold values from -5 to 5
- momentum_mix: float32 [2048, 2048], P('fs', 'tp'), may hold values from -5 to 5
- grads_in: float32 [2, 2048, 5632], P(None, 'fs', 'tp'), may hold values from -5 to 5
- grads_mix: float32 [2048, 2048], P('fs', 'tp'), may hold values from -5 to 5
Outputs:
- momentum_in_next: float32 [2, 2048, 5632], P(None, 'fs', 'tp')
- momentum_mix_next: float32 [2048, 2048], P('fs', 'tp')
- weights_in_next: float32 [2, 2048, 5632], P(None, 'fs', 'tp')
- weights_mix_next: float32 [2048, 2048], P('fs', 'tp')
- update_in: float32 [2, 2048, 5632], P(None, 'fs', 'tp')
- update_mix: float32 [2048, 2048], P('fs', 'tp')
All inputs are finite; a program needn't handle non-finite values.
Results may differ from a plain program's by a relative error of at most 0.0003.
Values sent between devices are 32-bit elements; how exact they have to be, the bound alone decides.
A program may use at most 128 MiB of HBM per device.

v0:
```python
import math

import jax
import jax.numpy as jnp
from jax import lax
from jax.sharding import PartitionSpec as P

D = 2048
FF = 5632
ITERS = 3


A_COEF = 3.4445
B_COEF = -4.775
C_COEF = 2.0315
MOMENTUM_DECAY = 0.95
STEP_RATE = 0.02
HIGH = lax.Precision.HIGHEST


def gather_turned(arrays, axis, dims):
    turned = [jnp.moveaxis(a, dim, 0) for a, dim in zip(arrays, dims)]
    both = jnp.concatenate([t.reshape(len(t), -1) for t in turned], axis=1)
    result, at, gathered = (lax.all_gather(both, axis, axis=0, tiled=True), 0, [])
    for t, dim in zip(turned, dims):
        share = result[:, at : at + t[0].size].reshape(-1, *t.shape[1:])
        gathered.append(jnp.moveaxis(share, 0, dim))
        at += t[0].size
    return tuple(gathered)


def rows_for(lines, peers):
    spare = -lines.shape[0] % peers
    if not spare:
        return lines
    return jnp.concatenate([lines, jnp.zeros((spare, *lines.shape[1:]), lines.dtype)])


def sum_by_parts(shard, axis):
    lines = shard.reshape(-1, *shard.shape[1:][-1:])
    own = lax.psum_scatter(
        rows_for(lines, lax.axis_size(axis)), axis, scatter_dimension=0, tiled=True
    )
    whole = lax.all_gather(own, axis).reshape(-1, *lines.shape[1:])
    return lax.slice_in_dim(whole, 0, len(lines)).reshape(shard.shape)


def scale_from(summed):
    return (0.5 * lax.rsqrt(jnp.maximum(summed / D, 1.0)))[:, None, None]


def block_trace(shard, row_start, col_start):
    row_ids = row_start + lax.iota(jnp.int32, shard.shape[1])[:, None]
    col_ids = col_start + lax.iota(jnp.int32, shard.shape[2])[None, :]
    return jnp.sum(jnp.where((row_ids == col_ids)[None], shard, 0.0), axis=(1, 2))


def local(weights_in, weights_mix, momentum_in, momentum_mix, grads_in, grads_mix):
    fs_pos = lax.axis_index("fs")
    tp_pos = lax.axis_index("tp")
    moment_in = MOMENTUM_DECAY * momentum_in + grads_in
    moment_mix = MOMENTUM_DECAY * momentum_mix + grads_mix
    local_in = moment_in
    local_mix = moment_mix[None]
    row_count = local_in.shape[1]
    block_width = local_mix.shape[2]
    for iteration in range(ITERS):
        cols_in, cols_mix = gather_turned((local_in, local_mix), "fs", (1, 1))
        partial_value = jnp.concatenate(
            [
                jnp.einsum("krc,ksc->krs", local_in, cols_in, precision=HIGH),
                jnp.einsum("krc,ksc->krs", local_mix, cols_mix, precision=HIGH),
            ]
        )
        gram_rows = sum_by_parts(partial_value, "tp")
        gram_block = lax.dynamic_slice_in_dim(gram_rows, tp_pos * block_width, block_width, 2)
        if iteration == 0:
            traces = block_trace(gram_block, fs_pos * row_count, tp_pos * block_width)
            scaling = scale_from(lax.psum(traces, ("fs", "tp")))
        factor = scaling if iteration == 0 else jnp.ones_like(scaling)
        gram_cols = lax.all_gather(gram_block, "fs", axis=1, tiled=True)
        square = jnp.einsum("krs,ksc->krc", gram_rows, gram_cols, precision=HIGH)
        poly_mat = factor**2 * B_COEF * gram_block + factor**4 * C_COEF * square
        poly_rows = lax.all_gather(poly_mat, "tp", axis=2, tiled=True)
        local_in = factor[:2] * (
            A_COEF * local_in + jnp.einsum("krs,ksc->krc", poly_rows[:2], cols_in, precision=HIGH)
        )
        local_mix = factor[2:] * (
            A_COEF * local_mix + jnp.einsum("krs,ksc->krc", poly_rows[2:], cols_mix, precision=HIGH)
        )
    step_in = local_in * math.sqrt(max(D, FF))
    step_mix = local_mix[0] * math.sqrt(D)
    return (
        moment_in,
        moment_mix,
        weights_in - STEP_RATE * step_in,
        weights_mix - STEP_RATE * step_mix,
        step_in,
        step_mix,
    )


def solution(mesh):
    in_specs = (
        P(None, "fs", "tp"),
        P("fs", "tp"),
        P(None, "fs", "tp"),
        P("fs", "tp"),
        P(None, "fs", "tp"),
        P("fs", "tp"),
    )
    out_specs = (
        P(None, "fs", "tp"),
        P("fs", "tp"),
        P(None, "fs", "tp"),
        P("fs", "tp"),
        P(None, "fs", "tp"),
        P("fs", "tp"),
    )
    return jax.shard_map(local, mesh=mesh, in_specs=in_specs, out_specs=out_specs, check_vma=False)
```

profile of v0, /device:TPU:1, one launch (start us, length us, event | category | flops | bytes accessed | tf_op | source)
XLA Modules:
  0.0 954.9 jit_solution(4597433947635089846)
XLA Ops:
  10.9 105.9 %all-gather.16.cloned.1.call-done = f32[2048,1664]{0,1:T(8,128)} async-done(((f32[128,1664]{0,1:T(8,128)}), f32[2048,1664]{0,1:T(8,128)}) %all-gather.16.cloned.1.call-update) | async-done | bytes 13631504 | tf_op jit(solution)/shard_map/all_gather | solution.py:24
  116.8 10.4 %slice.58 = f32[2048,1408]{0,1:T(8,128)} slice(f32[2048,1664]{0,1:T(8,128)} %all-gather.16.cloned.1.call-done), slice={[0:2048], [0:1408]} | slice | bytes 23068672 | tf_op jit(solution)/shard_map/slice | solution.py:26
  127.2 9.2 fusion.25
  141.2 33.7 %reduce-scatter.4.cloned.1.call-done = f32[48,2048]{1,0:T(8,128)} async-done(((f32[384,2048]{1,0:T(8,128)}), f32[48,2048]{1,0:T(8,128)}) %reduce-scatter.4.cloned.1.call-update) | async-done | bytes 393232 | tf_op jit(solution)/shard_map/reduce_scatter | solution.py:41
  175.1 31.3 %all-gather.34.cloned.1.call-done = f32[384,2048]{1,0:T(8,128)} async-done(((f32[48,2048]{1,0:T(8,128)}), f32[384,2048]{1,0:T(8,128)}) %all-gather.34.cloned.1.call-update) | async-done | bytes 3145744 | tf_op jit(solution)/shard_map/all_gather | solution.py:44
  208.3 67.5 %psum.7 = f32[3]{0:T(128)S(1)} all-reduce(f32[3]{0:T(128)S(1)} %get-tuple-element.8), channel_id=1, replica_groups=mesh['fs'=16,'tp'=8] {'fs','tp'}, use_global_device_ids=true, to_apply=%region_2.3 | all-reduce | flops 3 | bytes 24 | tf_op jit(solution)/shard_map/psum | solution.py:79
  285.2 23.5 %all-gather.20.cloned.1.call-done = f32[3,128,2048]{2,1,0:T(8,128)} async-done(((f32[3,128,256]{2,1,0:T(8,128)}), f32[3,128,2048]{2,1,0:T(8,128)}) %all-gather.20.cloned.1.call-update) | async-done | bytes 3145744 | tf_op jit(solution)/shard_map/all_gather | solution.py:84
  313.6 13.0 %fusion.9 = f32[2,128,704]{1,2,0:T(8,128)S(1)} fusion(f32[3,128,2048]{2,1,0:T(8,128)} %all-gather.20.cloned.1.call-done, f32[2,2048,704]{1,2,0:T(8,128)} %bitcast.65, f32[2,128,704]{1,2,0:T(8,128)S(1)} %multiply_add_fusion, f32[2]{0:T(128)S(1)} %bitcast.82), kind=kOutput, calls=%fused_computation.18 | convolution fusion | flops 4429725696 | bytes 16121864 | tf_op jit(solution)/shard_map/krs,ksc->krc/dot_general | solution.py:86
  327.8 102.1 %all-gather.22.cloned.1.call-done = f32[2048,1664]{0,1:T(8,128)} async-done(((f32[128,1664]{0,1:T(8,128)}), f32[2048,1664]{0,1:T(8,128)}) %all-gather.22.cloned.1.call-update) | async-done | bytes 13631504 | tf_op jit(solution)/shard_map/all_gather | solution.py:24
  429.9 10.4 %slice.61 = f32[2048,1408]{0,1:T(8,128)} slice(f32[2048,1664]{0,1:T(8,128)} %all-gather.22.cloned.1.call-done), slice={[0:2048], [0:1408]} | slice | bytes 23068672 | tf_op jit(solution)/shard_map/slice | solution.py:26
  440.3 9.2 fusion.26
  454.4 33.7 %reduce-scatter.6.cloned.1.call-done = f32[48,2048]{1,0:T(8,128)} async-done(((f32[384,2048]{1,0:T(8,128)}), f32[48,2048]{1,0:T(8,128)}) %reduce-scatter.6.cloned.1.call-update) | async-done | bytes 393232 | tf_op jit(solution)/shard_map/reduce_scatter | solution.py:41
  488.1 31.5 %all-gather.36.cloned.1.call-done = f32[384,2048]{1,0:T(8,128)} async-done(((f32[48,2048]{1,0:T(8,128)}), f32[384,2048]{1,0:T(8,128)}) %all-gather.36.cloned.1.call-update) | async-done | bytes 3145744 | tf_op jit(solution)/shard_map/all_gather | solution.py:44
  521.4 61.7 %all-gather.24.cloned.1.call-done = f32[3,2048,256]{2,1,0:T(8,128)} async-done(((f32[3,128,256]{2,1,0:T(8,128)}), f32[3,2048,256]{2,1,0:T(8,128)}) %all-gather.24.cloned.1.call-update) | async-done | bytes 6291472 | tf_op jit(solution)/shard_map/all_gather | solution.py:81
  591.6 27.7 %all-gather.26.cloned.1.call-done = f32[3,128,2048]{2,1,0:T(8,128)} async-done(((f32[3,128,256]{2,1,0:T(8,128)}), f32[3,128,2048]{2,1,0:T(8,128)}) %all-gather.26.cloned.1.call-update) | async-done | bytes 3145744 | tf_op jit(solution)/shard_map/all_gather | solution.py:84
  623.5 13.0 %convolution_add_fusion.1 = f32[2,128,704]{1,2,0:T(8,128)S(1)} fusion(f32[3,128,2048]{2,1,0:T(8,128)} %all-gather.26.cloned.1.call-done, f32[2,2048,704]{1,2,0:T(8,128)} %bitcast.69, f32[2,128,704]{1,2,0:T(8,128)S(1)} %fusion.9), kind=kOutput, calls=%fused_computation.16 | convolution fusion | flops 4429545472 | bytes 16121856 | tf_op jit(solution)/shard_map/krs,ksc->krc/dot_general | solution.py:86
  637.6 102.3 %all-gather.28.cloned.1.call-done = f32[2048,1664]{0,1:T(8,128)} async-done(((f32[128,1664]{0,1:T(8,128)}), f32[2048,1664]{0,1:T(8,128)}) %all-gather.28.cloned.1.call-update) | async-done | bytes 13631504 | tf_op jit(solution)/shard_map/all_gather | solution.py:24
  739.8 10.4 %slice.64 = f32[2048,1408]{0,1:T(8,128)} slice(f32[2048,1664]{0,1:T(8,128)} %all-gather.28.cloned.1.call-done), slice={[0:2048], [0:1408]} | slice | bytes 23068672 | tf_op jit(solution)/shard_map/slice | solution.py:26
  750.2 9.2 fusion.27
  764.3 33.7 %reduce-scatter.8.cloned.1.call-done = f32[48,2048]{1,0:T(8,128)} async-done(((f32[384,2048]{1,0:T(8,128)}), f32[48,2048]{1,0:T(8,128)}) %reduce-scatter.8.cloned.1.call-update) | async-done | bytes 393232 | tf_op jit(solution)/shard_map/reduce_scatter | solution.py:41
  798.0 31.5 %all-gather.38.cloned.1.call-done = f32[384,2048]{1,0:T(8,128)} async-done(((f32[48,2048]{1,0:T(8,128)}), f32[384,2048]{1,0:T(8,128)}) %all-gather.38.cloned.1.call-update) | async-done | bytes 3145744 | tf_op jit(solution)/shard_map/all_gather | solution.py:44
  831.6 61.3 %all-gather.30.cloned.1.call-done = f32[3,2048,256]{2,1,0:T(8,128)} async-done(((f32[3,128,256]{2,1,0:T(8,128)}), f32[3,2048,256]{2,1,0:T(8,128)}) %all-gather.30.cloned.1.call-update) | async-done | bytes 6291472 | tf_op jit(solution)/shard_map/all_gather | solution.py:81
  901.1 27.9 %all-gather.32.cloned.1.call-done = f32[3,128,2048]{2,1,0:T(8,128)} async-done(((f32[3,128,256]{2,1,0:T(8,128)}), f32[3,128,2048]{2,1,0:T(8,128)}) %all-gather.32.cloned.1.call-update) | async-done | bytes 3145744 | tf_op jit(solution)/shard_map/all_gather | solution.py:84
  934.0 13.9 %broadcast_multiply_fusion = (f32[2,128,704]{1,2,0:T(8,128)}, f32[2,128,704]{1,2,0:T(8,128)}) fusion(f32[2,128,704]{1,2,0:T(8,128)S(1)} %copy-done.3, f32[3,128,2048]{2,1,0:T(8,128)S(1)} %copy-done.1, f32[2,2048,704]{1,2,0:T(8,128)} %bitcast.67, f32[2,128,704]{1,2,0:T(8,128)S(1)} %convolution_add_fusion.1), kind=kOutput, calls=%fused_computation.38 | convolution fusion | flops 4430086144 | bytes 17563648 | tf_op jit(solution)/shard_map/krs,ksc->krc/dot_general | solution.py:86
  (70 shorter events, 66.5 us)
Async XLA Ops:
  7.2 109.6 %all-gather.16.cloned.1.call-start = ((), (), s32[]{:S(2)}) async-start(), calls=%async_computation.3 | async-start | bytes 14483456 | tf_op jit(solution)/shard_map/all_gather | solution.py:24
  8.2 300.5 %copy-start.2 = (f32[128,256]{1,0:T(8,128)}, f32[128,256]{1,0:T(8,128)S(1)}, u32[]{:S(2)}) copy-start(f32[128,256]{1,0:T(8,128)S(1)} %multiply_add_fusion.1) | copy-start | bytes 393220
  9.7 303.9 %copy-start = (f32[2,128,704]{1,2,0:T(8,128)}, f32[2,128,704]{1,2,0:T(8,128)S(1)}, u32[]{:S(2)}) copy-start(f32[2,128,704]{1,2,0:T(8,128)S(1)} %multiply_add_fusion) | copy-start | bytes 2162692
  10.8 164.1 %reduce-scatter.4.cloned.1.call-start = ((), (), s32[]{:S(2)}) async-start(), calls=%async_computation.4 | async-start | bytes 3538944 | tf_op jit(solution)/shard_map/reduce_scatter | solution.py:41
  141.2 65.3 %all-gather.34.cloned.1.call-start = ((), (), s32[]{:S(2)}) async-start(), calls=%async_computation.15 | async-start | bytes 3538944 | tf_op jit(solution)/shard_map/all_gather | solution.py:44
  174.9 100.9 %all-gather.18.cloned.1.call-start = ((), (), s32[]{:S(2)}) async-start(), calls=%async_computation.5 | async-start | bytes 6684672 | tf_op jit(solution)/shard_map/all_gather | solution.py:81
  208.2 100.5 %all-gather.20.cloned.1.call-start = ((), (), s32[]{:S(2)}) async-start(), calls=%async_computation.6 | async-start | bytes 3538944 | tf_op jit(solution)/shard_map/all_gather | solution.py:84
  284.1 145.9 %all-gather.22.cloned.1.call-start = ((), (), s32[]{:S(2)}) async-start(), calls=%async_computation.7 | async-start | bytes 14483456 | tf_op jit(solution)/shard_map/all_gather | solution.py:24
  327.6 160.4 %reduce-scatter.6.cloned.1.call-start = ((), (), s32[]{:S(2)}) async-start(), calls=%async_computation.8 | async-start | bytes 3538944 | tf_op jit(solution)/shard_map/reduce_scatter | solution.py:41
  454.3 65.3 %all-gather.36.cloned.1.call-start = ((), (), s32[]{:S(2)}) async-start(), calls=%async_computation.16 | async-start | bytes 3538944 | tf_op jit(solution)/shard_map/all_gather | solution.py:44
  488.1 95.1 %all-gather.24.cloned.1.call-start = ((), (), s32[]{:S(2)}) async-start(), calls=%async_computation.9 | async-start | bytes 6684672 | tf_op jit(solution)/shard_map/all_gather | solution.py:81
  521.4 97.9 %all-gather.26.cloned.1.call-start = ((), (), s32[]{:S(2)}) async-start(), calls=%async_computation.10 | async-start | bytes 3538944 | tf_op jit(solution)/shard_map/all_gather | solution.py:84
  591.3 148.5 %all-gather.28.cloned.1.call-start = ((), (), s32[]{:S(2)}) async-start(), calls=%async_computation.11 | async-start | bytes 14483456 | tf_op jit(solution)/shard_map/all_gather | solution.py:24
  637.5 160.4 %reduce-scatter.8.cloned.1.call-start = ((), (), s32[]{:S(2)}) async-start(), calls=%async_computation.12 | async-start | bytes 3538944 | tf_op jit(solution)/shard_map/reduce_scatter | solution.py:41
  764.2 65.3 %all-gather.38.cloned.1.call-start = ((), (), s32[]{:S(2)}) async-start(), calls=%async_computation.17 | async-start | bytes 3538944 | tf_op jit(solution)/shard_map/all_gather | solution.py:44
  797.9 94.9 %all-gather.30.cloned.1.call-start = ((), (), s32[]{:S(2)}) async-start(), calls=%async_computation.13 | async-start | bytes 6684672 | tf_op jit(solution)/shard_map/all_gather | solution.py:81
  831.2 97.8 %copy-start.4 = (f32[128,256]{1,0:T(8,128)S(1)}, f32[128,256]{1,0:T(8,128)}, u32[]{:S(2)}) copy-start(f32[128,256]{1,0:T(8,128)} %param.7) | copy-start | bytes 393220
  831.3 97.8 %all-gather.32.cloned.1.call-start = ((), (), s32[]{:S(2)}) async-start(), calls=%async_computation.14 | async-start | bytes 3538944 | tf_op jit(solution)/shard_map/all_gather | solution.py:84
  901.1 33.0 %copy-start.3 = (f32[2,128,704]{1,2,0:T(8,128)S(1)}, f32[2,128,704]{1,2,0:T(8,128)}, u32[]{:S(2)}) copy-start(f32[2,128,704]{1,2,0:T(8,128)} %param.6) | copy-start | bytes 2162692
  929.0 5.0 copy-start.1
Sparse Core Ops, SparseCore 0:
  10.9 105.7 all-gather.15
  141.3 33.5 reduce-scatter.3
  176.6 29.8 all-gather.33
  209.0 61.3 all-gather.17
  284.2 24.4 all-gather.19
  327.7 102.1 all-gather.21
  454.4 33.5 reduce-scatter.5
  489.7 29.8 all-gather.35
  522.3 60.7 all-gather.23
  591.5 27.7 all-gather.25
  637.6 102.1 all-gather.27
  764.3 33.5 reduce-scatter.7
  799.6 29.8 all-gather.37
  832.0 60.7 all-gather.29
  901.2 27.7 all-gather.31
where the time goes:
time: 963 us; the launch traced here: 955 us
  waiting for transfers between devices  708 us (74%)
  matrix products  114 us (12%)
  blocking collectives  67.5 us (7%)
  local copies, waits for them, and re-layouts  35.7 us (4%)
  between operations  14.6 us (2%)
  other arithmetic  13.1 us (1%)
    all_gather x3, waiting for transfers between devices, gather_turned(): lax.all_gather(both, axis, axis=0, tiled=True)  310 us
    all_gather x3, waiting for transfers between devices, local(): gram_cols = lax.all_gather(gram_block, 'fs', axis=1, tiled=True)  123 us
    reduce_scatter x3, waiting for transfers between devices, sum_by_parts(): lax.psum_scatter(rows_for(lines, lax.axis_size(axis)), axis, scatter_dime...  101 us
    all_gather x3, waiting for transfers between devices, sum_by_parts(): whole = lax.all_gather(own, axis).reshape(-1, *lines.shape[1:])  94.3 us
    all_gather x3, waiting for transfers between devices, local(): poly_rows = lax.all_gather(poly_mat, 'tp', axis=2, tiled=True)  79.2 us
    psum x1, blocking collectives, local(): scaling = scale_from(lax.psum(traces, ('fs', 'tp')))  67.5 us
    dot_general x3, matrix products, local(): jnp.einsum('krs,ksc->krc', poly_rows[:2], cols_in, precision=HIGH)  39.9 us
    slice x3, local copies, waits for them, and re-layouts, gather_turned(): share = result[:, at:at + t[0].size].reshape(-1, *t.shape[1:])  31.2 us
  transfers between devices with their start and end apart: 15, of which 14 were waited for; matrix products, arithmetic and copies ran while one was open for 0% of the time, Pallas kernels for 0%

commit v1 on v0

v1 whole, which is shorter than its diff:
```python
import functools
import math

import jax
import jax.numpy as jnp
from jax import lax
from jax.experimental import pallas as pl
from jax.experimental.pallas import tpu as pltpu
from jax.sharding import PartitionSpec as P

D = 2048
FF = 5632
ITERS = 3

A_COEF = 3.4445
B_COEF = -4.775
C_COEF = 2.0315
MOMENTUM_DECAY = 0.95
STEP_RATE = 0.02
HIGH = lax.Precision.HIGH
MESH = pl.DeviceIdType.MESH

SIDE = 4
PLANE = SIDE * SIDE
WIDE = 640
ODD = 64
MIX = 256
PACKED = 2 * WIDE + 2 * ODD + MIX


def put(src, dst, send, recv, fs, tp):
    return pltpu.make_async_remote_copy(
        src_ref=src, dst_ref=dst, send_sem=send, recv_sem=recv, device_id=(fs, tp), device_id_type=MESH
    )


def greet(peers):
    barrier = pltpu.get_barrier_semaphore()
    for fs, tp in peers:
        pl.semaphore_signal(barrier, inc=1, device_id=(fs, tp), device_id_type=MESH)
    pl.semaphore_wait(barrier, len(peers))


def ring_place(cycle, z, y):
    return SIDE * (z if cycle == 0 else y) + lax.rem(z + y, SIDE)


def ring_fs(cycle, place):
    a = place // SIDE
    b = lax.rem(place - a + SIDE, SIDE)
    return SIDE * a + b if cycle == 0 else SIDE * b + a


def plane_gather_kernel(pieces, paired, block, out, send, recv, own_sem, pair_send, pair_recv):
    fs, tp = lax.axis_index("fs"), lax.axis_index("tp")
    z, y = fs // SIDE, lax.rem(fs, SIDE)
    core = lax.rem(tp, 2)
    other = tp + 1 - 2 * core
    rows, cols = block.shape
    quarter = rows // 4
    per_ring = len(pieces)
    rings = [(cycle, way) for cycle in (0, 1) for way in (1, -1)]
    place = [ring_place(cycle, z, y) for cycle in (0, 1)]
    nexts = [ring_fs(c, lax.rem(place[c] + PLANE + w, PLANE)) for c, w in rings]
    peers = [(n, tp) for n in nexts]
    if paired:
        peers.append((fs, other))
    greet(peers)

    def slot(origin, row, height, col, width):
        where = (origin, core) if paired else (origin,)
        return out.at[where + (pl.ds(row, height), pl.ds(col, width))]

    def own(row, height, col, width):
        return block.at[pl.ds(row, height), pl.ds(col, width)]

    def piece_of(k, i):
        row, height, col, width = pieces[i]
        return quarter * k + row, height, col, width

    def hop(step, k, i, first):
        c, w = rings[k]
        origin = ring_fs(c, lax.rem(place[c] + 2 * PLANE - w * step, PLANE))
        spot = piece_of(k, i)
        lane = k * per_ring + i
        return put(own(*spot) if first else slot(origin, *spot), slot(origin, *spot), send.at[lane], recv.at[lane, step], nexts[k], tp)

    mine = out.at[fs, core] if paired else out.at[fs]
    keep = pltpu.make_async_copy(block, mine, own_sem)
    for i in range(per_ring):
        for k in range(4):
            hop(0, k, i, True).start()
    keep.start()
    if paired:
        put(block, mine, pair_send, pair_recv, fs, other).start()

    def pass_on(step, last):
        for i in range(per_ring):
            for k in range(4):
                before = hop(step - 1, k, i, False)
                before.wait_send()
                before.wait_recv()
                if not last:
                    hop(step, k, i, False).start()
        if paired:
            for k in range(4):
                c, w = rings[k]
                origin = ring_fs(c, lax.rem(place[c] + 2 * PLANE - w * step, PLANE))
                there = slot(origin, quarter * k, quarter, 0, cols)
                put(there, there, pair_send, pair_recv, fs, other).start()

    @pl.loop(1, PLANE - 1)
    def _(step):
        pass_on(step, False)

    pass_on(PLANE - 1, True)
    keep.wait()
    if paired:
        sent = put(out.at[:, core], out.at[:, 1 - core], pair_send, pair_recv, fs, other)
        sent.wait_send()
        sent.wait_recv()


def plane_gather(block, pieces, paired, cid):
    rows, cols = block.shape
    shape = (PLANE, 2, rows, cols) if paired else (PLANE, rows, cols)
    lanes = 4 * len(pieces)
    return pl.pallas_call(
        functools.partial(plane_gather_kernel, pieces, paired),
        out_shape=jax.ShapeDtypeStruct(shape, jnp.float32),
        in_specs=[pl.BlockSpec(memory_space=pltpu.VMEM)],
        out_specs=pl.BlockSpec(memory_space=pltpu.VMEM),
        scratch_shapes=[
            pltpu.SemaphoreType.DMA((lanes,)),
            pltpu.SemaphoreType.DMA((lanes, PLANE - 1)),
            pltpu.SemaphoreType.DMA,
            pltpu.SemaphoreType.DMA,
            pltpu.SemaphoreType.DMA,
        ],
        compiler_params=pltpu.CompilerParams(collective_id=cid, has_side_effects=True, vmem_limit_bytes=40 << 20),
        name=f"plane_gather_{cid}",
    )(block)


def reduce_kernel(part, out, pair, total, near, far, hold, send, recv):
    fs, tp = lax.axis_index("fs"), lax.axis_index("tp")
    x, core = tp // 2, lax.rem(tp, 2)
    right = 2 * lax.rem(x + 1, SIDE) + core
    left = 2 * lax.rem(x + SIDE - 1, SIDE) + core
    other = tp + 1 - 2 * core
    greet([(fs, right), (fs, left), (fs, other)])
    copies = [put(part.at[m, 1 - core], pair.at[m], send.at[m], recv.at[m], fs, other) for m in range(3)]
    for c in copies:
        c.start()
    for m, c in enumerate(copies):
        c.wait()
        total[m] = part[m, core] + pair[m]
    total[3] = jnp.zeros_like(total[3])
    half = total.shape[1] // 2
    up, down = pl.ds(0, half), pl.ds(half, half)
    ahead, back, across = lax.rem(x + 1, SIDE), lax.rem(x + SIDE - 1, SIDE), lax.rem(x + 2, SIDE)
    far_right = put(total.at[across, up], far.at[0], send.at[3], recv.at[3], fs, right)
    far_left = put(total.at[across, down], far.at[1], send.at[4], recv.at[4], fs, left)
    near_right = put(total.at[ahead, down], near.at[0], send.at[5], recv.at[5], fs, right)
    near_left = put(total.at[back, up], near.at[1], send.at[6], recv.at[6], fs, left)
    for c in (far_right, far_left, near_right, near_left):
        c.start()
    far_right.wait_recv()
    hold[0] = far[0] + total[ahead, up]
    on_right = put(hold.at[0], near.at[2], send.at[7], recv.at[7], fs, right)
    on_right.start()
    far_left.wait_recv()
    hold[1] = far[1] + total[back, down]
    on_left = put(hold.at[1], near.at[3], send.at[8], recv.at[8], fs, left)
    on_left.start()
    near_right.wait_recv()
    near_left.wait_recv()
    on_right.wait_recv()
    out[up, :] = total[x, up] + near[2] + near[1]
    on_left.wait_recv()
    out[down, :] = total[x, down] + near[3] + near[0]
    for c in (far_right, far_left, near_right, near_left, on_right, on_left):
        c.wait_send()


def reduce_to_planes(part, cid):
    rows, cols = part.shape[2:]
    f32 = jnp.float32
    return pl.pallas_call(
        reduce_kernel,
        out_shape=jax.ShapeDtypeStruct((rows, cols), f32),
        in_specs=[pl.BlockSpec(memory_space=pltpu.VMEM)],
        out_specs=pl.BlockSpec(memory_space=pltpu.VMEM),
        scratch_shapes=[
            pltpu.VMEM((3, rows, cols), f32),
            pltpu.VMEM((4, rows, cols), f32),
            pltpu.VMEM((4, rows // 2, cols), f32),
            pltpu.VMEM((2, rows // 2, cols), f32),
            pltpu.VMEM((2, rows // 2, cols), f32),
            pltpu.SemaphoreType.DMA((9,)),
            pltpu.SemaphoreType.DMA((9,)),
        ],
        compiler_params=pltpu.CompilerParams(collective_id=cid, has_side_effects=True, vmem_limit_bytes=32 << 20),
        name="reduce_to_planes",
    )(part)


def spread_kernel(block, out, send, recv, own_sem, pair_send, pair_recv):
    fs, tp = lax.axis_index("fs"), lax.axis_index("tp")
    x, core = tp // 2, lax.rem(tp, 2)
    right = 2 * lax.rem(x + 1, SIDE) + core
    left = 2 * lax.rem(x + SIDE - 1, SIDE) + core
    other = tp + 1 - 2 * core
    ahead, back, across = lax.rem(x + 1, SIDE), lax.rem(x + SIDE - 1, SIDE), lax.rem(x + 2, SIDE)
    greet([(fs, right), (fs, left), (fs, other)])
    half = block.shape[0] // 2
    parts = [pl.ds(0, half), pl.ds(half, half)]
    go_right = [put(block.at[parts[h]], out.at[x, core, parts[h]], send.at[h], recv.at[h], fs, right) for h in (0, 1)]
    go_left = [put(block.at[parts[1 - h]], out.at[x, core, parts[1 - h]], send.at[2 + h], recv.at[2 + h], fs, left) for h in (0, 1)]
    for h in (0, 1):
        go_right[h].start()
        go_left[h].start()
    keep = pltpu.make_async_copy(block, out.at[x, core], own_sem)
    keep.start()
    put(block, out.at[x, core], pair_send, pair_recv, fs, other).start()
    go_right[0].wait_recv()
    first = out.at[back, core, parts[0]]
    relay_right = put(first, first, send.at[4], recv.at[4], fs, right)
    relay_right.start()
    go_left[0].wait_recv()
    second = out.at[ahead, core, parts[1]]
    relay_left = put(second, second, send.at[5], recv.at[5], fs, left)
    relay_left.start()
    go_right[1].wait_recv()
    put(out.at[back, core], out.at[back, core], pair_send, pair_recv, fs, other).start()
    go_left[1].wait_recv()
    put(out.at[ahead, core], out.at[ahead, core], pair_send, pair_recv, fs, other).start()
    relay_right.wait_recv()
    relay_left.wait_recv()
    put(out.at[across, core], out.at[across, core], pair_send, pair_recv, fs, other).start()
    for c in go_right + go_left + [relay_right, relay_left]:
        c.wait_send()
    keep.wait()
    whole = put(out.at[:, core], out.at[:, 1 - core], pair_send, pair_recv, fs, other)
    whole.wait_send()
    whole.wait_recv()


def spread(block, cid):
    rows, cols = block.shape
    return pl.pallas_call(
        spread_kernel,
        out_shape=jax.ShapeDtypeStruct((SIDE, 2, rows, cols), jnp.float32),
        in_specs=[pl.BlockSpec(memory_space=pltpu.VMEM)],
        out_specs=pl.BlockSpec(memory_space=pltpu.VMEM),
        scratch_shapes=[
            pltpu.SemaphoreType.DMA((6,)),
            pltpu.SemaphoreType.DMA((6,)),
            pltpu.SemaphoreType.DMA,
            pltpu.SemaphoreType.DMA,
            pltpu.SemaphoreType.DMA,
        ],
        compiler_params=pltpu.CompilerParams(collective_id=cid, has_side_effects=True, vmem_limit_bytes=32 << 20),
        name="spread",
    )(block)


def split_into(src, scale, high, low):
    step = 64

    @pl.loop(0, src.shape[0] // step)
    def _(i):
        rows = pl.ds(pl.multiple_of(i * step, step), step)
        value = src[rows, :] * scale
        top = value.astype(jnp.bfloat16)
        high[rows, :] = top
        low[rows, :] = (value - top.astype(jnp.float32)).astype(jnp.bfloat16)


def times(src, dst, pair, high, low):
    rows, size = src.shape
    value = src[...]
    top = value.astype(jnp.bfloat16)
    pair[:rows, :] = top
    pair[rows:, :] = (value - top.astype(jnp.float32)).astype(jnp.bfloat16)
    width = 256

    @pl.loop(0, size // width)
    def _(j):
        cols = pl.ds(pl.multiple_of(j * width, width), width)
        main = jnp.dot(pair[...], high[:, cols], preferred_element_type=jnp.float32)
        rest = jnp.dot(pair[:rows, :], low[:, cols], preferred_element_type=jnp.float32)
        dst[:, cols] = main[:rows] + (main[rows:] + rest)


def first_chain_kernel(whole, own, next_rows, coef_rows, high, low, pair, v, p, w):
    size = whole.shape[1]
    lane = 128

    def diag(i, total):
        at = pl.ds(pl.multiple_of(i * lane, lane), lane)
        block = whole[at, at]
        eye = lax.broadcasted_iota(jnp.int32, block.shape, 0) == lax.broadcasted_iota(jnp.int32, block.shape, 1)
        return total + jnp.where(eye, block, 0.0)

    acc = lax.fori_loop(0, size // lane, diag, jnp.zeros((lane, lane), jnp.float32))
    ssq = jnp.sum(jnp.sum(acc, axis=0, keepdims=True), axis=1, keepdims=True)
    s = 0.5 * lax.rsqrt(jnp.maximum(ssq / D, 1.0))
    split_into(whole, s * s, high, low)
    fs, tp = lax.axis_index("fs"), lax.axis_index("tp")
    start = 128 * fs + 64 * lax.rem(tp, 2)
    shape = own.shape
    on_diag = lax.broadcasted_iota(jnp.int32, shape, 1) == start + lax.broadcasted_iota(jnp.int32, shape, 0)
    v[...] = own[...] * (s * s)
    times(v, p, pair, high, low)
    coef_rows[...] = s * (jnp.where(on_diag, A_COEF, 0.0) + B_COEF * v[...] + C_COEF * p[...])
    times(p, w, pair, high, low)
    w[...] = A_COEF * v[...] + B_COEF * p[...] + C_COEF * w[...]
    times(w, v, pair, high, low)
    times(v, p, pair, high, low)
    next_rows[...] = A_COEF * w[...] + B_COEF * v[...] + C_COEF * p[...]


def second_chain_kernel(whole, coef, out, high, low, pair, base, v, p, q):
    split_into(whole, 1.0, high, low)

    def by_a1(src, dst):
        times(src, p, pair, high, low)
        times(p, q, pair, high, low)
        dst[...] = A_COEF * src[...] + B_COEF * p[...] + C_COEF * q[...]

    by_a1(coef, base)
    out[...] = A_COEF * base[...]
    for src, weight in ((base, B_COEF), (v, C_COEF)):
        times(src, q, pair, high, low)
        v[...] = q[...]
        by_a1(v, v)
        by_a1(v, v)
        out[...] += weight * v[...]


def chain_call(kernel, whole, own, outs, works, name):
    rows, cols = own.shape
    size = whole.shape[0]
    f32, bf16 = jnp.float32, jnp.bfloat16
    vmem = pl.BlockSpec(memory_space=pltpu.VMEM)
    return pl.pallas_call(
        kernel,
        out_shape=[jax.ShapeDtypeStruct((rows, cols), f32)] * outs,
        in_specs=[vmem, vmem],
        out_specs=[vmem] * outs,
        scratch_shapes=[
            pltpu.VMEM((size, cols), bf16),
            pltpu.VMEM((size, cols), bf16),
            pltpu.VMEM((2 * rows, cols), bf16),
        ]
        + [pltpu.VMEM((rows, cols), f32)] * works,
        compiler_params=pltpu.CompilerParams(vmem_limit_bytes=56 << 20),
        name=name,
    )(whole, own)


def only(lanes_low, x):
    lane = lax.broadcasted_iota(jnp.int32, x.shape, x.ndim - 1)
    return jnp.where((lane < ODD) == lanes_low, x, 0.0)


def local(weights_in, weights_mix, momentum_in, momentum_mix, grads_in, grads_mix):
    moment_in = MOMENTUM_DECAY * momentum_in + grads_in
    moment_mix = MOMENTUM_DECAY * momentum_mix + grads_mix
    first, second = moment_in[0], moment_in[1]
    packed = jnp.concatenate(
        [first[:, :WIDE], second[:, :WIDE], first[:, WIDE:], second[:, WIDE:], moment_mix], axis=1
    )
    x_pieces = tuple((16 * i, 16, 0, PACKED) for i in range(2))
    g_pieces = tuple((8 * i, 8, 1024 * j, 1024) for i in range(2) for j in range(2))
    cols = plane_gather(packed, x_pieces, False, 0).reshape(D, PACKED)
    spans = [slice(0, WIDE), slice(WIDE, 2 * WIDE), slice(2 * WIDE, 2 * WIDE + 2 * ODD), slice(2 * WIDE + 2 * ODD, PACKED)]
    a0, a1, odd, mix = (cols[:, s] for s in spans)
    r0, r1, rodd, rmix = (packed[:, s] for s in spans)
    dot_t = functools.partial(lax.dot_general, dimension_numbers=(((1,), (1,)), ((), ())), precision=HIGH)
    part = jnp.stack(
        [
            dot_t(r0, a0) + dot_t(only(True, rodd), odd),
            dot_t(r1, a1) + dot_t(only(False, rodd), odd),
            dot_t(rmix, mix),
        ]
    ).reshape(3, 2, 64, D)
    own = reduce_to_planes(part, 1)
    gram = plane_gather(own, g_pieces, True, 2).reshape(D, D)
    next_rows, coef = chain_call(first_chain_kernel, gram, own, 2, 3, "first_chain")
    gram1 = plane_gather(next_rows, g_pieces, True, 3).reshape(D, D)
    (poly,) = chain_call(second_chain_kernel, gram1, coef, 1, 4, "second_chain")
    polys = spread(poly, 4).reshape(SIDE, 128, D)
    dot = functools.partial(jnp.dot, precision=HIGH)
    odds = dot(polys[:2].reshape(256, D), odd)
    y0 = jnp.concatenate([dot(polys[0], a0), odds[:128, :ODD]], axis=1)
    y1 = jnp.concatenate([dot(polys[1], a1), odds[128:, ODD:]], axis=1)
    step_in = jnp.stack([y0, y1]) * math.sqrt(max(D, FF))
    step_mix = dot(polys[2], mix) * math.sqrt(D)
    return (
        moment_in,
        moment_mix,
        weights_in - STEP_RATE * step_in,
        weights_mix - STEP_RATE * step_mix,
        step_in,
        step_mix,
    )


def solution(mesh):
    specs = (
        P(None, "fs", "tp"),
        P("fs", "tp"),
        P(None, "fs", "tp"),
        P("fs", "tp"),
        P(None, "fs", "tp"),
        P("fs", "tp"),
    )
    return jax.shard_map(local, mesh=mesh, in_specs=specs, out_specs=specs, check_vma=False)
```

time: 963 us -> 382 us (0.40)
  waiting for transfers between devices: 708 us -> 0 us
  Pallas kernels: 0 us -> 351 us
  matrix products: 114 us -> 17.2 us
  blocking collectives: 67.5 us -> 0 us
  local copies, waits for them, and re-layouts: 35.7 us -> 10.2 us
  between operations: 14.6 us -> 0.99 us
  other arithmetic: 13.1 us -> 1.8 us
    all_gather x12 -> x0, waiting for transfers between devices: 607 us -> none  [the longest x3 310 us: gather_turned(): lax.all_gather(both, axis, axis=0, tiled=True)]
    pallas_call x0 -> x7, Pallas kernels: none -> 351 us  [the longest x3 212 us: plane_gather(): pl.pallas_call(functools.partial(plane_gather_kernel, pieces, paired), ou...]
    reduce_scatter x3 -> x0, waiting for transfers between devices: 101 us -> none  [sum_by_parts(): lax.psum_scatter(rows_for(lines, lax.axis_size(axis)), axis, scatter_dime...]
    dot_general x15 -> x9, matrix products: 114 us -> 17.2 us  [the longest x1 2.97 us: local(): step_mix = dot(polys[2], mix) * math.sqrt(D)]
    psum x1 -> x0, blocking collectives: 67.5 us -> none  [local(): scaling = scale_from(lax.psum(traces, ('fs', 'tp')))]
    slice x4 -> x7, local copies, waits for them, and re-layouts: 31.8 us -> 0.61 us  [the longest x1 0.26 us: local(): step_mix = dot(polys[2], mix) * math.sqrt(D)]
  transfers between devices with their start and end apart: 15 -> 0, of which waited for: 14 -> 0; matrix products, arithmetic and copies ran while one was open for 0% -> 0% of each run, Pallas kernels for 0% -> 0%
where the time goes in v1:
time: 382 us; the launch traced here: 381 us
  Pallas kernels  351 us (92%)
  matrix products  17.2 us (5%)
  local copies, waits for them, and re-layouts  10.2 us (3%)
    pallas_call x3, Pallas kernels, plane_gather(): pl.pallas_call(functools.partial(plane_gather_kernel, pieces, paired), ou...  212 us
    pallas_call x2, Pallas kernels, chain_call(): pl.pallas_call(kernel, out_shape=[jax.ShapeDtypeStruct((rows, cols), f32)...  85.1 us
    pallas_call x1, Pallas kernels, reduce_to_planes(): pl.pallas_call(reduce_kernel, out_shape=jax.ShapeDtypeStruct((rows, cols)...  31.3 us
    pallas_call x1, Pallas kernels, spread(): pl.pallas_call(spread_kernel, out_shape=jax.ShapeDtypeStruct((SIDE, 2, ro...  22.7 us
    unnamed x30, local copies, waits for them, and re-layouts  9.46 us

profile of v1, /device:TPU:1, one launch (start us, length us, event | category | flops | bytes accessed | tf_op | source)
XLA Modules:
  0.0 381.2 jit_solution(16329184418560895756)
XLA Ops:
  0.7 1.4 copy.13
  2.1 1.4 copy.12
  3.6 1.1 copy.17
  5.0 75.3 %plane_gather_0.1 = f32[16,128,1664]{2,1,0:T(8,128)S(1)} custom-call(f32[128,1664]{1,0:T(8,128)S(1)} %concatenate.13.block), custom_call_target="tpu_custom_call" | custom-call | tf_op jit(solution)/shard_map/plane_gather_0/pallas_call | solution.py:128
  80.3 1.2 fusion.16
  82.1 2.7 fusion.11
  84.9 0.6 fusion.22
  85.5 2.7 fusion.8
  88.6 31.3 %reduce_to_planes.1.block.own = f32[64,2048]{1,0:T(8,128)S(1)} custom-call(f32[3,2,64,2048]{3,2,1,0:T(8,128)S(1)} %pad_maximum_fusion.part), custom_call_target="tpu_custom_call" | custom-call | tf_op jit(solution)/shard_map/reduce_to_planes/pallas_call | solution.py:189
  119.9 68.3 %plane_gather_2.1 = f32[16,2,64,2048]{3,2,1,0:T(8,128)} custom-call(f32[64,2048]{1,0:T(8,128)S(1)} %reduce_to_planes.1.block.own), custom_call_target="tpu_custom_call" | custom-call | tf_op jit(solution)/shard_map/plane_gather_2/pallas_call | solution.py:128
  188.3 26.5 %first_chain.1 = (f32[64,2048]{1,0:T(8,128)}, f32[64,2048]{1,0:T(8,128)}) custom-call(f32[2048,2048]{1,0:T(8,128)} %bitcast.34, f32[64,2048]{1,0:T(8,128)} %copy-done.1), custom_call_target="tpu_custom_call" | custom-call | tf_op jit(solution)/shard_map/first_chain/pallas_call | solution.py:347
  214.8 1.0 copy-done.3
  215.8 68.2 %plane_gather_3.1 = f32[16,2,64,2048]{3,2,1,0:T(8,128)} custom-call(f32[64,2048]{1,0:T(8,128)S(1)} %copy-done.3), custom_call_target="tpu_custom_call" | custom-call | tf_op jit(solution)/shard_map/plane_gather_3/pallas_call | solution.py:128
  284.1 58.6 %second_chain.1.block = f32[64,2048]{1,0:T(8,128)} custom-call(f32[2048,2048]{1,0:T(8,128)} %bitcast.35, f32[64,2048]{1,0:T(8,128)} %get-tuple-element.9.coef), custom_call_target="tpu_custom_call" | custom-call | tf_op jit(solution)/shard_map/second_chain/pallas_call | solution.py:347
  342.7 1.0 copy-done.2
  343.8 22.7 %spread.1 = f32[4,2,64,2048]{3,2,1,0:T(8,128)S(1)} custom-call(f32[64,2048]{1,0:T(8,128)S(1)} %copy-done.2), custom_call_target="tpu_custom_call" | custom-call | tf_op jit(solution)/shard_map/spread/pallas_call | solution.py:251
  366.7 2.4 fusion.18
  369.5 2.0 fusion.4
  371.5 2.0 fusion
  373.6 1.2 copy.16
  374.7 1.3 fusion.24
  376.0 1.1 copy.18
  377.1 3.0 broadcast_multiply_fusion
  380.1 1.1 copy.19
  (39 shorter events, 2.0 us)
Async XLA Ops:
  0.6 4.1 %copy-start.6 = (f32[128,256]{1,0:T(8,128)S(1)}, f32[128,256]{1,0:T(8,128)}, u32[]{:S(2)}) copy-start(f32[128,256]{1,0:T(8,128)} %param.11) | copy-start | bytes 393220
  0.6 4.0 %copy-start.7 = (f32[128,256]{1,0:T(8,128)S(1)}, f32[128,256]{1,0:T(8,128)}, u32[]{:S(2)}) copy-start(f32[128,256]{1,0:T(8,128)} %param.9) | copy-start | bytes 393220
  4.7 75.6 %copy-start.4 = (f32[128,256]{1,0:T(8,128)}, f32[128,256]{1,0:T(8,128)S(1)}, u32[]{:S(2)}) copy-start(f32[128,256]{1,0:T(8,128)S(1)} %multiply_add_fusion.1) | copy-start | bytes 393220
  80.3 5.2 %copy-start = (f32[16,128,1664]{2,1,0:T(8,128)}, f32[16,128,1664]{2,1,0:T(8,128)S(1)}, u32[]{:S(2)}) copy-start(f32[16,128,1664]{2,1,0:T(8,128)S(1)} %plane_gather_0.1) | copy-start | bytes 40894468
  119.9 68.4 %copy-start.1 = (f32[64,2048]{1,0:T(8,128)}, f32[64,2048]{1,0:T(8,128)S(1)}, u32[]{:S(2)}) copy-start(f32[64,2048]{1,0:T(8,128)S(1)} %reduce_to_planes.1.block.own) | copy-start | bytes 1572868
  214.8 1.0 copy-start.3
  284.1 85.4 %slice-start = ((s8[13631488]{0:T(1024)(128)(4,1)}), s8[1048576]{0:T(1024)(128)(4,1)S(1)}, s32[]{:S(2)}) async-start(s8[13631488]{0:T(1024)(128)(4,1)} %bitcast.30), calls=%async_computation | async-start | bytes 2097152
  284.1 85.4 %slice-start.1 = ((s8[13631488]{0:T(1024)(128)(4,1)}), s8[4194304]{0:T(1024)(128)(4,1)S(1)}, s32[]{:S(2)}) async-start(s8[13631488]{0:T(1024)(128)(4,1)} %bitcast.30), calls=%async_computation.1 | async-start | bytes 8388608
  342.7 1.0 copy-start.2
  343.8 25.7 %slice-start.2 = ((s8[13631488]{0:T(1024)(128)(4,1)}), s8[4194304]{0:T(1024)(128)(4,1)S(1)}, s32[]{:S(2)}) async-start(s8[13631488]{0:T(1024)(128)(4,1)} %bitcast.30), calls=%async_computation.2 | async-start | bytes 8388608
  366.7 2.8 slice-start.3
  371.5 2.1 copy-start.5

commit v2 on v1

--- a/solution.py
+++ b/solution.py
@@ -22,6 +22,8 @@
 
 SIDE = 4
 PLANE = SIDE * SIDE
+LANE = 128
+TURN = PLANE // 2 + 1
 WIDE = 640
 ODD = 64
 MIX = 256
@@ -41,79 +43,86 @@
     pl.semaphore_wait(barrier, len(peers))
 
 
-def ring_place(cycle, z, y):
-    return SIDE * (z if cycle == 0 else y) + lax.rem(z + y, SIDE)
-
-
-def ring_fs(cycle, place):
-    a = place // SIDE
-    b = lax.rem(place - a + SIDE, SIDE)
-    return SIDE * a + b if cycle == 0 else SIDE * b + a
-
-
-def plane_gather_kernel(pieces, paired, block, out, send, recv, own_sem, pair_send, pair_recv):
+def plane_gather_kernel(paired, block, out, send, recv, own_sem, pair_send, pair_recv):
     fs, tp = lax.axis_index("fs"), lax.axis_index("tp")
     z, y = fs // SIDE, lax.rem(fs, SIDE)
     core = lax.rem(tp, 2)
     other = tp + 1 - 2 * core
-    rows, cols = block.shape
-    quarter = rows // 4
-    per_ring = len(pieces)
-    rings = [(cycle, way) for cycle in (0, 1) for way in (1, -1)]
-    place = [ring_place(cycle, z, y) for cycle in (0, 1)]
-    nexts = [ring_fs(c, lax.rem(place[c] + PLANE + w, PLANE)) for c, w in rings]
-    peers = [(n, tp) for n in nexts]
+    half = block.shape[0] // 2
+    quarter = half // 2
+    ways = (1, -1)
+
+    def at(along_y, along_z):
+        return SIDE * lax.rem(z + along_z + SIDE, SIDE) + lax.rem(y + along_y + SIDE, SIDE)
+
+    def near(h, first, second):
+        return at(first, second) if h == 0 else at(second, first)
+
+    peers = [(near(0, w, 0), tp) for w in ways] + [(near(1, w, 0), tp) for w in ways]
     if paired:
         peers.append((fs, other))
     greet(peers)
 
-    def slot(origin, row, height, col, width):
-        where = (origin, core) if paired else (origin,)
-        return out.at[where + (pl.ds(row, height), pl.ds(col, width))]
-
-    def own(row, height, col, width):
-        return block.at[pl.ds(row, height), pl.ds(col, width)]
-
-    def piece_of(k, i):
-        row, height, col, width = pieces[i]
-        return quarter * k + row, height, col, width
-
-    def hop(step, k, i, first):
-        c, w = rings[k]
-        origin = ring_fs(c, lax.rem(place[c] + 2 * PLANE - w * step, PLANE))
-        spot = piece_of(k, i)
-        lane = k * per_ring + i
-        return put(own(*spot) if first else slot(origin, *spot), slot(origin, *spot), send.at[lane], recv.at[lane, step], nexts[k], tp)
-
+    def slot(origin, rows):
+        return out.at[origin, core, rows] if paired else out.at[origin, rows]
+
+    count = iter(range(40))
+    started = []
+
+    def move(origin, rows, target, src=None):
+        lane = next(count)
+        dst = slot(origin, rows)
+        copy = put(dst if src is None else src, dst, send.at[lane], recv.at[lane], target, tp)
+        copy.start()
+        started.append(copy)
+        return copy
+
+    def halves(h):
+        return pl.ds(h * half, half)
+
+    def quarters(h, i):
+        return pl.ds(h * half + i * quarter, quarter)
+
+    def to_pair(origin, rows):
+        if paired:
+            put(slot(origin, rows), slot(origin, rows), pair_send, pair_recv, fs, other).start()
+
+    direct = {(h, i): move(fs, halves(h), near(h, w, 0), block.at[halves(h)]) for i, w in enumerate(ways) for h in (0, 1)}
+    second = {(h, i, 0): move(fs, halves(h), near(h, 0, w), block.at[halves(h)]) for i, w in enumerate(ways) for h in (0, 1)}
     mine = out.at[fs, core] if paired else out.at[fs]
     keep = pltpu.make_async_copy(block, mine, own_sem)
-    for i in range(per_ring):
-        for k in range(4):
-            hop(0, k, i, True).start()
     keep.start()
     if paired:
         put(block, mine, pair_send, pair_recv, fs, other).start()
-
-    def pass_on(step, last):
-        for i in range(per_ring):
-            for k in range(4):
-                before = hop(step - 1, k, i, False)
-                before.wait_send()
-                before.wait_recv()
-                if not last:
-                    hop(step, k, i, False).start()
-        if paired:
-            for k in range(4):
-                c, w = rings[k]
-                origin = ring_fs(c, lax.rem(place[c] + 2 * PLANE - w * step, PLANE))
-                there = slot(origin, quarter * k, quarter, 0, cols)
-                put(there, there, pair_send, pair_recv, fs, other).start()
-
-    @pl.loop(1, PLANE - 1)
-    def _(step):
-        pass_on(step, False)
-
-    pass_on(PLANE - 1, True)
+    relay = {}
+    for i, w in enumerate(ways):
+        for h in (0, 1):
+            direct[h, i].wait_recv()
+            origin = near(h, -w, 0)
+            relay[h, i] = move(origin, quarters(h, i), near(h, w, 0))
+            for j, w2 in enumerate(ways):
+                second[h, j, -w] = move(origin, halves(h), near(h, 0, w2))
+            to_pair(origin, halves(h))
+    for h in (0, 1):
+        for i in (0, 1):
+            relay[h, i].wait_recv()
+        origin = near(h, 2, 0)
+        for j, w2 in enumerate(ways):
+            second[h, j, 2] = move(origin, halves(h), near(h, 0, w2))
+        to_pair(origin, halves(h))
+    tail = []
+    for e in (0, -1, 1, 2):
+        for j, w2 in enumerate(ways):
+            for h in (0, 1):
+                second[h, j, e].wait_recv()
+                origin = near(h, e, -w2)
+                tail.append((h, j, e, move(origin, quarters(h, j), near(h, 0, w2))))
+                to_pair(origin, halves(h))
+    for h, j, e, copy in tail:
+        copy.wait_recv()
+        to_pair(near(h, e, 2), quarters(h, j))
+    for copy in started:
+        copy.wait_send()
     keep.wait()
     if paired:
         sent = put(out.at[:, core], out.at[:, 1 - core], pair_send, pair_recv, fs, other)
@@ -121,28 +130,34 @@
         sent.wait_recv()
 
 
-def plane_gather(block, pieces, paired, cid):
+def plane_gather(block, paired, cid):
     rows, cols = block.shape
     shape = (PLANE, 2, rows, cols) if paired else (PLANE, rows, cols)
-    lanes = 4 * len(pieces)
     return pl.pallas_call(
-        functools.partial(plane_gather_kernel, pieces, paired),
+        functools.partial(plane_gather_kernel, paired),
         out_shape=jax.ShapeDtypeStruct(shape, jnp.float32),
         in_specs=[pl.BlockSpec(memory_space=pltpu.VMEM)],
         out_specs=pl.BlockSpec(memory_space=pltpu.VMEM),
         scratch_shapes=[
-            pltpu.SemaphoreType.DMA((lanes,)),
-            pltpu.SemaphoreType.DMA((lanes, PLANE - 1)),
+            pltpu.SemaphoreType.DMA((40,)),
+            pltpu.SemaphoreType.DMA((40,)),
             pltpu.SemaphoreType.DMA,
             pltpu.SemaphoreType.DMA,
             pltpu.SemaphoreType.DMA,
         ],
-        compiler_params=pltpu.CompilerParams(collective_id=cid, has_side_effects=True, vmem_limit_bytes=40 << 20),
+        compiler_params=pltpu.CompilerParams(collective_id=cid, has_side_effects=True, vmem_limit_bytes=24 << 20),
         name=f"plane_gather_{cid}",
     )(block)
 
 
-def reduce_kernel(part, out, pair, total, near, far, hold, send, recv):
+def turned(rows, dst):
+    fs = lax.axis_index("fs")
+    for b in range(TURN):
+        col = pl.multiple_of(LANE * lax.rem(fs + b, PLANE), LANE)
+        dst[:, pl.ds(LANE * b, LANE)] = rows[:, pl.ds(col, LANE)]
+
+
+def reduce_kernel(part, out, out_turned, pair, total, near, far, hold, send, recv):
     fs, tp = lax.axis_index("fs"), lax.axis_index("tp")
     x, core = tp // 2, lax.rem(tp, 2)
     right = 2 * lax.rem(x + 1, SIDE) + core
@@ -179,6 +194,7 @@
     out[up, :] = total[x, up] + near[2] + near[1]
     on_left.wait_recv()
     out[down, :] = total[x, down] + near[3] + near[0]
+    turned(out, out_turned)
     for c in (far_right, far_left, near_right, near_left, on_right, on_left):
         c.wait_send()
 
@@ -188,9 +204,9 @@
     f32 = jnp.float32
     return pl.pallas_call(
         reduce_kernel,
-        out_shape=jax.ShapeDtypeStruct((rows, cols), f32),
+        out_shape=[jax.ShapeDtypeStruct((rows, cols), f32), jax.ShapeDtypeStruct((rows, TURN * LANE), f32)],
         in_specs=[pl.BlockSpec(memory_space=pltpu.VMEM)],
-        out_specs=pl.BlockSpec(memory_space=pltpu.VMEM),
+        out_specs=[pl.BlockSpec(memory_space=pltpu.VMEM)] * 2,
         scratch_shapes=[
             pltpu.VMEM((3, rows, cols), f32),
             pltpu.VMEM((4, rows, cols), f32),
@@ -265,48 +281,46 @@
     )(block)
 
 
-def split_into(src, scale, high, low):
-    step = 64
-
-    @pl.loop(0, src.shape[0] // step)
+def split(value):
+    top = value.astype(jnp.bfloat16)
+    return top, (value - top.astype(jnp.float32)).astype(jnp.bfloat16)
+
+
+def unturn(src, scale, high, low):
+    @pl.loop(0, PLANE)
     def _(i):
-        rows = pl.ds(pl.multiple_of(i * step, step), step)
-        value = src[rows, :] * scale
-        top = value.astype(jnp.bfloat16)
-        high[rows, :] = top
-        low[rows, :] = (value - top.astype(jnp.float32)).astype(jnp.bfloat16)
+        rows = pl.ds(pl.multiple_of(i * LANE, LANE), LANE)
+        for b in range(TURN):
+            cols = pl.ds(pl.multiple_of(LANE * lax.rem(i + b, PLANE), LANE), LANE)
+            value = src[rows, pl.ds(LANE * b, LANE)] * scale
+            high[rows, cols], low[rows, cols] = split(value)
+            if 0 < b < TURN - 1:
+                high[cols, rows], low[cols, rows] = split(value.T)
 
 
 def times(src, dst, pair, high, low):
     rows, size = src.shape
-    value = src[...]
-    top = value.astype(jnp.bfloat16)
-    pair[:rows, :] = top
-    pair[rows:, :] = (value - top.astype(jnp.float32)).astype(jnp.bfloat16)
-    width = 256
+    pair[:rows, :], pair[rows:, :] = split(src[...])
+    width = 1024
 
     @pl.loop(0, size // width)
     def _(j):
         cols = pl.ds(pl.multiple_of(j * width, width), width)
         main = jnp.dot(pair[...], high[:, cols], preferred_element_type=jnp.float32)
-        rest = jnp.dot(pair[:rows, :], low[:, cols], preferred_element_type=jnp.float32)
-        dst[:, cols] = main[:rows] + (main[rows:] + rest)
+        rest = jnp.dot(pair[...], low[:, cols], preferred_element_type=jnp.float32)
+        dst[:, cols] = main[:rows] + (main[rows:] + (rest[:rows] + rest[rows:]))
 
 
 def first_chain_kernel(whole, own, next_rows, coef_rows, high, low, pair, v, p, w):
-    size = whole.shape[1]
-    lane = 128
-
     def diag(i, total):
-        at = pl.ds(pl.multiple_of(i * lane, lane), lane)
-        block = whole[at, at]
+        block = whole[pl.ds(pl.multiple_of(i * LANE, LANE), LANE), pl.ds(0, LANE)]
         eye = lax.broadcasted_iota(jnp.int32, block.shape, 0) == lax.broadcasted_iota(jnp.int32, block.shape, 1)
         return total + jnp.where(eye, block, 0.0)
 
-    acc = lax.fori_loop(0, size // lane, diag, jnp.zeros((lane, lane), jnp.float32))
+    acc = lax.fori_loop(0, PLANE, diag, jnp.zeros((LANE, LANE), jnp.float32))
     ssq = jnp.sum(jnp.sum(acc, axis=0, keepdims=True), axis=1, keepdims=True)
     s = 0.5 * lax.rsqrt(jnp.maximum(ssq / D, 1.0))
-    split_into(whole, s * s, high, low)
+    unturn(whole, s * s, high, low)
     fs, tp = lax.axis_index("fs"), lax.axis_index("tp")
     start = 128 * fs + 64 * lax.rem(tp, 2)
     shape = own.shape
@@ -318,11 +332,12 @@
     w[...] = A_COEF * v[...] + B_COEF * p[...] + C_COEF * w[...]
     times(w, v, pair, high, low)
     times(v, p, pair, high, low)
-    next_rows[...] = A_COEF * w[...] + B_COEF * v[...] + C_COEF * p[...]
+    w[...] = A_COEF * w[...] + B_COEF * v[...] + C_COEF * p[...]
+    turned(w, next_rows)
 
 
 def second_chain_kernel(whole, coef, out, high, low, pair, base, v, p, q):
-    split_into(whole, 1.0, high, low)
+    unturn(whole, 1.0, high, low)
 
     def by_a1(src, dst):
         times(src, p, pair, high, low)
@@ -330,32 +345,38 @@
         dst[...] = A_COEF * src[...] + B_COEF * p[...] + C_COEF * q[...]
 
     by_a1(coef, base)
+    v[...] = base[...]
     out[...] = A_COEF * base[...]
-    for src, weight in ((base, B_COEF), (v, C_COEF)):
-        times(src, q, pair, high, low)
+
+    @pl.loop(0, 2)
+    def _(power):
+        times(v, q, pair, high, low)
         v[...] = q[...]
-        by_a1(v, v)
-        by_a1(v, v)
-        out[...] += weight * v[...]
-
-
-def chain_call(kernel, whole, own, outs, works, name):
+
+        @pl.loop(0, 2)
+        def _(_):
+            by_a1(v, v)
+
+        out[...] += jnp.where(power == 0, B_COEF, C_COEF) * v[...]
+
+
+def chain_call(kernel, whole, own, widths, works, name):
     rows, cols = own.shape
     size = whole.shape[0]
     f32, bf16 = jnp.float32, jnp.bfloat16
     vmem = pl.BlockSpec(memory_space=pltpu.VMEM)
     return pl.pallas_call(
         kernel,
-        out_shape=[jax.ShapeDtypeStruct((rows, cols), f32)] * outs,
+        out_shape=[jax.ShapeDtypeStruct((rows, width), f32) for width in widths],
         in_specs=[vmem, vmem],
-        out_specs=[vmem] * outs,
+        out_specs=[vmem] * len(widths),
         scratch_shapes=[
             pltpu.VMEM((size, cols), bf16),
             pltpu.VMEM((size, cols), bf16),
             pltpu.VMEM((2 * rows, cols), bf16),
         ]
         + [pltpu.VMEM((rows, cols), f32)] * works,
-        compiler_params=pltpu.CompilerParams(vmem_limit_bytes=56 << 20),
+        compiler_params=pltpu.CompilerParams(vmem_limit_bytes=36 << 20),
         name=name,
     )(whole, own)
 
@@ -372,9 +393,7 @@
     packed = jnp.concatenate(
         [first[:, :WIDE], second[:, :WIDE], first[:, WIDE:], second[:, WIDE:], moment_mix], axis=1
     )
-    x_pieces = tuple((16 * i, 16, 0, PACKED) for i in range(2))
-    g_pieces = tuple((8 * i, 8, 1024 * j, 1024) for i in range(2) for j in range(2))
-    cols = plane_gather(packed, x_pieces, False, 0).reshape(D, PACKED)
+    cols = plane_gather(packed, False, 0).reshape(D, PACKED)
     spans = [slice(0, WIDE), slice(WIDE, 2 * WIDE), slice(2 * WIDE, 2 * WIDE + 2 * ODD), slice(2 * WIDE + 2 * ODD, PACKED)]
     a0, a1, odd, mix = (cols[:, s] for s in spans)
     r0, r1, rodd, rmix = (packed[:, s] for s in spans)
@@ -386,11 +405,11 @@
             dot_t(rmix, mix),
         ]
     ).reshape(3, 2, 64, D)
-    own = reduce_to_planes(part, 1)
-    gram = plane_gather(own, g_pieces, True, 2).reshape(D, D)
-    next_rows, coef = chain_call(first_chain_kernel, gram, own, 2, 3, "first_chain")
-    gram1 = plane_gather(next_rows, g_pieces, True, 3).reshape(D, D)
-    (poly,) = chain_call(second_chain_kernel, gram1, coef, 1, 4, "second_chain")
+    own, sent = reduce_to_planes(part, 1)
+    gram = plane_gather(sent, True, 2).reshape(D, TURN * LANE)
+    sent, coef = chain_call(first_chain_kernel, gram, own, (TURN * LANE, D), 3, "first_chain")
+    gram = plane_gather(sent, True, 3).reshape(D, TURN * LANE)
+    (poly,) = chain_call(second_chain_kernel, gram, coef, (D,), 4, "second_chain")
     polys = spread(poly, 4).reshape(SIDE, 128, D)
     dot = functools.partial(jnp.dot, precision=HIGH)
     odds = dot(polys[:2].reshape(256, D), odd)

time: 382 us -> 269 us (0.70)
  Pallas kernels: 351 us -> 243 us
    pallas_call x6, Pallas kernels: 328 us -> 220 us  [the longest x3 140 us: plane_gather(): pl.pallas_call(functools.partial(plane_gather_kernel, paired), out_shape=...]
    unnamed x30 -> x18, local copies, waits for them, and re-layouts: 9.46 us -> 6.46 us
where the time goes in v2:
time: 269 us
  Pallas kernels  243 us (90%)
  matrix products  15.8 us (6%)
  local copies, waits for them, and re-layouts  7.15 us (3%)
    pallas_call x3, Pallas kernels, plane_gather(): pl.pallas_call(functools.partial(plane_gather_kernel, paired), out_shape=...  140 us
    pallas_call x2, Pallas kernels, chain_call(): pl.pallas_call(kernel, out_shape=[jax.ShapeDtypeStruct((rows, width), f32...  54.2 us
    pallas_call x1, Pallas kernels, reduce_to_planes(): pl.pallas_call(reduce_kernel, out_shape=[jax.ShapeDtypeStruct((rows, cols...  25.9 us
    pallas_call x1, Pallas kernels, spread(): pl.pallas_call(spread_kernel, out_shape=jax.ShapeDtypeStruct((SIDE, 2, ro...  22.7 us
    unnamed x18, local copies, waits for them, and re-layouts  6.46 us

profile of v2, /device:TPU:1, one launch (start us, length us, event | category | flops | bytes accessed | tf_op | source)
XLA Modules:
  0.0 269.1 jit_solution(3993724134580187494)
XLA Ops:
  0.7 1.4 copy.13
  2.1 1.4 copy.12
  3.6 1.1 copy.17
  5.0 76.7 %plane_gather_0.1 = f32[16,128,1664]{2,1,0:T(8,128)S(1)} custom-call(f32[128,1664]{1,0:T(8,128)S(1)} %concatenate.13.block), custom_call_target="tpu_custom_call" | custom-call | tf_op jit(solution)/shard_map/plane_gather_0/pallas_call | solution.py:136
  81.7 1.2 fusion.16
  82.9 0.6 fusion.20
  83.5 2.7 %fusion.11 = f32[128,2048]{1,0:T(8,128)S(1)} fusion(f32[128,2048]{1,0:T(8,128)S(1)} %fusion.20, f32[2048,1664]{1,0:T(8,128)S(1)} %bitcast.25, f32[128,704]{1,0:T(8,128)S(1)} %get-tuple-element.25), kind=kOutput, calls=%fused_computation.10 | convolution fusion | flops 1006895104 | bytes 7667712 | tf_op jit(solution)/shard_map/dot_general | solution.py:404
  86.3 0.6 fusion.22
  86.9 2.7 %fusion.8 = f32[128,2048]{1,0:T(8,128)S(1)} fusion(f32[128,2048]{1,0:T(8,128)S(1)} %fusion.22, f32[2048,1664]{1,0:T(8,128)S(1)} %bitcast.27, f32[128,704]{1,0:T(8,128)S(1)} %get-tuple-element.26), kind=kOutput, calls=%fused_computation.9 | convolution fusion | flops 1006895104 | bytes 7667712 | tf_op jit(solution)/shard_map/dot_general | solution.py:403
  89.7 0.3 pad_maximum_fusion.part
  90.0 25.9 %reduce_to_planes.1 = (f32[64,2048]{1,0:T(8,128)S(1)}, f32[64,1152]{1,0:T(8,128)S(1)}) custom-call(f32[3,2,64,2048]{3,2,1,0:T(8,128)S(1)} %pad_maximum_fusion.part), custom_call_target="tpu_custom_call" | custom-call | tf_op jit(solution)/shard_map/reduce_to_planes/pallas_call | solution.py:205
  115.9 30.8 %plane_gather_2.1 = f32[16,2,64,1152]{3,2,1,0:T(8,128)S(1)} custom-call(f32[64,1152]{1,0:T(8,128)S(1)} %get-tuple-element.10.block), custom_call_target="tpu_custom_call" | custom-call | tf_op jit(solution)/shard_map/plane_gather_2/pallas_call | solution.py:136
  146.7 16.9 %first_chain.1 = (f32[64,1152]{1,0:T(8,128)S(1)}, f32[64,2048]{1,0:T(8,128)S(1)}) custom-call(f32[2048,1152]{1,0:T(8,128)S(1)} %bitcast.32, f32[64,2048]{1,0:T(8,128)S(1)} %get-tuple-element.11.own), custom_call_target="tpu_custom_call" | custom-call | tf_op jit(solution)/shard_map/first_chain/pallas_call | solution.py:368
  163.7 32.2 %plane_gather_3.1 = f32[16,2,64,1152]{3,2,1,0:T(8,128)S(1)} custom-call(f32[64,1152]{1,0:T(8,128)S(1)} %get-tuple-element.12.block), custom_call_target="tpu_custom_call" | custom-call | tf_op jit(solution)/shard_map/plane_gather_3/pallas_call | solution.py:136
  195.9 37.2 %second_chain.1.block = f32[64,2048]{1,0:T(8,128)S(1)} custom-call(f32[2048,1152]{1,0:T(8,128)S(1)} %bitcast.33, f32[64,2048]{1,0:T(8,128)S(1)} %get-tuple-element.13.coef), custom_call_target="tpu_custom_call" | custom-call | tf_op jit(solution)/shard_map/second_chain/pallas_call | solution.py:368
  233.1 22.7 %spread.1 = f32[4,2,64,2048]{3,2,1,0:T(8,128)S(1)} custom-call(f32[64,2048]{1,0:T(8,128)S(1)} %second_chain.1.block), custom_call_target="tpu_custom_call" | custom-call | tf_op jit(solution)/shard_map/spread/pallas_call | solution.py:267
  256.0 1.0 fusion.18
  257.4 2.0 fusion.4
  259.4 2.0 fusion
  261.4 0.9 maximum_bitcast_fusion
  262.6 1.3 fusion.24
  263.9 1.1 copy.18
  265.0 3.0 %broadcast_multiply_fusion = (f32[128,256]{1,0:T(8,128)}, f32[128,256]{1,0:T(8,128)}) fusion(f32[128,256]{1,0:T(8,128)S(1)} %copy-done.3, f32[128,2048]{1,0:T(8,128)S(1)} %bitcast.35, f32[2048,1664]{1,0:T(8,128)} %bitcast.31), kind=kOutput, calls=%fused_computation.32 | convolution fusion | flops 402751488 | bytes 3538944 | tf_op jit(solution)/shard_map/dot_general | solution.py:419
  268.0 1.1 copy.19
  (26 shorter events, 1.1 us)
Async XLA Ops:
  0.6 4.1 %copy-start.4 = (f32[128,256]{1,0:T(8,128)S(1)}, f32[128,256]{1,0:T(8,128)}, u32[]{:S(2)}) copy-start(f32[128,256]{1,0:T(8,128)} %param.11) | copy-start | bytes 393220
  0.6 4.0 %copy-start.5 = (f32[128,256]{1,0:T(8,128)S(1)}, f32[128,256]{1,0:T(8,128)}, u32[]{:S(2)}) copy-start(f32[128,256]{1,0:T(8,128)} %param.9) | copy-start | bytes 393220
  4.7 77.0 %copy-start.1 = (f32[128,256]{1,0:T(8,128)}, f32[128,256]{1,0:T(8,128)S(1)}, u32[]{:S(2)}) copy-start(f32[128,256]{1,0:T(8,128)S(1)} %multiply_add_fusion.1) | copy-start | bytes 393220
  81.7 177.7 %copy-start = (f32[16,128,1664]{2,1,0:T(8,128)}, f32[16,128,1664]{2,1,0:T(8,128)S(1)}, u32[]{:S(2)}) copy-start(f32[16,128,1664]{2,1,0:T(8,128)S(1)} %plane_gather_0.1) | copy-start | bytes 40894468
  259.4 2.9 %copy-start.2 = (f32[2,128,704]{1,2,0:T(8,128)S(1)}, f32[2,128,704]{1,2,0:T(8,128)}, u32[]{:S(2)}) copy-start(f32[2,128,704]{1,2,0:T(8,128)} %param.6) | copy-start | bytes 2162692
  261.4 3.6 %copy-start.3 = (f32[128,256]{1,0:T(8,128)S(1)}, f32[128,256]{1,0:T(8,128)}, u32[]{:S(2)}) copy-start(f32[128,256]{1,0:T(8,128)} %param.7) | copy-start | bytes 393220

commit v3 on v2

--- a/solution.py
+++ b/solution.py
@@ -28,6 +28,11 @@
 ODD = 64
 MIX = 256
 PACKED = 2 * WIDE + 2 * ODD + MIX
+WAYS = (1, -1)
+FAR = (-1, 1, 2)
+CUT = 768
+EARLY = ((-1, 0, PACKED), (1, 0, CUT))
+LATE = ((2, 0, PACKED), (1, CUT, PACKED - CUT))
 
 
 def put(src, dst, send, recv, fs, tp):
@@ -150,26 +155,125 @@
     )(block)
 
 
-def turned(rows, dst):
-    fs = lax.axis_index("fs")
-    for b in range(TURN):
-        col = pl.multiple_of(LANE * lax.rem(fs + b, PLANE), LANE)
-        dst[:, pl.ds(LANE * b, LANE)] = rows[:, pl.ds(col, LANE)]
-
-
-def reduce_kernel(part, out, out_turned, pair, total, near, far, hold, send, recv):
+def places():
     fs, tp = lax.axis_index("fs"), lax.axis_index("tp")
-    x, core = tp // 2, lax.rem(tp, 2)
+    return fs, tp, fs // SIDE, lax.rem(fs, SIDE), tp // 2, lax.rem(tp, 2)
+
+
+def plane_at(z, y, along_z, along_y):
+    return SIDE * lax.rem(z + along_z + SIDE, SIDE) + lax.rem(y + along_y + SIDE, SIDE)
+
+
+def cross_kernel(block, row_y, col_z, send, recv, own):
+    fs, tp, z, y, x, core = places()
+    near = [[plane_at(z, y, 0, w) for w in WAYS], [plane_at(z, y, w, 0) for w in WAYS]]
+    greet([(n, tp) for side in near for n in side])
+    outs, here = (row_y, col_z), (y, z)
+    half = block.shape[0] // 2
+    lane = iter(range(8))
+
+    def move(src, dst, target):
+        i = next(lane)
+        copy = put(src, dst, send.at[i], recv.at[i], target, tp)
+        copy.start()
+        return copy
+
+    direct = {(i, d): move(block, outs[d].at[here[d]], near[d][i]) for i in (0, 1) for d in (0, 1)}
+    keeps = [pltpu.make_async_copy(block, outs[d].at[here[d]], own.at[d]) for d in (0, 1)]
+    for keep in keeps:
+        keep.start()
+    relays = []
+    for i, w in enumerate(WAYS):
+        for d in (0, 1):
+            direct[i, d].wait_recv()
+            part = outs[d].at[lax.rem(here[d] - w + SIDE, SIDE), pl.ds(half * i, half)]
+            relays.append(move(part, part, near[d][i]))
+    for copy in relays:
+        copy.wait()
+    for copy in direct.values():
+        copy.wait_send()
+    for keep in keeps:
+        keep.wait()
+
+
+def cross_gather(block, cid):
+    rows, cols = block.shape
+    vmem = pl.BlockSpec(memory_space=pltpu.VMEM)
+    return pl.pallas_call(
+        cross_kernel,
+        out_shape=[jax.ShapeDtypeStruct((SIDE, rows, cols), jnp.float32)] * 2,
+        in_specs=[vmem],
+        out_specs=[vmem] * 2,
+        scratch_shapes=[pltpu.SemaphoreType.DMA((8,)), pltpu.SemaphoreType.DMA((8,)), pltpu.SemaphoreType.DMA((2,))],
+        compiler_params=pltpu.CompilerParams(collective_id=cid, has_side_effects=True, vmem_limit_bytes=16 << 20),
+        name="cross_gather",
+    )(block)
+
+
+class Rest:
+    def __init__(self, row_y, col_z, spans, slot, send, recv):
+        fs, tp, z, y, x, core = places()
+        self.tp, self.spans, self.slot, self.send, self.recv = tp, spans, slot, send, recv
+        self.sources, self.here = (row_y, col_z), (y, z)
+        self.half = row_y.shape[1] // 2
+        self.near = [[plane_at(z, y, w, 0) for w in WAYS], [plane_at(z, y, 0, w) for w in WAYS]]
+        self.peers = [(n, tp) for side in self.near for n in side]
+        self.count = 0
+        self.started = []
+
+    def move(self, src, dst, target):
+        i = self.count
+        self.count += 1
+        copy = put(src, dst, self.send.at[i], self.recv.at[i], target, self.tp)
+        copy.start()
+        self.started.append(copy)
+        return copy
+
+    def start(self):
+        self.direct = {}
+        for s, (e, col, width) in enumerate(self.spans):
+            for i, w in enumerate(WAYS):
+                for h in (0, 1):
+                    rows = pl.ds(h * self.half, self.half)
+                    block = lax.rem(self.here[h] + e + SIDE, SIDE)
+                    src = self.sources[h].at[block, rows, pl.ds(col, width)]
+                    self.direct[s, i, h] = self.move(src, self.slot(h, s, e, -w, w, 0, self.half), self.near[h][i])
+
+    def relay(self, s):
+        e = self.spans[s][0]
+        part = self.half // 2
+        for i, w in enumerate(WAYS):
+            for h in (0, 1):
+                self.direct[s, i, h].wait_recv()
+                src = self.slot(h, s, e, -w, 0, part * i, part)
+                self.direct[s, i, h, 2] = self.move(src, self.slot(h, s, e, 2, w, part * i, part), self.near[h][i])
+
+    def finish(self):
+        for key, copy in self.direct.items():
+            if len(key) == 4:
+                copy.wait_recv()
+        for copy in self.started:
+            copy.wait_send()
+
+
+def reduce_kernel(part, row_y, col_z, out, rest_a, rest_b, pair, total, near, far, hold, send, recv, rest_send, rest_recv):
+    fs, tp, z, y, x, core = places()
     right = 2 * lax.rem(x + 1, SIDE) + core
     left = 2 * lax.rem(x + SIDE - 1, SIDE) + core
     other = tp + 1 - 2 * core
-    greet([(fs, right), (fs, left), (fs, other)])
-    copies = [put(part.at[m, 1 - core], pair.at[m], send.at[m], recv.at[m], fs, other) for m in range(3)]
+
+    def slot(h, s, e, f, to, row, rows):
+        return (rest_a, rest_b)[s].at[h, FAR.index(f), pl.ds(row, rows)]
+
+    rest = Rest(row_y, col_z, EARLY, slot, rest_send, rest_recv)
+    greet([(fs, right), (fs, left), (fs, other)] + rest.peers)
+    copies = [put(part.at[m, :, 1 - core], pair.at[m], send.at[m], recv.at[m], fs, other) for m in range(3)]
     for c in copies:
         c.start()
+    rest.start()
     for m, c in enumerate(copies):
         c.wait()
-        total[m] = part[m, core] + pair[m]
+        total[m] = part[m, :, core] + pair[m]
     total[3] = jnp.zeros_like(total[3])
     half = total.shape[1] // 2
     up, down = pl.ds(0, half), pl.ds(half, half)
@@ -188,47 +292,70 @@
     hold[1] = far[1] + total[back, down]
     on_left = put(hold.at[1], near.at[3], send.at[8], recv.at[8], fs, left)
     on_left.start()
+    rest.relay(0)
     near_right.wait_recv()
     near_left.wait_recv()
     on_right.wait_recv()
-    out[up, :] = total[x, up] + near[2] + near[1]
     on_left.wait_recv()
-    out[down, :] = total[x, down] + near[3] + near[0]
-    turned(out, out_turned)
+    hold_up, hold_down = pair.at[0, up], pair.at[0, down]
+    hold_up[...] = total[x, up] + near[2] + near[1]
+    hold_down[...] = total[x, down] + near[3] + near[0]
+    for b in range(TURN):
+        chip = lax.rem(fs + b, PLANE)
+        col = pl.multiple_of(LANE * (chip // SIDE), LANE)
+        out[:, pl.ds(LANE * b, LANE)] = pair[0, lax.rem(chip, SIDE), :, pl.ds(col, LANE)]
+    for s in range(1, len(EARLY)):
+        rest.relay(s)
     for c in (far_right, far_left, near_right, near_left, on_right, on_left):
         c.wait_send()
-
-
-def reduce_to_planes(part, cid):
-    rows, cols = part.shape[2:]
+    rest.finish()
+
+
+def reduce_to_planes(part, row_y, col_z, cid):
     f32 = jnp.float32
+    shape = (part.shape[1],) + part.shape[3:]
+    half = (shape[0] // 2,) + shape[1:]
+    rows = row_y.shape[1] // 2
+    vmem = pl.BlockSpec(memory_space=pltpu.VMEM)
+    lanes = 8 * len(EARLY)
     return pl.pallas_call(
         reduce_kernel,
-        out_shape=[jax.ShapeDtypeStruct((rows, cols), f32), jax.ShapeDtypeStruct((rows, TURN * LANE), f32)],
-        in_specs=[pl.BlockSpec(memory_space=pltpu.VMEM)],
-        out_specs=[pl.BlockSpec(memory_space=pltpu.VMEM)] * 2,
+        out_shape=[jax.ShapeDtypeStruct((shape[1], TURN * LANE), f32)]
+        + [jax.ShapeDtypeStruct((2, len(FAR), rows, width), f32) for _, _, width in EARLY],
+        in_specs=[vmem] * 3,
+        out_specs=[vmem] * 3,
         scratch_shapes=[
-            pltpu.VMEM((3, rows, cols), f32),
-            pltpu.VMEM((4, rows, cols), f32),
-            pltpu.VMEM((4, rows // 2, cols), f32),
-            pltpu.VMEM((2, rows // 2, cols), f32),
-            pltpu.VMEM((2, rows // 2, cols), f32),
+            pltpu.VMEM((3,) + shape, f32),
+            pltpu.VMEM((4,) + shape, f32),
+            pltpu.VMEM((4,) + half, f32),
+            pltpu.VMEM((2,) + half, f32),
+            pltpu.VMEM((2,) + half, f32),
             pltpu.SemaphoreType.DMA((9,)),
             pltpu.SemaphoreType.DMA((9,)),
+            pltpu.SemaphoreType.DMA((lanes,)),
+            pltpu.SemaphoreType.DMA((lanes,)),
         ],
         compiler_params=pltpu.CompilerParams(collective_id=cid, has_side_effects=True, vmem_limit_bytes=32 << 20),
         name="reduce_to_planes",
-    )(part)
-
-
-def spread_kernel(block, out, send, recv, own_sem, pair_send, pair_recv):
-    fs, tp = lax.axis_index("fs"), lax.axis_index("tp")
-    x, core = tp // 2, lax.rem(tp, 2)
+    )(part, row_y, col_z)
+
+
+def spread_kernel(block, row_y, col_z, rest_a, rest_b, out, full, send, recv, own, pair_send, pair_recv, rest_send, rest_recv):
+    fs, tp, z, y, x, core = places()
     right = 2 * lax.rem(x + 1, SIDE) + core
     left = 2 * lax.rem(x + SIDE - 1, SIDE) + core
     other = tp + 1 - 2 * core
     ahead, back, across = lax.rem(x + 1, SIDE), lax.rem(x + SIDE - 1, SIDE), lax.rem(x + 2, SIDE)
-    greet([(fs, right), (fs, left), (fs, other)])
+
+    def origin(h, e, f):
+        return plane_at(z, y, f, e) if h == 0 else plane_at(z, y, e, f)
+
+    def slot(h, s, e, f, to, row, rows):
+        _, col, width = LATE[s]
+        return full.at[origin(h, e, f + to), pl.ds(h * rest.half + row, rows), pl.ds(col, width)]
+
+    rest = Rest(row_y, col_z, LATE, slot, rest_send, rest_recv)
+    greet([(fs, right), (fs, left), (fs, other)] + rest.peers)
     half = block.shape[0] // 2
     parts = [pl.ds(0, half), pl.ds(half, half)]
     go_right = [put(block.at[parts[h]], out.at[x, core, parts[h]], send.at[h], recv.at[h], fs, right) for h in (0, 1)]
@@ -236,8 +363,18 @@
     for h in (0, 1):
         go_right[h].start()
         go_left[h].start()
-    keep = pltpu.make_async_copy(block, out.at[x, core], own_sem)
-    keep.start()
+    rest.start()
+    moves = [(block, out.at[x, core])]
+    moves += [(row_y.at[lax.rem(y + e + SIDE, SIDE)], full.at[plane_at(z, y, 0, e)]) for e in (0,) + FAR]
+    moves += [(col_z.at[lax.rem(z + e + SIDE, SIDE)], full.at[plane_at(z, y, e, 0)]) for e in FAR]
+    for buf, (e, col, width) in zip((rest_a, rest_b), EARLY):
+        for h in (0, 1):
+            for i, f in enumerate(FAR):
+                dst = full.at[origin(h, e, f), pl.ds(h * rest.half, rest.half), pl.ds(col, width)]
+                moves.append((buf.at[h, i], dst))
+    keeps = [pltpu.make_async_copy(src, dst, own.at[i]) for i, (src, dst) in enumerate(moves)]
+    for keep in keeps:
+        keep.start()
     put(block, out.at[x, core], pair_send, pair_recv, fs, other).start()
     go_right[0].wait_recv()
     first = out.at[back, core, parts[0]]
@@ -247,38 +384,57 @@
     second = out.at[ahead, core, parts[1]]
     relay_left = put(second, second, send.at[5], recv.at[5], fs, left)
     relay_left.start()
+    rest.relay(0)
     go_right[1].wait_recv()
     put(out.at[back, core], out.at[back, core], pair_send, pair_recv, fs, other).start()
     go_left[1].wait_recv()
     put(out.at[ahead, core], out.at[ahead, core], pair_send, pair_recv, fs, other).start()
+    for s in range(1, len(LATE)):
+        rest.relay(s)
     relay_right.wait_recv()
     relay_left.wait_recv()
     put(out.at[across, core], out.at[across, core], pair_send, pair_recv, fs, other).start()
     for c in go_right + go_left + [relay_right, relay_left]:
         c.wait_send()
-    keep.wait()
+    for keep in keeps:
+        keep.wait()
+    rest.finish()
     whole = put(out.at[:, core], out.at[:, 1 - core], pair_send, pair_recv, fs, other)
     whole.wait_send()
     whole.wait_recv()
 
 
-def spread(block, cid):
+def spread(block, row_y, col_z, rest_a, rest_b, cid):
     rows, cols = block.shape
+    vmem = pl.BlockSpec(memory_space=pltpu.VMEM)
+    lanes = 8 * len(LATE)
     return pl.pallas_call(
         spread_kernel,
-        out_shape=jax.ShapeDtypeStruct((SIDE, 2, rows, cols), jnp.float32),
-        in_specs=[pl.BlockSpec(memory_space=pltpu.VMEM)],
-        out_specs=pl.BlockSpec(memory_space=pltpu.VMEM),
+        out_shape=[
+            jax.ShapeDtypeStruct((SIDE, 2, rows, cols), jnp.float32),
+            jax.ShapeDtypeStruct((PLANE,) + row_y.shape[1:], jnp.float32),
+        ],
+        in_specs=[vmem] * 5,
+        out_specs=[vmem] * 2,
         scratch_shapes=[
             pltpu.SemaphoreType.DMA((6,)),
             pltpu.SemaphoreType.DMA((6,)),
+            pltpu.SemaphoreType.DMA((8 + 12,)),
             pltpu.SemaphoreType.DMA,
             pltpu.SemaphoreType.DMA,
-            pltpu.SemaphoreType.DMA,
+            pltpu.SemaphoreType.DMA((lanes,)),
+            pltpu.SemaphoreType.DMA((lanes,)),
         ],
-        compiler_params=pltpu.CompilerParams(collective_id=cid, has_side_effects=True, vmem_limit_bytes=32 << 20),
+        compiler_params=pltpu.CompilerParams(collective_id=cid, has_side_effects=True, vmem_limit_bytes=44 << 20),
         name="spread",
-    )(block)
+    )(block, row_y, col_z, rest_a, rest_b)
+
+
+def turned(rows, dst):
+    fs = lax.axis_index("fs")
+    for b in range(TURN):
+        col = pl.multiple_of(LANE * lax.rem(fs + b, PLANE), LANE)
+        dst[:, pl.ds(LANE * b, LANE)] = rows[:, pl.ds(col, LANE)]
 
 
 def split(value):
@@ -286,13 +442,19 @@
     return top, (value - top.astype(jnp.float32)).astype(jnp.bfloat16)
 
 
-def unturn(src, scale, high, low):
+def unturn(src, scale, high, low, crossed):
     @pl.loop(0, PLANE)
     def _(i):
-        rows = pl.ds(pl.multiple_of(i * LANE, LANE), LANE)
+        sent = pl.ds(pl.multiple_of(i * LANE, LANE), LANE)
         for b in range(TURN):
-            cols = pl.ds(pl.multiple_of(LANE * lax.rem(i + b, PLANE), LANE), LANE)
-            value = src[rows, pl.ds(LANE * b, LANE)] * scale
+            j = lax.rem(i + b, PLANE)
+            row, col = i, j
+            if crossed:
+                row = i - lax.rem(i, SIDE) + lax.rem(j, SIDE)
+                col = j - lax.rem(j, SIDE) + lax.rem(i, SIDE)
+            rows = pl.ds(pl.multiple_of(LANE * row, LANE), LANE)
+            cols = pl.ds(pl.multiple_of(LANE * col, LANE), LANE)
+            value = src[sent, pl.ds(LANE * b, LANE)] * scale
             high[rows, cols], low[rows, cols] = split(value)
             if 0 < b < TURN - 1:
                 high[cols, rows], low[cols, rows] = split(value.T)
@@ -311,7 +473,7 @@
         dst[:, cols] = main[:rows] + (main[rows:] + (rest[:rows] + rest[rows:]))
 
 
-def first_chain_kernel(whole, own, next_rows, coef_rows, high, low, pair, v, p, w):
+def first_chain_kernel(whole, next_rows, coef_rows, high, low, pair, v, p, w):
     def diag(i, total):
         block = whole[pl.ds(pl.multiple_of(i * LANE, LANE), LANE), pl.ds(0, LANE)]
         eye = lax.broadcasted_iota(jnp.int32, block.shape, 0) == lax.broadcasted_iota(jnp.int32, block.shape, 1)
@@ -320,12 +482,13 @@
     acc = lax.fori_loop(0, PLANE, diag, jnp.zeros((LANE, LANE), jnp.float32))
     ssq = jnp.sum(jnp.sum(acc, axis=0, keepdims=True), axis=1, keepdims=True)
     s = 0.5 * lax.rsqrt(jnp.maximum(ssq / D, 1.0))
-    unturn(whole, s * s, high, low)
+    unturn(whole, s * s, high, low, True)
     fs, tp = lax.axis_index("fs"), lax.axis_index("tp")
-    start = 128 * fs + 64 * lax.rem(tp, 2)
-    shape = own.shape
+    shape = v.shape
+    start = pl.multiple_of(128 * fs + 64 * lax.rem(tp, 2), 64)
     on_diag = lax.broadcasted_iota(jnp.int32, shape, 1) == start + lax.broadcasted_iota(jnp.int32, shape, 0)
-    v[...] = own[...] * (s * s)
+    mine = pl.ds(start, shape[0])
+    v[...] = high[mine, :].astype(jnp.float32) + low[mine, :].astype(jnp.float32)
     times(v, p, pair, high, low)
     coef_rows[...] = s * (jnp.where(on_diag, A_COEF, 0.0) + B_COEF * v[...] + C_COEF * p[...])
     times(p, w, pair, high, low)
@@ -337,7 +500,7 @@
 
 
 def second_chain_kernel(whole, coef, out, high, low, pair, base, v, p, q):
-    unturn(whole, 1.0, high, low)
+    unturn(whole, 1.0, high, low, False)
 
     def by_a1(src, dst):
         times(src, p, pair, high, low)
@@ -360,25 +523,21 @@
         out[...] += jnp.where(power == 0, B_COEF, C_COEF) * v[...]
 
 
-def chain_call(kernel, whole, own, widths, works, name):
-    rows, cols = own.shape
-    size = whole.shape[0]
+def chain_call(kernel, args, widths, works, name):
+    size, rows = D, 64
     f32, bf16 = jnp.float32, jnp.bfloat16
     vmem = pl.BlockSpec(memory_space=pltpu.VMEM)
     return pl.pallas_call(
         kernel,
         out_shape=[jax.ShapeDtypeStruct((rows, width), f32) for width in widths],
-        in_specs=[vmem, vmem],
+        in_specs=[vmem] * len(args),
         out_specs=[vmem] * len(widths),
-        scratch_shapes=[
-            pltpu.VMEM((size, cols), bf16),
-            pltpu.VMEM((size, cols), bf16),
-            pltpu.VMEM((2 * rows, cols), bf16),
-        ]
-        + [pltpu.VMEM((rows, cols), f32)] * works,
+        scratch_shapes=[pltpu.VMEM((size, size), bf16)] * 2
+        + [pltpu.VMEM((2 * rows, size), bf16)]
+        + [pltpu.VMEM((rows, size), f32)] * works,
         compiler_params=pltpu.CompilerParams(vmem_limit_bytes=36 << 20),
         name=name,
-    )(whole, own)
+    )(*args)
 
 
 def only(lanes_low, x):
@@ -393,24 +552,26 @@
     packed = jnp.concatenate(
         [first[:, :WIDE], second[:, :WIDE], first[:, WIDE:], second[:, WIDE:], moment_mix], axis=1
     )
-    cols = plane_gather(packed, False, 0).reshape(D, PACKED)
+    row_y, col_z = cross_gather(packed, 0)
     spans = [slice(0, WIDE), slice(WIDE, 2 * WIDE), slice(2 * WIDE, 2 * WIDE + 2 * ODD), slice(2 * WIDE + 2 * ODD, PACKED)]
-    a0, a1, odd, mix = (cols[:, s] for s in spans)
-    r0, r1, rodd, rmix = (packed[:, s] for s in spans)
+    l0, l1, lodd, lmix = (row_y.reshape(-1, PACKED)[:, s] for s in spans)
+    r0, r1, rodd, rmix = (col_z.reshape(-1, PACKED)[:, s] for s in spans)
     dot_t = functools.partial(lax.dot_general, dimension_numbers=(((1,), (1,)), ((), ())), precision=HIGH)
     part = jnp.stack(
         [
-            dot_t(r0, a0) + dot_t(only(True, rodd), odd),
-            dot_t(r1, a1) + dot_t(only(False, rodd), odd),
-            dot_t(rmix, mix),
+            dot_t(l0, r0) + dot_t(only(True, lodd), rodd),
+            dot_t(l1, r1) + dot_t(only(False, lodd), rodd),
+            dot_t(lmix, rmix),
         ]
-    ).reshape(3, 2, 64, D)
-    own, sent = reduce_to_planes(part, 1)
+    ).reshape(3, SIDE, 2, 64, SIDE * LANE)
+    sent, rest_a, rest_b = reduce_to_planes(part, row_y, col_z, 1)
     gram = plane_gather(sent, True, 2).reshape(D, TURN * LANE)
-    sent, coef = chain_call(first_chain_kernel, gram, own, (TURN * LANE, D), 3, "first_chain")
+    sent, coef = chain_call(first_chain_kernel, (gram,), (TURN * LANE, D), 3, "first_chain")
     gram = plane_gather(sent, True, 3).reshape(D, TURN * LANE)
-    (poly,) = chain_call(second_chain_kernel, gram, coef, (D,), 4, "second_chain")
-    polys = spread(poly, 4).reshape(SIDE, 128, D)
+    (poly,) = chain_call(second_chain_kernel, (gram, coef), (D,), 4, "second_chain")
+    polys, cols = spread(poly, row_y, col_z, rest_a, rest_b, 4)
+    polys = polys.reshape(SIDE, 128, D)
+    a0, a1, odd, mix = (cols.reshape(D, PACKED)[:, s] for s in spans)
     dot = functools.partial(jnp.dot, precision=HIGH)
     odds = dot(polys[:2].reshape(256, D), odd)
     y0 = jnp.concatenate([dot(polys[0], a0), odds[:128, :ODD]], axis=1)

time: 269 us -> 247 us (0.918)
  Pallas kernels: 243 us -> 217 us
  local copies, waits for them, and re-layouts: 7.15 us -> 11 us
    pallas_call x3 -> x2, Pallas kernels: 140 us -> 62.1 us  [plane_gather(): pl.pallas_call(functools.partial(plane_gather_kernel, paired), out_shape=...]
    pallas_call x2 -> x3, Pallas kernels: 48.6 us -> 101 us  [the longest x1 35 us: cross_gather(): pl.pallas_call(cross_kernel, out_shape=[jax.ShapeDtypeStruct((SIDE, rows,...]
    dot_general x5, matrix products: 7.87 us -> 4.65 us  [the longest x1 1.44 us: local(): dot_t(l0, r0) + dot_t(only(True, lodd), rodd)]
    unnamed x18 -> x20, local copies, waits for them, and re-layouts: 6.46 us -> 6.47 us
where the time goes in v3:
time: 247 us
  Pallas kernels  217 us (88%)
  matrix products  14.6 us (6%)
  local copies, waits for them, and re-layouts  11 us (4%)
  other arithmetic  2.78 us (1%)
    pallas_call x2, Pallas kernels, plane_gather(): pl.pallas_call(functools.partial(plane_gather_kernel, paired), out_shape=...  62.1 us
    pallas_call x2, Pallas kernels, chain_call(): pl.pallas_call(kernel, out_shape=[jax.ShapeDtypeStruct((rows, width), f32...  54.2 us
    pallas_call x1, Pallas kernels, cross_gather(): pl.pallas_call(cross_kernel, out_shape=[jax.ShapeDtypeStruct((SIDE, rows,...  35 us
    pallas_call x1, Pallas kernels, spread(): pl.pallas_call(spread_kernel, out_shape=[jax.ShapeDtypeStruct((SIDE, 2, r...  34.7 us
    pallas_call x1, Pallas kernels, reduce_to_planes(): pl.pallas_call(reduce_kernel, out_shape=[jax.ShapeDtypeStruct((shape[1],...  31.5 us
    unnamed x20, local copies, waits for them, and re-layouts  6.47 us

profile of v3, /device:TPU:1, one launch (start us, length us, event | category | flops | bytes accessed | tf_op | source)
XLA Modules:
  0.0 246.8 jit_solution(9130420994516748274)
XLA Ops:
  0.7 1.4 copy.13
  2.1 1.4 copy.12
  3.6 1.1 copy.17
  5.0 35.0 %cross_gather.1 = (f32[4,128,1664]{2,1,0:T(8,128)S(1)}, f32[4,128,1664]{2,1,0:T(8,128)S(1)}) custom-call(f32[128,1664]{1,0:T(8,128)S(1)} %concatenate.10.block), custom_call_target="tpu_custom_call" | custom-call | tf_op jit(solution)/shard_map/cross_gather/pallas_call | solution.py:202
  40.0 0.6 fusion.15
  40.6 1.4 fusion.6
  42.1 0.6 convolution_add_fusion
  42.7 1.4 fusion.9
  45.2 31.5 %reduce_to_planes.1 = (f32[64,1152]{1,0:T(8,128)S(1)}, f32[2,3,64,1664]{3,2,1,0:T(8,128)S(1)}, f32[2,3,64,768]{3,2,1,0:T(8,128)S(1)}) custom-call(f32[3,4,2,64,512]{4,3,2,1,0:T(8,128)S(1)} %pad_maximum_fusion.part, f32[4,128,1664]{2,1,0:T(8,128)S(1)} %get-tuple-element.15.row_y, f32[4,128,1664]{2,1,0:T(8,128)S(1)} %get-tuple-element.16.col_z), custom_call_target="tpu_custom_call" | custom-call | tf_op jit(solution)/shard_map/reduce_to_planes/pallas_call | solution.py:321
  76.7 30.6 %plane_gather_2.1 = f32[16,2,64,1152]{3,2,1,0:T(8,128)S(1)} custom-call(f32[64,1152]{1,0:T(8,128)S(1)} %get-tuple-element.17.block), custom_call_target="tpu_custom_call" | custom-call | tf_op jit(solution)/shard_map/plane_gather_2/pallas_call | solution.py:141
  107.3 16.9 %first_chain.1 = (f32[64,1152]{1,0:T(8,128)S(1)}, f32[64,2048]{1,0:T(8,128)S(1)}) custom-call(f32[2048,1152]{1,0:T(8,128)S(1)} %bitcast.24), custom_call_target="tpu_custom_call" | custom-call | tf_op jit(solution)/shard_map/first_chain/pallas_call | solution.py:530
  124.3 31.4 %plane_gather_3.1 = f32[16,2,64,1152]{3,2,1,0:T(8,128)S(1)} custom-call(f32[64,1152]{1,0:T(8,128)S(1)} %get-tuple-element.18.block), custom_call_target="tpu_custom_call" | custom-call | tf_op jit(solution)/shard_map/plane_gather_3/pallas_call | solution.py:141
  155.7 37.2 %second_chain.1.block = f32[64,2048]{1,0:T(8,128)S(1)} custom-call(f32[2048,1152]{1,0:T(8,128)S(1)} %bitcast.25, f32[64,2048]{1,0:T(8,128)S(1)} %get-tuple-element.19.coef), custom_call_target="tpu_custom_call" | custom-call | tf_op jit(solution)/shard_map/second_chain/pallas_call | solution.py:530
  192.9 34.7 %spread.1 = (f32[4,2,64,2048]{3,2,1,0:T(8,128)}, f32[16,128,1664]{2,1,0:T(8,128)}) custom-call(f32[64,2048]{1,0:T(8,128)S(1)} %second_chain.1.block, f32[4,128,1664]{2,1,0:T(8,128)S(1)} %get-tuple-element.15.row_y, f32[4,128,1664]{2,1,0:T(8,128)} %copy-done, f32[2,3,64,1664]{3,2,1,0:T(8,128)S(1)} %get-tuple-element.20.rest_a, ...), custom_call_target="tpu_custom_call" | custom-call | tf_op jit(solution)/shard_map/spread/pallas_call | solution.py:411
  227.7 1.9 slice.92
  229.6 2.5 %fusion.12 = f32[256,128]{1,0:T(8,128)S(1)} fusion(f32[256,2048]{1,0:T(8,128)S(1)} %bitcast.40, f32[2048,1664]{1,0:T(8,128)} %bitcast.36), kind=kOutput, calls=%fused_computation.15 | convolution fusion | flops 402653184 | bytes 3276800 | tf_op jit(solution)/shard_map/dot_general | solution.py:576
  232.2 2.4 fusion.30
  234.6 2.2 fusion.2
  236.9 2.2 fusion
  239.1 0.9 maximum_bitcast_fusion
  240.3 1.3 fusion.14
  241.6 1.1 copy.18
  242.7 3.0 %broadcast_multiply_fusion = (f32[128,256]{1,0:T(8,128)}, f32[128,256]{1,0:T(8,128)}) fusion(f32[128,256]{1,0:T(8,128)S(1)} %copy-done.4, f32[128,2048]{1,0:T(8,128)S(1)} %bitcast.41, f32[2048,1664]{1,0:T(8,128)} %bitcast.37), kind=kOutput, calls=%fused_computation.40 | convolution fusion | flops 402751488 | bytes 3538944 | tf_op jit(solution)/shard_map/dot_general | solution.py:580
  245.7 1.1 copy.19
  (28 shorter events, 1.7 us)
Async XLA Ops:
  0.6 4.1 %copy-start.5 = (f32[128,256]{1,0:T(8,128)S(1)}, f32[128,256]{1,0:T(8,128)}, u32[]{:S(2)}) copy-start(f32[128,256]{1,0:T(8,128)} %param.11) | copy-start | bytes 393220
  0.6 4.0 %copy-start.6 = (f32[128,256]{1,0:T(8,128)S(1)}, f32[128,256]{1,0:T(8,128)}, u32[]{:S(2)}) copy-start(f32[128,256]{1,0:T(8,128)} %param.9) | copy-start | bytes 393220
  4.7 35.9 %copy-start.3 = (f32[128,256]{1,0:T(8,128)}, f32[128,256]{1,0:T(8,128)S(1)}, u32[]{:S(2)}) copy-start(f32[128,256]{1,0:T(8,128)S(1)} %multiply_add_fusion.1) | copy-start | bytes 393220
  40.0 5.2 %copy-start = (f32[4,128,1664]{2,1,0:T(8,128)}, f32[4,128,1664]{2,1,0:T(8,128)S(1)}, u32[]{:S(2)}) copy-start(f32[4,128,1664]{2,1,0:T(8,128)S(1)} %get-tuple-element.16.col_z) | copy-start | bytes 10223620
  227.7 6.9 %copy-start.1 = (f32[16,128,1664]{2,1,0:T(8,128)S(1)}, f32[16,128,1664]{2,1,0:T(8,128)}, u32[]{:S(2)}) copy-start(f32[16,128,1664]{2,1,0:T(8,128)} %get-tuple-element.23) | copy-start | bytes 40894468
  236.9 3.2 %copy-start.2 = (f32[2,128,704]{1,2,0:T(8,128)S(1)}, f32[2,128,704]{1,2,0:T(8,128)}, u32[]{:S(2)}) copy-start(f32[2,128,704]{1,2,0:T(8,128)} %param.6) | copy-start | bytes 2162692
  240.0 2.7 %copy-start.4 = (f32[128,256]{1,0:T(8,128)S(1)}, f32[128,256]{1,0:T(8,128)}, u32[]{:S(2)}) copy-start(f32[128,256]{1,0:T(8,128)} %param.7) | copy-start | bytes 393220

commit v4 on v3

v4 whole, which is shorter than its diff:
```python
import functools
import math

import jax
import jax.numpy as jnp
from jax import lax
from jax.experimental import pallas as pl
from jax.experimental.pallas import tpu as pltpu
from jax.sharding import PartitionSpec as P

D = 2048
FF = 5632
ITERS = 3

A_COEF = 3.4445
B_COEF = -4.775
C_COEF = 2.0315
MOMENTUM_DECAY = 0.95
STEP_RATE = 0.02
HIGH = lax.Precision.HIGH
MESH = pl.DeviceIdType.MESH
ANY = pl.BlockSpec(memory_space=pl.ANY)

SIDE = 4
PLANE = SIDE * SIDE
LANE = 128
TURN = PLANE // 2 + 1
WIDE = 640
ODD = 64
MIX = 256
FFB = WIDE + ODD
PACKED = 2 * FFB + MIX
WAYS = (1, -1)
FAR = (-1, 1, 2)
CUT = 768
EARLY = ((-1, 0, CUT),)
AMID = ((1, 0, PACKED), (2, 0, PACKED))
LATE = ((-1, CUT, PACKED - CUT),)


def put(src, dst, send, recv, fs, tp):
    return pltpu.make_async_remote_copy(
        src_ref=src, dst_ref=dst, send_sem=send, recv_sem=recv, device_id=(fs, tp), device_id_type=MESH
    )


def greet(peers):
    barrier = pltpu.get_barrier_semaphore()
    for fs, tp in peers:
        pl.semaphore_signal(barrier, inc=1, device_id=(fs, tp), device_id_type=MESH)
    pl.semaphore_wait(barrier, len(peers))


def plane_gather(block, buf, high, low, crossed, send, recv, own_sem, pair_send, pair_recv):
    fs, tp, z, y, x, core = places()
    other = tp + 1 - 2 * core
    half = block.shape[0] // 2
    quarter = half // 2

    def near(h, first, second):
        return plane_at(z, y, second, first) if h == 0 else plane_at(z, y, first, second)

    started, moves, pairs = [], iter(range(40)), {}

    def move(origin, rows, target, src=None):
        lane = next(moves)
        dst = buf.at[origin, core, rows]
        copy = put(dst if src is None else src, dst, send.at[lane], recv.at[lane], target, tp)
        copy.start()
        started.append(copy)
        return copy

    def halves(h):
        return pl.ds(h * half, half)

    def quarters(h, i):
        return pl.ds(h * half + i * quarter, quarter)

    def to_pair(along_z, along_y, src=None):
        at = buf.at[plane_at(z, y, along_z, along_y), core]
        k = len(pairs)
        copy = put(at if src is None else src, at, pair_send.at[k], pair_recv.at[k], fs, other)
        copy.start()
        pairs[along_z, along_y] = copy
        started.append(copy)

    direct = {(h, i): move(fs, halves(h), near(h, w, 0), block.at[halves(h)]) for i, w in enumerate(WAYS) for h in (0, 1)}
    second = {(h, i, 0): move(fs, halves(h), near(h, 0, w), block.at[halves(h)]) for i, w in enumerate(WAYS) for h in (0, 1)}
    keep = pltpu.make_async_copy(block, buf.at[fs, core], own_sem)
    keep.start()
    to_pair(0, 0, block)
    relay = {}
    for i, w in enumerate(WAYS):
        for h in (0, 1):
            direct[h, i].wait_recv()
            origin = near(h, -w, 0)
            relay[h, i] = move(origin, quarters(h, i), near(h, w, 0))
            for j, w2 in enumerate(WAYS):
                second[h, j, -w] = move(origin, halves(h), near(h, 0, w2))
    for h in (0, 1):
        for i in (0, 1):
            relay[h, i].wait_recv()
        origin = near(h, 2, 0)
        for j, w2 in enumerate(WAYS):
            second[h, j, 2] = move(origin, halves(h), near(h, 0, w2))
    tail = {}
    for e in (0, -1, 1, 2):
        for j, w2 in enumerate(WAYS):
            for h in (0, 1):
                second[h, j, e].wait_recv()
                tail[h, j, e] = move(near(h, e, -w2), quarters(h, j), near(h, 0, w2))
        if e == 0:
            for w in WAYS:
                to_pair(0, w)
                to_pair(w, 0)
        if e == 1:
            for w in WAYS:
                for w2 in WAYS:
                    to_pair(w, w2)

    def rebuild(i):
        sent = buf.at[i]
        for b in range(TURN):
            j = lax.rem(i + b, PLANE)
            row, col = i, j
            if crossed:
                row = SIDE * (i // SIDE) + lax.rem(j, SIDE)
                col = SIDE * (j // SIDE) + lax.rem(i, SIDE)
            rows = pl.ds(pl.multiple_of(LANE * row, LANE), LANE)
            cols = pl.ds(pl.multiple_of(LANE * col, LANE), LANE)
            value = sent[:, :, pl.ds(LANE * b, LANE)].reshape(LANE, LANE)
            high[rows, cols], low[rows, cols] = split(value)
            if 0 < b < TURN - 1:
                high[cols, rows], low[cols, rows] = split(value.T)

    keep.wait()
    for copy in pairs.values():
        copy.wait_recv()

    @pl.loop(0, 9)
    def _(n):
        rebuild(plane_at(z, y, n // 3 - 1, lax.rem(n, 3) - 1))

    for e in (0, -1, 1, 2):
        for j in (0, 1):
            for h in (0, 1):
                tail[h, j, e].wait_recv()
        to_pair(2, e)
        if e != 2:
            to_pair(e, 2)
    for e in FAR[:2] + (0,):
        pairs[e, 2].wait_recv()
        pairs[2, e].wait_recv()

    @pl.loop(0, 3)
    def _(n):
        rebuild(plane_at(z, y, n - 1, 2))

    pairs[2, 2].wait_recv()

    @pl.loop(0, 4)
    def _(n):
        rebuild(plane_at(z, y, 2, n - 1))

    for copy in started:
        copy.wait_send()


def places():
    fs, tp = lax.axis_index("fs"), lax.axis_index("tp")
    return fs, tp, fs // SIDE, lax.rem(fs, SIDE), tp // 2, lax.rem(tp, 2)


def plane_at(z, y, along_z, along_y):
    return SIDE * lax.rem(z + along_z + SIDE, SIDE) + lax.rem(y + along_y + SIDE, SIDE)


def cross_kernel(block, row_y, col_z, send, recv, own):
    fs, tp, z, y, x, core = places()
    near = [[plane_at(z, y, 0, w) for w in WAYS], [plane_at(z, y, w, 0) for w in WAYS]]
    greet([(n, tp) for side in near for n in side])
    outs, here = (row_y, col_z), (y, z)
    half = block.shape[0] // 2
    lane = iter(range(12))

    def move(src, dst, target):
        i = next(lane)
        copy = put(src, dst, send.at[i], recv.at[i], target, tp)
        copy.start()
        return copy

    parts = [pl.ds(0, half), pl.ds(half, half)]
    direct = {
        (i, d, k): move(block.at[parts[(i + k) % 2]], outs[d].at[here[d], parts[(i + k) % 2]], near[d][i])
        for k in (0, 1)
        for i in (0, 1)
        for d in (0, 1)
    }
    keeps = [pltpu.make_async_copy(block, outs[d].at[here[d]], own.at[d]) for d in (0, 1)]
    for keep in keeps:
        keep.start()
    relays = []
    for i, w in enumerate(WAYS):
        for d in (0, 1):
            direct[i, d, 0].wait_recv()
            part = outs[d].at[lax.rem(here[d] - w + SIDE, SIDE), parts[i]]
            relays.append(move(part, part, near[d][i]))
    for (i, d, k), copy in direct.items():
        copy.wait_send()
        if k == 1:
            copy.wait_recv()
    for copy in relays:
        copy.wait()
    for keep in keeps:
        keep.wait()


def cross_gather(block, cid):
    rows, cols = block.shape
    vmem = pl.BlockSpec(memory_space=pltpu.VMEM)
    return pl.pallas_call(
        cross_kernel,
        out_shape=[jax.ShapeDtypeStruct((SIDE, rows, cols), jnp.float32)] * 2,
        in_specs=[vmem],
        out_specs=[vmem] * 2,
        scratch_shapes=[pltpu.SemaphoreType.DMA((12,)), pltpu.SemaphoreType.DMA((12,)), pltpu.SemaphoreType.DMA((2,))],
        compiler_params=pltpu.CompilerParams(collective_id=cid, has_side_effects=True, vmem_limit_bytes=16 << 20),
        name="cross_gather",
    )(block)


class Rest:
    def __init__(self, row_y, col_z, spans, slot, send, recv):
        fs, tp, z, y, x, core = places()
        self.tp, self.spans, self.slot, self.send, self.recv = tp, spans, slot, send, recv
        self.sources, self.here = (row_y, col_z), (y, z)
        self.half = row_y.shape[1] // 2
        self.near = [[plane_at(z, y, w, 0) for w in WAYS], [plane_at(z, y, 0, w) for w in WAYS]]
        self.peers = [(n, tp) for side in self.near for n in side]
        self.count = 0
        self.started = []

    def move(self, src, dst, target):
        i = self.count
        self.count += 1
        copy = put(src, dst, self.send.at[i], self.recv.at[i], target, self.tp)
        copy.start()
        self.started.append(copy)
        return copy

    def start(self):
        self.direct = {}
        for s, (e, col, width) in enumerate(self.spans):
            for i, w in enumerate(WAYS):
                for h in (0, 1):
                    rows = pl.ds(h * self.half, self.half)
                    block = lax.rem(self.here[h] + e + SIDE, SIDE)
                    src = self.sources[h].at[block, rows, pl.ds(col, width)]
                    self.direct[s, i, h] = self.move(src, self.slot(h, s, e, -w, w, 0, self.half), self.near[h][i])

    def relay(self, s):
        e = self.spans[s][0]
        part = self.half // 2
        for i, w in enumerate(WAYS):
            for h in (0, 1):
                self.direct[s, i, h].wait_recv()
                src = self.slot(h, s, e, -w, 0, part * i, part)
                self.direct[s, i, h, 2] = self.move(src, self.slot(h, s, e, 2, w, part * i, part), self.near[h][i])

    def finish(self):
        for key, copy in self.direct.items():
            if len(key) == 4:
                copy.wait_recv()
        for copy in self.started:
            copy.wait_send()


def reduce_kernel(part, row_y, col_z, out, rest_a, pair, total, near, far, hold, send, recv, rest_send, rest_recv):
    fs, tp, z, y, x, core = places()
    right = 2 * lax.rem(x + 1, SIDE) + core
    left = 2 * lax.rem(x + SIDE - 1, SIDE) + core
    other = tp + 1 - 2 * core

    def slot(h, s, e, f, to, row, rows):
        return rest_a.at[h, FAR.index(f), pl.ds(row, rows)]

    rest = Rest(row_y, col_z, EARLY, slot, rest_send, rest_recv)
    greet([(fs, right), (fs, left), (fs, other)] + rest.peers)
    copies = [put(part.at[m, :, 1 - core], pair.at[m], send.at[m], recv.at[m], fs, other) for m in range(3)]
    for c in copies:
        c.start()
    rest.start()
    for m, c in enumerate(copies):
        c.wait()
        total[m] = part[m, :, core] + pair[m]
    total[3] = jnp.zeros_like(total[3])
    half = total.shape[1] // 2
    up, down = pl.ds(0, half), pl.ds(half, half)
    ahead, back, across = lax.rem(x + 1, SIDE), lax.rem(x + SIDE - 1, SIDE), lax.rem(x + 2, SIDE)
    far_right = put(total.at[across, up], far.at[0], send.at[3], recv.at[3], fs, right)
    far_left = put(total.at[across, down], far.at[1], send.at[4], recv.at[4], fs, left)
    near_right = put(total.at[ahead, down], near.at[0], send.at[5], recv.at[5], fs, right)
    near_left = put(total.at[back, up], near.at[1], send.at[6], recv.at[6], fs, left)
    for c in (far_right, far_left, near_right, near_left):
        c.start()
    far_right.wait_recv()
    hold[0] = far[0] + total[ahead, up]
    on_right = put(hold.at[0], near.at[2], send.at[7], recv.at[7], fs, right)
    on_right.start()
    far_left.wait_recv()
    hold[1] = far[1] + total[back, down]
    on_left = put(hold.at[1], near.at[3], send.at[8], recv.at[8], fs, left)
    on_left.start()
    rest.relay(0)
    near_right.wait_recv()
    near_left.wait_recv()
    on_right.wait_recv()
    on_left.wait_recv()
    hold_up, hold_down = pair.at[0, up], pair.at[0, down]
    hold_up[...] = total[x, up] + near[2] + near[1]
    hold_down[...] = total[x, down] + near[3] + near[0]
    for b in range(TURN):
        chip = lax.rem(fs + b, PLANE)
        col = pl.multiple_of(LANE * (chip // SIDE), LANE)
        out[:, pl.ds(LANE * b, LANE)] = pair[0, lax.rem(chip, SIDE), :, pl.ds(col, LANE)]
    for c in (far_right, far_left, near_right, near_left, on_right, on_left):
        c.wait_send()
    rest.finish()


def reduce_to_planes(part, row_y, col_z, cid):
    f32 = jnp.float32
    shape = (part.shape[1],) + part.shape[3:]
    half = (shape[0] // 2,) + shape[1:]
    rows = row_y.shape[1] // 2
    vmem = pl.BlockSpec(memory_space=pltpu.VMEM)
    lanes = 8 * len(EARLY)
    return pl.pallas_call(
        reduce_kernel,
        out_shape=[jax.ShapeDtypeStruct((shape[1], TURN * LANE), f32)]
        + [jax.ShapeDtypeStruct((2, len(FAR), rows, width), f32) for _, _, width in EARLY],
        in_specs=[vmem, ANY, ANY],
        out_specs=[vmem, ANY],
        scratch_shapes=[
            pltpu.VMEM((3,) + shape, f32),
            pltpu.VMEM((4,) + shape, f32),
            pltpu.VMEM((4,) + half, f32),
            pltpu.VMEM((2,) + half, f32),
            pltpu.VMEM((2,) + half, f32),
            pltpu.SemaphoreType.DMA((9,)),
            pltpu.SemaphoreType.DMA((9,)),
            pltpu.SemaphoreType.DMA((lanes,)),
            pltpu.SemaphoreType.DMA((lanes,)),
        ],
        compiler_params=pltpu.CompilerParams(collective_id=cid, has_side_effects=True, vmem_limit_bytes=32 << 20),
        name="reduce_to_planes",
    )(part, row_y, col_z)


def last_kernel(
    block, row_y, col_z, rest_a, rest_m, y_out, out, full, high, low, pair, send, recv, own, pair_send, pair_recv, rest_send, rest_recv
):
    fs, tp, z, y, x, core = places()
    right = 2 * lax.rem(x + 1, SIDE) + core
    left = 2 * lax.rem(x + SIDE - 1, SIDE) + core
    other = tp + 1 - 2 * core
    ahead, back, across = lax.rem(x + 1, SIDE), lax.rem(x + SIDE - 1, SIDE), lax.rem(x + 2, SIDE)

    def origin(h, e, f):
        return plane_at(z, y, f, e) if h == 0 else plane_at(z, y, e, f)

    def slot(h, s, e, f, to, row, rows):
        _, col, width = LATE[s]
        return full.at[origin(h, e, f + to), pl.ds(h * rest.half + row, rows), pl.ds(col, width)]

    rest = Rest(row_y, col_z, LATE, slot, rest_send, rest_recv)
    greet([(fs, right), (fs, left), (fs, other)] + rest.peers)
    half = block.shape[0] // 2
    parts = [pl.ds(0, half), pl.ds(half, half)]
    go_right = [put(block.at[parts[h]], out.at[x, core, parts[h]], send.at[h], recv.at[h], fs, right) for h in (0, 1)]
    go_left = [put(block.at[parts[1 - h]], out.at[x, core, parts[1 - h]], send.at[2 + h], recv.at[2 + h], fs, left) for h in (0, 1)]
    for h in (0, 1):
        go_right[h].start()
        go_left[h].start()
    rest.start()
    moves = [(block, out.at[x, core])]
    moves += [(row_y.at[lax.rem(y + e + SIDE, SIDE)], full.at[plane_at(z, y, 0, e)]) for e in (0,) + FAR]
    moves += [(col_z.at[lax.rem(z + e + SIDE, SIDE)], full.at[plane_at(z, y, e, 0)]) for e in FAR]
    for buf, (e, col, width) in ((rest_a, EARLY[0]), (rest_m.at[0], AMID[0]), (rest_m.at[1], AMID[1])):
        for h in (0, 1):
            for i, f in enumerate(FAR):
                dst = full.at[origin(h, e, f), pl.ds(h * rest.half, rest.half), pl.ds(col, width)]
                moves.append((buf.at[h, i], dst))
    keeps = [pltpu.make_async_copy(src, dst, own.at[i]) for i, (src, dst) in enumerate(moves)]
    for keep in keeps:
        keep.start()
    put(block, out.at[x, core], pair_send, pair_recv, fs, other).start()
    go_right[0].wait_recv()
    first = out.at[back, core, parts[0]]
    relay_right = put(first, first, send.at[4], recv.at[4], fs, right)
    relay_right.start()
    go_left[0].wait_recv()
    second = out.at[ahead, core, parts[1]]
    relay_left = put(second, second, send.at[5], recv.at[5], fs, left)
    relay_left.start()
    rest.relay(0)
    go_right[1].wait_recv()
    put(out.at[back, core], out.at[back, core], pair_send, pair_recv, fs, other).start()
    go_left[1].wait_recv()
    put(out.at[ahead, core], out.at[ahead, core], pair_send, pair_recv, fs, other).start()
    for keep in keeps:
        keep.wait()
    rest.finish()

    @pl.loop(0, PLANE)
    def _(i):
        for k in (0, 1):
            rows = pl.ds(pl.multiple_of(LANE * i + 64 * k, 64), 64)
            high[rows, :], low[rows, :] = split(full[i, pl.ds(64 * k, 64), :])

    relay_right.wait_recv()
    relay_left.wait_recv()
    put(out.at[across, core], out.at[across, core], pair_send, pair_recv, fs, other).start()
    for c in go_right + go_left + [relay_right, relay_left]:
        c.wait_send()
    whole = put(out.at[:, core], out.at[:, 1 - core], pair_send, pair_recv, fs, other)
    whole.wait_send()
    whole.wait_recv()
    for m, (start, tiles) in enumerate(((0, 3), (WIDE, 3), (2 * FFB, 1))):
        for c in (0, 1):
            pair[pl.ds(64 * c, 64), :], pair[pl.ds(LANE + 64 * c, 64), :] = split(out[m, c])
        scale = math.sqrt(D) if m == 2 else math.sqrt(max(D, FF))
        for t in range(tiles):
            cols = pl.ds(start + 256 * t, 256)
            main = jnp.dot(pair[...], high[:, cols], preferred_element_type=jnp.float32)
            side = jnp.dot(pair[:LANE, :], low[:, cols], preferred_element_type=jnp.float32)
            value = scale * (main[:LANE] + (main[LANE:] + side))
            if m == 1 and t == 0:
                shared = pl.ds(start, LANE)
                lane = lax.broadcasted_iota(jnp.int32, (LANE, LANE), 1)
                y_out[:, shared] = jnp.where(lane < ODD, y_out[:, shared], value[:, :LANE])
                y_out[:, pl.ds(start + LANE, LANE)] = value[:, LANE:]
            else:
                y_out[:, cols] = value


def last_product(block, row_y, col_z, rest_a, rest_m, cid):
    rows, cols = block.shape
    f32, bf16 = jnp.float32, jnp.bfloat16
    vmem = pl.BlockSpec(memory_space=pltpu.VMEM)
    lanes = 8 * len(LATE)
    return pl.pallas_call(
        last_kernel,
        out_shape=jax.ShapeDtypeStruct((LANE, PACKED), f32),
        in_specs=[vmem] + [ANY] * 4,
        out_specs=vmem,
        scratch_shapes=[
            pltpu.VMEM((SIDE, 2, rows, cols), f32),
            pltpu.VMEM((PLANE,) + row_y.shape[1:], f32),
            pltpu.VMEM((D, PACKED), bf16),
            pltpu.VMEM((D, PACKED), bf16),
            pltpu.VMEM((2 * LANE, D), bf16),
            pltpu.SemaphoreType.DMA((6,)),
            pltpu.SemaphoreType.DMA((6,)),
            pltpu.SemaphoreType.DMA((8 + 18,)),
            pltpu.SemaphoreType.DMA,
            pltpu.SemaphoreType.DMA,
            pltpu.SemaphoreType.DMA((lanes,)),
            pltpu.SemaphoreType.DMA((lanes,)),
        ],
        compiler_params=pltpu.CompilerParams(collective_id=cid, has_side_effects=True, vmem_limit_bytes=44 << 20),
        name="last_product",
    )(block, row_y, col_z, rest_a, rest_m)


def turned(rows, dst):
    fs = lax.axis_index("fs")
    for b in range(TURN):
        col = pl.multiple_of(LANE * lax.rem(fs + b, PLANE), LANE)
        dst[:, pl.ds(LANE * b, LANE)] = rows[:, pl.ds(col, LANE)]


def split(value):
    top = value.astype(jnp.bfloat16)
    return top, (value - top.astype(jnp.float32)).astype(jnp.bfloat16)


def times(src, dst, pair, high, low, scale=None):
    rows, size = src.shape
    pair[:rows, :], pair[rows:, :] = split(src[...])
    width = 1024

    @pl.loop(0, size // width)
    def _(j):
        cols = pl.ds(pl.multiple_of(j * width, width), width)
        main = jnp.dot(pair[...], high[:, cols], preferred_element_type=jnp.float32)
        rest = jnp.dot(pair[...], low[:, cols], preferred_element_type=jnp.float32)
        value = main[:rows] + (main[rows:] + (rest[:rows] + rest[rows:]))
        dst[:, cols] = value if scale is None else scale * value


def plane_peers():
    fs, tp, z, y, x, core = places()
    return [(plane_at(z, y, 0, w), tp) for w in WAYS] + [(plane_at(z, y, w, 0), tp) for w in WAYS] + [(fs, tp + 1 - 2 * core)]


def first_chain_kernel(sent, next_rows, coef_rows, buf, high, low, pair, v, p, w, *sems):
    greet(plane_peers())
    plane_gather(sent, buf, high, low, True, *sems)

    def diag(i, total):
        block = buf[i, :, :, pl.ds(0, LANE)].reshape(LANE, LANE)
        eye = lax.broadcasted_iota(jnp.int32, block.shape, 0) == lax.broadcasted_iota(jnp.int32, block.shape, 1)
        return total + jnp.where(eye, block, 0.0)

    acc = lax.fori_loop(0, PLANE, diag, jnp.zeros((LANE, LANE), jnp.float32))
    ssq = jnp.sum(jnp.sum(acc, axis=0, keepdims=True), axis=1, keepdims=True)
    s = 0.5 * lax.rsqrt(jnp.maximum(ssq / D, 1.0))
    s2 = s * s
    fs, tp = lax.axis_index("fs"), lax.axis_index("tp")
    shape = v.shape
    start = pl.multiple_of(128 * fs + 64 * lax.rem(tp, 2), 64)
    on_diag = lax.broadcasted_iota(jnp.int32, shape, 1) == start + lax.broadcasted_iota(jnp.int32, shape, 0)
    mine = pl.ds(start, shape[0])
    v[...] = s2 * (high[mine, :].astype(jnp.float32) + low[mine, :].astype(jnp.float32))
    times(v, p, pair, high, low, s2)
    coef_rows[...] = s * (jnp.where(on_diag, A_COEF, 0.0) + B_COEF * v[...] + C_COEF * p[...])
    times(p, w, pair, high, low, s2)
    w[...] = A_COEF * v[...] + B_COEF * p[...] + C_COEF * w[...]
    times(w, v, pair, high, low, s2)
    times(v, p, pair, high, low, s2)
    w[...] = A_COEF * w[...] + B_COEF * v[...] + C_COEF * p[...]
    turned(w, next_rows)


def second_chain_kernel(
    sent, coef, row_y, col_z, out, rest_m, buf, high, low, pair, v, p, q, send, recv, own_sem, pair_send, pair_recv, rest_send, rest_recv
):
    def slot(h, s, e, f, to, row, rows):
        return rest_m.at[s, h, FAR.index(f), pl.ds(row, rows)]

    greet(plane_peers())
    plane_gather(sent, buf, high, low, False, send, recv, own_sem, pair_send, pair_recv)
    rest = Rest(row_y, col_z, AMID, slot, rest_send, rest_recv)
    rest.start()

    def by_a1(src, dst):
        times(src, p, pair, high, low)
        times(p, q, pair, high, low)
        dst[...] = A_COEF * src[...] + B_COEF * p[...] + C_COEF * q[...]

    def by_t2():
        times(v, q, pair, high, low)
        v[...] = q[...]

        @pl.loop(0, 2)
        def _(_):
            by_a1(v, v)

    by_a1(coef, v)
    out[...] = A_COEF * v[...]
    by_t2()
    out[...] += B_COEF * v[...]
    for s in range(len(AMID)):
        rest.relay(s)
    by_t2()
    out[...] += C_COEF * v[...]
    rest.finish()


def chain_call(kernel, args, outs, cid, extra_sems, name):
    size, rows = D, 64
    f32, bf16 = jnp.float32, jnp.bfloat16
    vmem = pl.BlockSpec(memory_space=pltpu.VMEM)
    dma = pltpu.SemaphoreType.DMA
    return pl.pallas_call(
        kernel,
        out_shape=[jax.ShapeDtypeStruct(shape, f32) for shape in outs],
        in_specs=[vmem if a.ndim == 2 else ANY for a in args],
        out_specs=[vmem if len(shape) == 2 else ANY for shape in outs],
        scratch_shapes=[pltpu.VMEM((PLANE, 2, rows, TURN * LANE), f32)]
        + [pltpu.VMEM((size, size), bf16)] * 2
        + [pltpu.VMEM((2 * rows, size), bf16)]
        + [pltpu.VMEM((rows, size), f32)] * 3
        + [dma((40,)), dma((40,)), dma, dma((PLANE,)), dma((PLANE,))]
        + [dma((extra_sems,))] * (2 if extra_sems else 0),
        compiler_params=pltpu.CompilerParams(collective_id=cid, has_side_effects=True, vmem_limit_bytes=40 << 20),
        name=name,
    )(*args)


def only(lanes_low, x):
    lane = lax.broadcasted_iota(jnp.int32, x.shape, x.ndim - 1)
    return jnp.where((lane < ODD) == lanes_low, x, 0.0)


def local(weights_in, weights_mix, momentum_in, momentum_mix, grads_in, grads_mix):
    moment_in = MOMENTUM_DECAY * momentum_in + grads_in
    moment_mix = MOMENTUM_DECAY * momentum_mix + grads_mix
    packed = jnp.concatenate([moment_in[0], moment_in[1], moment_mix], axis=1)
    row_y, col_z = cross_gather(packed, 0)
    spans = [slice(0, WIDE), slice(WIDE + LANE, 2 * FFB), slice(WIDE, WIDE + LANE), slice(2 * FFB, PACKED)]
    l0, l1, lodd, lmix = (row_y.reshape(-1, PACKED)[:, s] for s in spans)
    r0, r1, rodd, rmix = (col_z.reshape(-1, PACKED)[:, s] for s in spans)
    dot_t = functools.partial(lax.dot_general, dimension_numbers=(((1,), (1,)), ((), ())), precision=HIGH)
    part = jnp.stack(
        [
            dot_t(l0, r0) + dot_t(only(True, lodd), rodd),
            dot_t(l1, r1) + dot_t(only(False, lodd), rodd),
            dot_t(lmix, rmix),
        ]
    ).reshape(3, SIDE, 2, 64, SIDE * LANE)
    sent, rest_a = reduce_to_planes(part, row_y, col_z, 1)
    turn = (64, TURN * LANE)
    sent, coef = chain_call(first_chain_kernel, (sent,), (turn, (64, D)), 2, 0, "first_chain")
    mid = (len(AMID), 2, len(FAR), 64, PACKED)
    poly, rest_m = chain_call(second_chain_kernel, (sent, coef, row_y, col_z), ((64, D), mid), 3, 8 * len(AMID), "second_chain")
    steps = last_product(poly, row_y, col_z, rest_a, rest_m, 4)
    step_in = jnp.stack([steps[:, :FFB], steps[:, FFB : 2 * FFB]])
    step_mix = steps[:, 2 * FFB :]
    return (
        moment_in,
        moment_mix,
        weights_in - STEP_RATE * step_in,
        weights_mix - STEP_RATE * step_mix,
        step_in,
        step_mix,
    )


def solution(mesh):
    specs = (
        P(None, "fs", "tp"),
        P("fs", "tp"),
        P(None, "fs", "tp"),
        P("fs", "tp"),
        P(None, "fs", "tp"),
        P("fs", "tp"),
    )
    return jax.shard_map(local, mesh=mesh, in_specs=specs, out_specs=specs, check_vma=False)
```

time: 247 us -> 220 us (0.89)
  Pallas kernels: 217 us -> 202 us
  matrix products: 14.6 us -> 4.77 us
    pallas_call x5 -> x3, Pallas kernels: 151 us -> 141 us  [the longest x2 114 us: chain_call(): pl.pallas_call(kernel, out_shape=[jax.ShapeDtypeStruct(shape, f32) for sh...]
    dot_general x4 -> x0, matrix products: 9.95 us -> none  [the longest x1 2.97 us: local(): step_mix = dot(polys[2], mix) * math.sqrt(D)]
    pallas_call x1, Pallas kernels: 31.5 us -> 26.1 us  [reduce_to_planes(): pl.pallas_call(reduce_kernel, out_shape=[jax.ShapeDtypeStruct((shape[1],...]
    slice x7 -> x0, local copies, waits for them, and re-layouts: 4.39 us -> none  [the longest x1 2.37 us: local(): step_mix = dot(polys[2], mix) * math.sqrt(D)]
    unnamed x20 -> x18, local copies, waits for them, and re-layouts: 6.47 us -> 8.7 us
where the time goes in v4:
time: 220 us
  Pallas kernels  202 us (92%)
  local copies, waits for them, and re-layouts  9.98 us (5%)
  matrix products  4.77 us (2%)
  other arithmetic  2.4 us (1%)
    pallas_call x2, Pallas kernels, chain_call(): pl.pallas_call(kernel, out_shape=[jax.ShapeDtypeStruct(shape, f32) for sh...  114 us
    pallas_call x1, Pallas kernels, cross_gather(): pl.pallas_call(cross_kernel, out_shape=[jax.ShapeDtypeStruct((SIDE, rows,...  35.1 us
    pallas_call x1, Pallas kernels, last_product(): pl.pallas_call(last_kernel, out_shape=jax.ShapeDtypeStruct((LANE, PACKED)...  27 us
    pallas_call x1, Pallas kernels, reduce_to_planes(): pl.pallas_call(reduce_kernel, out_shape=[jax.ShapeDtypeStruct((shape[1],...  26.1 us
    unnamed x18, local copies, waits for them, and re-layouts  8.7 us

profile of v4, /device:TPU:1, one launch (start us, length us, event | category | flops | bytes accessed | tf_op | source)
XLA Modules:
  0.0 220.1 jit_solution(756052795798977637)
XLA Ops:
  0.7 1.4 copy.13
  2.1 1.4 copy.12
  3.5 0.1 multiply_add_fusion
  3.6 1.1 copy.15
  4.7 0.1 slice_bitcast_fusion
  4.8 0.2 concatenate.4.block
  5.0 35.1 %cross_gather.1 = (f32[4,128,1664]{2,1,0:T(8,128)S(1)}, f32[4,128,1664]{2,1,0:T(8,128)S(1)}) custom-call(f32[128,1664]{1,0:T(8,128)S(1)} %concatenate.4.block), custom_call_target="tpu_custom_call" | custom-call | tf_op jit(solution)/shard_map/cross_gather/pallas_call | solution.py:221
  40.1 0.6 fusion.6
  40.8 1.4 fusion
  42.2 0.6 convolution_add_fusion
  42.9 1.4 fusion.3
  44.3 0.6 convolution_add_fusion.1
  45.0 0.3 pad_maximum_fusion.part
  45.3 26.1 %reduce_to_planes.1 = (f32[64,1152]{1,0:T(8,128)S(1)}, f32[2,3,64,768]{3,2,1,0:T(8,128)S(1)}) custom-call(f32[3,4,2,64,512]{4,3,2,1,0:T(8,128)S(1)} %pad_maximum_fusion.part, f32[4,128,1664]{2,1,0:T(8,128)S(1)} %get-tuple-element.14.row_y, f32[4,128,1664]{2,1,0:T(8,128)S(1)} %get-tuple-element.15.col_z), custom_call_target="tpu_custom_call" | custom-call | tf_op jit(solution)/shard_map/reduce_to_planes/pallas_call | solution.py:338
  71.4 47.1 %first_chain.1 = (f32[64,1152]{1,0:T(8,128)S(1)}, f32[64,2048]{1,0:T(8,128)S(1)}) custom-call(f32[64,1152]{1,0:T(8,128)S(1)} %get-tuple-element.16.sent), custom_call_target="tpu_custom_call" | custom-call | tf_op jit(solution)/shard_map/first_chain/pallas_call | solution.py:576
  118.5 66.8 %second_chain.1 = (f32[64,2048]{1,0:T(8,128)S(1)}, f32[2,2,3,64,1664]{4,3,2,1,0:T(8,128)S(1)}) custom-call(f32[64,1152]{1,0:T(8,128)S(1)} %get-tuple-element.17.sent, f32[64,2048]{1,0:T(8,128)S(1)} %get-tuple-element.18.coef, f32[4,128,1664]{2,1,0:T(8,128)S(1)} %get-tuple-element.14.row_y, f32[4,128,1664]{2,1,0:T(8,128)S(1)} %get-tuple-element.15.col_z), custom_call_target="tpu_custom_call" | custom-call | tf_op jit(solution)/shard_map/second_chain/pallas_call | solution.py:576
  185.3 2.2 %copy-done = f32[2,2,3,64,1664]{4,3,2,1,0:T(8,128)} copy-done((f32[2,2,3,64,1664]{4,3,2,1,0:T(8,128)}, f32[2,2,3,64,1664]{4,3,2,1,0:T(8,128)S(1)}, u32[]{:S(2)}) %copy-start) | copy-done | bytes 5111832
  187.5 27.0 %last_product.1 = f32[128,1664]{1,0:T(8,128)S(1)} custom-call(f32[64,2048]{1,0:T(8,128)S(1)} %get-tuple-element.19.block, f32[4,128,1664]{2,1,0:T(8,128)S(1)} %get-tuple-element.14.row_y, f32[4,128,1664]{2,1,0:T(8,128)S(1)} %get-tuple-element.15.col_z, f32[2,3,64,768]{3,2,1,0:T(8,128)S(1)} %get-tuple-element.20.rest_a, f32[2,2,3,64,1664]{4,3,2,1,0:T(8,128)} %copy-done), custom_call_target="tpu_custom_call" | custom-call | tf_op jit(solution)/shard_map/last_product/pallas_call | solution.py:452
  214.6 1.0 slice_bitcast_fusion.3
  215.6 0.3 copy.14
  215.9 1.3 pad_maximum_fusion.1
  217.1 1.1 copy.16
  218.3 0.7 multiply_subtract_fusion.1
  219.0 1.1 copy.17
  (14 shorter events, 0.1 us)
Async XLA Ops:
  0.6 4.1 %copy-start.3 = (f32[128,256]{1,0:T(8,128)S(1)}, f32[128,256]{1,0:T(8,128)}, u32[]{:S(2)}) copy-start(f32[128,256]{1,0:T(8,128)} %param.11) | copy-start | bytes 393220
  0.6 4.0 %copy-start.4 = (f32[128,256]{1,0:T(8,128)S(1)}, f32[128,256]{1,0:T(8,128)}, u32[]{:S(2)}) copy-start(f32[128,256]{1,0:T(8,128)} %param.9) | copy-start | bytes 393220
  4.7 37.5 %copy-start.2 = (f32[128,256]{1,0:T(8,128)}, f32[128,256]{1,0:T(8,128)S(1)}, u32[]{:S(2)}) copy-start(f32[128,256]{1,0:T(8,128)S(1)} %multiply_add_fusion.1) | copy-start | bytes 393220
  185.3 2.3 %copy-start = (f32[2,2,3,64,1664]{4,3,2,1,0:T(8,128)}, f32[2,2,3,64,1664]{4,3,2,1,0:T(8,128)S(1)}, u32[]{:S(2)}) copy-start(f32[2,2,3,64,1664]{4,3,2,1,0:T(8,128)S(1)} %get-tuple-element.21.rest_m) | copy-start | bytes 15335428
  187.5 28.0 %copy-start.1 = (f32[2,128,704]{1,2,0:T(8,128)S(1)}, f32[2,128,704]{1,2,0:T(8,128)}, u32[]{:S(2)}) copy-start(f32[2,128,704]{1,2,0:T(8,128)} %param.6) | copy-start | bytes 2162692
  215.6 2.7 %copy-start.5 = (f32[128,256]{1,0:T(8,128)S(1)}, f32[128,256]{1,0:T(8,128)}, u32[]{:S(2)}) copy-start(f32[128,256]{1,0:T(8,128)} %param.7) | copy-start | bytes 393220

commit v5 on v4

--- a/solution.py
+++ b/solution.py
@@ -17,7 +17,6 @@
 C_COEF = 2.0315
 MOMENTUM_DECAY = 0.95
 STEP_RATE = 0.02
-HIGH = lax.Precision.HIGH
 MESH = pl.DeviceIdType.MESH
 ANY = pl.BlockSpec(memory_space=pl.ANY)
 
@@ -33,9 +32,13 @@
 WAYS = (1, -1)
 FAR = (-1, 1, 2)
 CUT = 768
-EARLY = ((-1, 0, CUT),)
-AMID = ((1, 0, PACKED), (2, 0, PACKED))
-LATE = ((-1, CUT, PACKED - CUT),)
+EARLY = ((-1, 0, PACKED),)
+AMID = ((1, 0, PACKED), (2, 0, CUT))
+LATE = ((2, CUT, PACKED - CUT),)
+GROUPS = ((0, WIDE + LANE), (WIDE + LANE, WIDE), (2 * FFB, MIX))
+LEFT = ((0, WIDE + LANE), (WIDE + LANE, WIDE + LANE), (2 * (WIDE + LANE), MIX))
+RIGHT = (0, WIDE, 2 * FFB)
+WIDTH_LEFT = 2 * (WIDE + LANE) + MIX
 
 
 def put(src, dst, send, recv, fs, tp):
@@ -175,60 +178,6 @@
     return SIDE * lax.rem(z + along_z + SIDE, SIDE) + lax.rem(y + along_y + SIDE, SIDE)
 
 
-def cross_kernel(block, row_y, col_z, send, recv, own):
-    fs, tp, z, y, x, core = places()
-    near = [[plane_at(z, y, 0, w) for w in WAYS], [plane_at(z, y, w, 0) for w in WAYS]]
-    greet([(n, tp) for side in near for n in side])
-    outs, here = (row_y, col_z), (y, z)
-    half = block.shape[0] // 2
-    lane = iter(range(12))
-
-    def move(src, dst, target):
-        i = next(lane)
-        copy = put(src, dst, send.at[i], recv.at[i], target, tp)
-        copy.start()
-        return copy
-
-    parts = [pl.ds(0, half), pl.ds(half, half)]
-    direct = {
-        (i, d, k): move(block.at[parts[(i + k) % 2]], outs[d].at[here[d], parts[(i + k) % 2]], near[d][i])
-        for k in (0, 1)
-        for i in (0, 1)
-        for d in (0, 1)
-    }
-    keeps = [pltpu.make_async_copy(block, outs[d].at[here[d]], own.at[d]) for d in (0, 1)]
-    for keep in keeps:
-        keep.start()
-    relays = []
-    for i, w in enumerate(WAYS):
-        for d in (0, 1):
-            direct[i, d, 0].wait_recv()
-            part = outs[d].at[lax.rem(here[d] - w + SIDE, SIDE), parts[i]]
-            relays.append(move(part, part, near[d][i]))
-    for (i, d, k), copy in direct.items():
-        copy.wait_send()
-        if k == 1:
-            copy.wait_recv()
-    for copy in relays:
-        copy.wait()
-    for keep in keeps:
-        keep.wait()
-
-
-def cross_gather(block, cid):
-    rows, cols = block.shape
-    vmem = pl.BlockSpec(memory_space=pltpu.VMEM)
-    return pl.pallas_call(
-        cross_kernel,
-        out_shape=[jax.ShapeDtypeStruct((SIDE, rows, cols), jnp.float32)] * 2,
-        in_specs=[vmem],
-        out_specs=[vmem] * 2,
-        scratch_shapes=[pltpu.SemaphoreType.DMA((12,)), pltpu.SemaphoreType.DMA((12,)), pltpu.SemaphoreType.DMA((2,))],
-        compiler_params=pltpu.CompilerParams(collective_id=cid, has_side_effects=True, vmem_limit_bytes=16 << 20),
-        name="cross_gather",
-    )(block)
-
-
 class Rest:
     def __init__(self, row_y, col_z, spans, slot, send, recv):
         fs, tp, z, y, x, core = places()
@@ -275,86 +224,259 @@
             copy.wait_send()
 
 
-def reduce_kernel(part, row_y, col_z, out, rest_a, pair, total, near, far, hold, send, recv, rest_send, rest_recv):
+def opening_kernel(
+    block, row_y, col_z, out, rest_a, lh, ll, rh, rl, part, pair, total, far, near, hold,
+    send, recv, own, pair_send, pair_recv, sum_send, sum_recv, rest_send, rest_recv,
+):
     fs, tp, z, y, x, core = places()
     right = 2 * lax.rem(x + 1, SIDE) + core
     left = 2 * lax.rem(x + SIDE - 1, SIDE) + core
     other = tp + 1 - 2 * core
-
-    def slot(h, s, e, f, to, row, rows):
-        return rest_a.at[h, FAR.index(f), pl.ds(row, rows)]
+    near_by = [[plane_at(z, y, 0, w) for w in WAYS], [plane_at(z, y, w, 0) for w in WAYS]]
+    outs, here = (row_y, col_z), (y, z)
+    rows = block.shape[0] // 2
+    parts = [pl.ds(0, rows), pl.ds(rows, rows)]
+    lane = iter(range(12 * len(GROUPS)))
+    direct, relays, started = {}, {}, []
+
+    def move(src, dst, target):
+        i = next(lane)
+        copy = put(src, dst, send.at[i], recv.at[i], target, tp)
+        copy.start()
+        started.append(copy)
+        return copy
+
+    def set_off(g):
+        cols = pl.ds(*GROUPS[g])
+        for k in (0, 1):
+            for i in (0, 1):
+                for d in (0, 1):
+                    half = parts[(i + k) % 2]
+                    direct[g, i, d, k] = move(block.at[half, cols], outs[d].at[here[d], half, cols], near_by[d][i])
+
+    def relay(g):
+        cols = pl.ds(*GROUPS[g])
+        for i, w in enumerate(WAYS):
+            for d in (0, 1):
+                direct[g, i, d, 0].wait_recv()
+                half = outs[d].at[lax.rem(here[d] - w + SIDE, SIDE), parts[i], cols]
+                relays[g, i, d] = move(half, half, near_by[d][i])
+
+    def arrived(g):
+        for i in (0, 1):
+            for d in (0, 1):
+                direct[g, i, d, 1].wait_recv()
+                relays[g, i, d].wait_recv()
+
+    def prepare(g):
+        first, width = GROUPS[g]
+        last = first + width
+
+        @pl.loop(0, 2 * SIDE)
+        def _(n):
+            at = pl.ds(pl.multiple_of(64 * n, 64), 64)
+            src = pl.ds(pl.multiple_of(64 * lax.rem(n, 2), 64), 64)
+            cols = pl.ds(first, width)
+            rh[at, cols], rl[at, cols] = split(col_z[n // 2, src, cols])
+            if g == 0:
+                plain, shared = pl.ds(0, WIDE), pl.ds(WIDE, LANE)
+                lh[at, plain], ll[at, plain] = split(row_y[n // 2, src, plain])
+                value = row_y[n // 2, src, shared]
+                low_lane = lax.broadcasted_iota(jnp.int32, value.shape, 1) < ODD
+                lh[at, shared], ll[at, shared] = split(jnp.where(low_lane, value, 0.0))
+                next_to = pl.ds(WIDE + LANE, LANE)
+                lh[at, next_to], ll[at, next_to] = split(jnp.where(low_lane, 0.0, value))
+            else:
+                to = pl.ds(first + LANE, width)
+                lh[at, to], ll[at, to] = split(row_y[n // 2, src, cols])
+
+    def gram(m):
+        lc = pl.ds(*LEFT[m])
+        rc = pl.ds(RIGHT[m], LEFT[m][1])
+        dot = functools.partial(
+            lax.dot_general, dimension_numbers=(((1,), (1,)), ((), ())), preferred_element_type=jnp.float32
+        )
+        for r in (0, 1):
+            at = pl.ds(256 * r, 256)
+            value = dot(lh[at, lc], rh[:, rc]) + (dot(lh[at, lc], rl[:, rc]) + dot(ll[at, lc], rh[:, rc]))
+            part[m, pl.ds(2 * r, 2)] = value.reshape((2,) + part.shape[2:])
+
+    def to_pair(m):
+        return put(part.at[m, :, 1 - core], pair.at[m], pair_send.at[m], pair_recv.at[m], fs, other)
+
+    up, down = pl.ds(0, 2), pl.ds(2, 2)
+
+    def far_copy(m, side, c):
+        src = total.at[m, c] if side == 0 else total.at[m, 2 + c]
+        i = 2 * side + c
+        return put(src, far.at[m, side, c], sum_send.at[m, i], sum_recv.at[m, i], fs, (right, left)[side])
+
+    def near_copy(m, side):
+        src = total.at[m, down] if side == 0 else total.at[m, up]
+        return put(src, near.at[side], sum_send.at[m, 4 + side], sum_recv.at[m, 4 + side], fs, (right, left)[side])
+
+    def hold_copy(m, side, c):
+        i = 6 + 2 * side + c
+        return put(hold.at[m, side, c], near.at[2 + side, c], sum_send.at[m, i], sum_recv.at[m, i], fs, (right, left)[side])
+
+    def before(m):
+        return x == (m + SIDE - 1) % SIDE
+
+    def after(m):
+        return x == (m + 1) % SIDE
+
+    def beyond(m):
+        return x == (m + 2) % SIDE
+
+    def sums(m):
+        to_pair(m).wait()
+        total[m] = part[m, :, core] + pair[m]
+
+        @pl.when(beyond(m))
+        def _():
+            for c in (0, 1):
+                for side in (0, 1):
+                    far_copy(m, side, c).start()
+
+        for side, role in ((0, before), (1, after)):
+
+            @pl.when(role(m))
+            def _():
+                near_copy(m, side).start()
+
+    def pass_on(m):
+        for side, role in ((0, before), (1, after)):
+
+            @pl.when(role(m))
+            def _():
+                for c in (0, 1):
+                    far_copy(m, side, c).wait_recv()
+                    hold[m, side, c] = far[m, side, c] + total[m, c if side == 0 else 2 + c]
+                    hold_copy(m, side, c).start()
+
+    def keep_sum(m):
+        @pl.when(x == m)
+        def _():
+            near_copy(m, 0).wait_recv()
+            near_copy(m, 1).wait_recv()
+            for c in (0, 1):
+                for side in (0, 1):
+                    hold_copy(m, side, c).wait_recv()
+            pair[m, up] = total[m, up] + near[2] + near[1]
+            pair[m, down] = total[m, down] + near[3] + near[0]
+            for b in range(TURN):
+                chip = lax.rem(fs + b, PLANE)
+                col = pl.multiple_of(LANE * (chip // SIDE), LANE)
+                out[:, pl.ds(LANE * b, LANE)] = pair[m, lax.rem(chip, SIDE), :, pl.ds(col, LANE)]
+
+    def sent(m):
+        @pl.when(beyond(m))
+        def _():
+            for c in (0, 1):
+                for side in (0, 1):
+                    far_copy(m, side, c).wait_send()
+
+        for side, role in ((0, before), (1, after)):
+
+            @pl.when(role(m))
+            def _():
+                near_copy(m, side).wait_send()
+                for c in (0, 1):
+                    hold_copy(m, side, c).wait_send()
+
+    def slot(h, s, e, f, to, row, count):
+        return rest_a.at[h, FAR.index(f), pl.ds(row, count)]
 
     rest = Rest(row_y, col_z, EARLY, slot, rest_send, rest_recv)
     greet([(fs, right), (fs, left), (fs, other)] + rest.peers)
-    copies = [put(part.at[m, :, 1 - core], pair.at[m], send.at[m], recv.at[m], fs, other) for m in range(3)]
-    for c in copies:
-        c.start()
+    set_off(0)
+    keeps = [pltpu.make_async_copy(block, outs[d].at[here[d]], own.at[d]) for d in (0, 1)]
+    for copy in keeps:
+        copy.start()
+    relay(0)
+    set_off(1)
+    for copy in keeps:
+        copy.wait()
+    arrived(0)
+    prepare(0)
+    gram(0)
+    to_pair(0).start()
+    relay(1)
+    set_off(2)
+    sums(0)
+    pass_on(0)
+    arrived(1)
+    prepare(1)
+    relay(2)
+    gram(1)
+    to_pair(1).start()
+    arrived(2)
+    prepare(2)
+    gram(2)
+    to_pair(2).start()
+    sums(1)
+    sums(2)
     rest.start()
-    for m, c in enumerate(copies):
-        c.wait()
-        total[m] = part[m, :, core] + pair[m]
-    total[3] = jnp.zeros_like(total[3])
-    half = total.shape[1] // 2
-    up, down = pl.ds(0, half), pl.ds(half, half)
-    ahead, back, across = lax.rem(x + 1, SIDE), lax.rem(x + SIDE - 1, SIDE), lax.rem(x + 2, SIDE)
-    far_right = put(total.at[across, up], far.at[0], send.at[3], recv.at[3], fs, right)
-    far_left = put(total.at[across, down], far.at[1], send.at[4], recv.at[4], fs, left)
-    near_right = put(total.at[ahead, down], near.at[0], send.at[5], recv.at[5], fs, right)
-    near_left = put(total.at[back, up], near.at[1], send.at[6], recv.at[6], fs, left)
-    for c in (far_right, far_left, near_right, near_left):
-        c.start()
-    far_right.wait_recv()
-    hold[0] = far[0] + total[ahead, up]
-    on_right = put(hold.at[0], near.at[2], send.at[7], recv.at[7], fs, right)
-    on_right.start()
-    far_left.wait_recv()
-    hold[1] = far[1] + total[back, down]
-    on_left = put(hold.at[1], near.at[3], send.at[8], recv.at[8], fs, left)
-    on_left.start()
+    pass_on(1)
+    pass_on(2)
     rest.relay(0)
-    near_right.wait_recv()
-    near_left.wait_recv()
-    on_right.wait_recv()
-    on_left.wait_recv()
-    hold_up, hold_down = pair.at[0, up], pair.at[0, down]
-    hold_up[...] = total[x, up] + near[2] + near[1]
-    hold_down[...] = total[x, down] + near[3] + near[0]
-    for b in range(TURN):
-        chip = lax.rem(fs + b, PLANE)
-        col = pl.multiple_of(LANE * (chip // SIDE), LANE)
-        out[:, pl.ds(LANE * b, LANE)] = pair[0, lax.rem(chip, SIDE), :, pl.ds(col, LANE)]
-    for c in (far_right, far_left, near_right, near_left, on_right, on_left):
-        c.wait_send()
+
+    @pl.when(x == SIDE - 1)
+    def _():
+        out[...] = jnp.zeros_like(out)
+
+    for m in range(3):
+        keep_sum(m)
+    for m in range(3):
+        sent(m)
+    for copy in started:
+        copy.wait_send()
     rest.finish()
 
 
-def reduce_to_planes(part, row_y, col_z, cid):
-    f32 = jnp.float32
-    shape = (part.shape[1],) + part.shape[3:]
-    half = (shape[0] // 2,) + shape[1:]
-    rows = row_y.shape[1] // 2
+def opening(block, cid):
+    f32, bf16 = jnp.float32, jnp.bfloat16
+    rows, cols = block.shape
+    size = SIDE * rows
+    quad = (SIDE, rows // 2, size)
+    duo = (2,) + quad[1:]
     vmem = pl.BlockSpec(memory_space=pltpu.VMEM)
-    lanes = 8 * len(EARLY)
+    dma = pltpu.SemaphoreType.DMA
+    moves = 12 * len(GROUPS)
     return pl.pallas_call(
-        reduce_kernel,
-        out_shape=[jax.ShapeDtypeStruct((shape[1], TURN * LANE), f32)]
-        + [jax.ShapeDtypeStruct((2, len(FAR), rows, width), f32) for _, _, width in EARLY],
-        in_specs=[vmem, ANY, ANY],
-        out_specs=[vmem, ANY],
+        opening_kernel,
+        out_shape=[
+            jax.ShapeDtypeStruct((SIDE, rows, cols), f32),
+            jax.ShapeDtypeStruct((SIDE, rows, cols), f32),
+            jax.ShapeDtypeStruct((rows // 2, TURN * LANE), f32),
+            jax.ShapeDtypeStruct((2, len(FAR), rows // 2, PACKED), f32),
+        ],
+        in_specs=[vmem],
+        out_specs=[vmem, vmem, vmem, ANY],
         scratch_shapes=[
-            pltpu.VMEM((3,) + shape, f32),
-            pltpu.VMEM((4,) + shape, f32),
-            pltpu.VMEM((4,) + half, f32),
-            pltpu.VMEM((2,) + half, f32),
-            pltpu.VMEM((2,) + half, f32),
-            pltpu.SemaphoreType.DMA((9,)),
-            pltpu.SemaphoreType.DMA((9,)),
-            pltpu.SemaphoreType.DMA((lanes,)),
-            pltpu.SemaphoreType.DMA((lanes,)),
+            pltpu.VMEM((size, WIDTH_LEFT), bf16),
+            pltpu.VMEM((size, WIDTH_LEFT), bf16),
+            pltpu.VMEM((size, cols), bf16),
+            pltpu.VMEM((size, cols), bf16),
+            pltpu.VMEM((3, SIDE, 2, rows // 2, size), f32),
+            pltpu.VMEM((3,) + quad, f32),
+            pltpu.VMEM((3,) + quad, f32),
+            pltpu.VMEM((3, 2) + duo, f32),
+            pltpu.VMEM((4,) + duo, f32),
+            pltpu.VMEM((3, 2) + duo, f32),
+            dma((moves,)),
+            dma((moves,)),
+            dma((2,)),
+            dma((3,)),
+            dma((3,)),
+            dma((3, 10)),
+            dma((3, 10)),
+            dma((8 * len(EARLY),)),
+            dma((8 * len(EARLY),)),
         ],
-        compiler_params=pltpu.CompilerParams(collective_id=cid, has_side_effects=True, vmem_limit_bytes=32 << 20),
-        name="reduce_to_planes",
-    )(part, row_y, col_z)
+        compiler_params=pltpu.CompilerParams(collective_id=cid, has_side_effects=True, vmem_limit_bytes=36 << 20),
+        name="opening",
+    )(block)
 
 
 def last_kernel(
@@ -390,7 +512,7 @@
         for h in (0, 1):
             for i, f in enumerate(FAR):
                 dst = full.at[origin(h, e, f), pl.ds(h * rest.half, rest.half), pl.ds(col, width)]
-                moves.append((buf.at[h, i], dst))
+                moves.append((buf.at[h, i, :, pl.ds(0, width)], dst))
     keeps = [pltpu.make_async_copy(src, dst, own.at[i]) for i, (src, dst) in enumerate(moves)]
     for keep in keeps:
         keep.start()
@@ -468,7 +590,7 @@
             pltpu.SemaphoreType.DMA((lanes,)),
             pltpu.SemaphoreType.DMA((lanes,)),
         ],
-        compiler_params=pltpu.CompilerParams(collective_id=cid, has_side_effects=True, vmem_limit_bytes=44 << 20),
+        compiler_params=pltpu.CompilerParams(collective_id=cid, has_side_effects=True, vmem_limit_bytes=36 << 20),
         name="last_product",
     )(block, row_y, col_z, rest_a, rest_m)
 
@@ -537,7 +659,7 @@
     sent, coef, row_y, col_z, out, rest_m, buf, high, low, pair, v, p, q, send, recv, own_sem, pair_send, pair_recv, rest_send, rest_recv
 ):
     def slot(h, s, e, f, to, row, rows):
-        return rest_m.at[s, h, FAR.index(f), pl.ds(row, rows)]
+        return rest_m.at[s, h, FAR.index(f), pl.ds(row, rows), pl.ds(0, AMID[s][2])]
 
     greet(plane_peers())
     plane_gather(sent, buf, high, low, False, send, recv, own_sem, pair_send, pair_recv)
@@ -589,28 +711,11 @@
     )(*args)
 
 
-def only(lanes_low, x):
-    lane = lax.broadcasted_iota(jnp.int32, x.shape, x.ndim - 1)
-    return jnp.where((lane < ODD) == lanes_low, x, 0.0)
-
-
 def local(weights_in, weights_mix, momentum_in, momentum_mix, grads_in, grads_mix):
     moment_in = MOMENTUM_DECAY * momentum_in + grads_in
     moment_mix = MOMENTUM_DECAY * momentum_mix + grads_mix
     packed = jnp.concatenate([moment_in[0], moment_in[1], moment_mix], axis=1)
-    row_y, col_z = cross_gather(packed, 0)
-    spans = [slice(0, WIDE), slice(WIDE + LANE, 2 * FFB), slice(WIDE, WIDE + LANE), slice(2 * FFB, PACKED)]
-    l0, l1, lodd, lmix = (row_y.reshape(-1, PACKED)[:, s] for s in spans)
-    r0, r1, rodd, rmix = (col_z.reshape(-1, PACKED)[:, s] for s in spans)
-    dot_t = functools.partial(lax.dot_general, dimension_numbers=(((1,), (1,)), ((), ())), precision=HIGH)
-    part = jnp.stack(
-        [
-            dot_t(l0, r0) + dot_t(only(True, lodd), rodd),
-            dot_t(l1, r1) + dot_t(only(False, lodd), rodd),
-            dot_t(lmix, rmix),
-        ]
-    ).reshape(3, SIDE, 2, 64, SIDE * LANE)
-    sent, rest_a = reduce_to_planes(part, row_y, col_z, 1)
+    row_y, col_z, sent, rest_a = opening(packed, 0)
     turn = (64, TURN * LANE)
     sent, coef = chain_call(first_chain_kernel, (sent,), (turn, (64, D)), 2, 0, "first_chain")
     mid = (len(AMID), 2, len(FAR), 64, PACKED)

time: 220 us -> 215 us (0.977)
  matrix products: 4.77 us -> 0 us
  Pallas kernels: 202 us -> 199 us
  local copies, waits for them, and re-layouts: 9.98 us -> 12.4 us
    dot_general x5 -> x0, matrix products: 4.77 us -> none  [the longest x1 1.44 us: local(): dot_t(l1, r1) + dot_t(only(False, lodd), rodd)]
    unnamed x18 -> x20, local copies, waits for them, and re-layouts: 8.7 us -> 11.2 us
    pallas_call x2, Pallas kernels: 114 us -> 111 us  [chain_call(): pl.pallas_call(kernel, out_shape=[jax.ShapeDtypeStruct(shape, f32) for sh...]
    pallas_call x2 -> x1, Pallas kernels: 61.2 us -> 60.7 us  [opening(): pl.pallas_call(opening_kernel, out_shape=[jax.ShapeDtypeStruct((SIDE, row...]
where the time goes in v5:
time: 215 us
  Pallas kernels  199 us (93%)
  local copies, waits for them, and re-layouts  12.4 us (6%)
    pallas_call x2, Pallas kernels, chain_call(): pl.pallas_call(kernel, out_shape=[jax.ShapeDtypeStruct(shape, f32) for sh...  111 us
    pallas_call x1, Pallas kernels, opening(): pl.pallas_call(opening_kernel, out_shape=[jax.ShapeDtypeStruct((SIDE, row...  60.7 us
    pallas_call x1, Pallas kernels, last_product(): pl.pallas_call(last_kernel, out_shape=jax.ShapeDtypeStruct((LANE, PACKED)...  27 us
    unnamed x20, local copies, waits for them, and re-layouts  11.2 us

profile of v5, /device:TPU:1, one launch (start us, length us, event | category | flops | bytes accessed | tf_op | source)
XLA Modules:
  0.0 214.5 jit_solution(7783140218639238002)
XLA Ops:
  0.6 0.0 copy-start.4
  0.6 0.0 copy-start.5
  0.7 1.4 copy.13
  2.1 1.4 copy.12
  3.5 0.1 multiply_add_fusion
  3.6 1.1 copy.15
  4.7 0.0 copy-done.4
  4.7 0.0 copy-done.5
  4.7 0.0 copy-start.3
  4.7 0.1 slice_bitcast_fusion
  4.8 0.2 concatenate.3.block
  5.0 60.7 %opening.1 = (f32[4,128,1664]{2,1,0:T(8,128)S(1)}, f32[4,128,1664]{2,1,0:T(8,128)S(1)}, f32[64,1152]{1,0:T(8,128)S(1)}, f32[2,3,64,1664]{3,2,1,0:T(8,128)S(1)}) custom-call(f32[128,1664]{1,0:T(8,128)S(1)} %concatenate.3.block), custom_call_target="tpu_custom_call" | custom-call | tf_op jit(solution)/shard_map/opening/pallas_call | solution.py:446
  65.7 46.1 %first_chain.1 = (f32[64,1152]{1,0:T(8,128)S(1)}, f32[64,2048]{1,0:T(8,128)S(1)}) custom-call(f32[64,1152]{1,0:T(8,128)S(1)} %get-tuple-element.14.sent), custom_call_target="tpu_custom_call" | custom-call | tf_op jit(solution)/shard_map/first_chain/pallas_call | solution.py:698
  111.9 65.4 %second_chain.1 = (f32[64,2048]{1,0:T(8,128)S(1)}, f32[2,2,3,64,1664]{4,3,2,1,0:T(8,128)S(1)}) custom-call(f32[64,1152]{1,0:T(8,128)S(1)} %get-tuple-element.15.sent, f32[64,2048]{1,0:T(8,128)S(1)} %get-tuple-element.16.coef, f32[4,128,1664]{2,1,0:T(8,128)S(1)} %get-tuple-element.17.row_y, f32[4,128,1664]{2,1,0:T(8,128)S(1)} %get-tuple-element.18.col_z), custom_call_target="tpu_custom_call" | custom-call | tf_op jit(solution)/shard_map/second_chain/pallas_call | solution.py:698
  177.3 2.2 %copy-done = f32[2,2,3,64,1664]{4,3,2,1,0:T(8,128)} copy-done((f32[2,2,3,64,1664]{4,3,2,1,0:T(8,128)}, f32[2,2,3,64,1664]{4,3,2,1,0:T(8,128)S(1)}, u32[]{:S(2)}) %copy-start) | copy-done | bytes 5111832
  179.5 2.4 %copy-done.1 = f32[2,2,3,64,1664]{4,3,2,1,0:T(8,128)S(1)} copy-done((f32[2,2,3,64,1664]{4,3,2,1,0:T(8,128)S(1)}, f32[2,2,3,64,1664]{4,3,2,1,0:T(8,128)}, u32[]{:S(2)}) %copy-start.1) | copy-done | bytes 5111832
  182.0 27.0 %last_product.1 = f32[128,1664]{1,0:T(8,128)S(1)} custom-call(f32[64,2048]{1,0:T(8,128)S(1)} %get-tuple-element.19.block, f32[4,128,1664]{2,1,0:T(8,128)S(1)} %get-tuple-element.17.row_y, f32[4,128,1664]{2,1,0:T(8,128)S(1)} %get-tuple-element.18.col_z, f32[2,3,64,1664]{3,2,1,0:T(8,128)S(1)} %get-tuple-element.20.rest_a, f32[2,2,3,64,1664]{4,3,2,1,0:T(8,128)S(1)} %copy-done.1), custom_call_target="tpu_custom_call" | custom-call | tf_op jit(solution)/shard_map/last_product/pallas_call | solution.py:574
  209.0 1.0 slice_bitcast_fusion.3
  210.0 0.3 copy.14
  210.3 1.3 pad_maximum_fusion
  211.5 1.1 copy.16
  212.7 0.0 copy-done.6
  212.7 0.7 multiply_subtract_fusion.1
  213.4 1.1 copy.17
  (7 shorter events, 0.0 us)
Async XLA Ops:
  0.6 4.1 %copy-start.4 = (f32[128,256]{1,0:T(8,128)S(1)}, f32[128,256]{1,0:T(8,128)}, u32[]{:S(2)}) copy-start(f32[128,256]{1,0:T(8,128)} %param.11) | copy-start | bytes 393220
  0.6 4.0 %copy-start.5 = (f32[128,256]{1,0:T(8,128)S(1)}, f32[128,256]{1,0:T(8,128)}, u32[]{:S(2)}) copy-start(f32[128,256]{1,0:T(8,128)} %param.9) | copy-start | bytes 393220
  4.7 172.5 %copy-start.3 = (f32[128,256]{1,0:T(8,128)}, f32[128,256]{1,0:T(8,128)S(1)}, u32[]{:S(2)}) copy-start(f32[128,256]{1,0:T(8,128)S(1)} %multiply_add_fusion.1) | copy-start | bytes 393220
  177.3 2.3 %copy-start = (f32[2,2,3,64,1664]{4,3,2,1,0:T(8,128)}, f32[2,2,3,64,1664]{4,3,2,1,0:T(8,128)S(1)}, u32[]{:S(2)}) copy-start(f32[2,2,3,64,1664]{4,3,2,1,0:T(8,128)S(1)} %get-tuple-element.21.rest_m) | copy-start | bytes 15335428
  179.5 2.4 %copy-start.1 = (f32[2,2,3,64,1664]{4,3,2,1,0:T(8,128)S(1)}, f32[2,2,3,64,1664]{4,3,2,1,0:T(8,128)}, u32[]{:S(2)}) copy-start(f32[2,2,3,64,1664]{4,3,2,1,0:T(8,128)} %copy-done) | copy-start | bytes 15335428
  182.0 28.0 %copy-start.2 = (f32[2,128,704]{1,2,0:T(8,128)S(1)}, f32[2,128,704]{1,2,0:T(8,128)}, u32[]{:S(2)}) copy-start(f32[2,128,704]{1,2,0:T(8,128)} %param.6) | copy-start | bytes 2162692
  210.0 2.7 %copy-start.6 = (f32[128,256]{1,0:T(8,128)S(1)}, f32[128,256]{1,0:T(8,128)}, u32[]{:S(2)}) copy-start(f32[128,256]{1,0:T(8,128)} %param.7) | copy-start | bytes 393220

commit v6 on v5

--- a/solution.py
+++ b/solution.py
@@ -31,10 +31,7 @@
 PACKED = 2 * FFB + MIX
 WAYS = (1, -1)
 FAR = (-1, 1, 2)
-CUT = 768
-EARLY = ((-1, 0, PACKED),)
-AMID = ((1, 0, PACKED), (2, 0, CUT))
-LATE = ((2, CUT, PACKED - CUT),)
+SPANS = tuple((e, 0, PACKED) for e in FAR)
 GROUPS = ((0, WIDE + LANE), (WIDE + LANE, WIDE), (2 * FFB, MIX))
 LEFT = ((0, WIDE + LANE), (WIDE + LANE, WIDE + LANE), (2 * (WIDE + LANE), MIX))
 RIGHT = (0, WIDE, 2 * FFB)
@@ -106,20 +103,6 @@
         origin = near(h, 2, 0)
         for j, w2 in enumerate(WAYS):
             second[h, j, 2] = move(origin, halves(h), near(h, 0, w2))
-    tail = {}
-    for e in (0, -1, 1, 2):
-        for j, w2 in enumerate(WAYS):
-            for h in (0, 1):
-                second[h, j, e].wait_recv()
-                tail[h, j, e] = move(near(h, e, -w2), quarters(h, j), near(h, 0, w2))
-        if e == 0:
-            for w in WAYS:
-                to_pair(0, w)
-                to_pair(w, 0)
-        if e == 1:
-            for w in WAYS:
-                for w2 in WAYS:
-                    to_pair(w, w2)
 
     def rebuild(i):
         sent = buf.at[i]
@@ -136,22 +119,55 @@
             if 0 < b < TURN - 1:
                 high[cols, rows], low[cols, rows] = split(value.T)
 
-    keep.wait()
-    for copy in pairs.values():
-        copy.wait_recv()
-
-    @pl.loop(0, 9)
+    tail = {}
+    for e in (0, -1, 1, 2):
+        for j, w2 in enumerate(WAYS):
+            for h in (0, 1):
+                second[h, j, e].wait_recv()
+                tail[h, j, e] = move(near(h, e, -w2), quarters(h, j), near(h, 0, w2))
+        if e == 0:
+            for w in WAYS:
+                to_pair(0, w)
+                to_pair(w, 0)
+        if e == -1:
+            keep.wait()
+            for w in WAYS:
+                pairs[0, w].wait_recv()
+                pairs[w, 0].wait_recv()
+            pairs[0, 0].wait_recv()
+
+            @pl.loop(0, 3)
+            def _(n):
+                rebuild(plane_at(z, y, 0, n - 1))
+
+            @pl.loop(0, 2)
+            def _(n):
+                rebuild(plane_at(z, y, 2 * n - 1, 0))
+
+        if e == 1:
+            for w in WAYS:
+                for w2 in WAYS:
+                    to_pair(w, w2)
+
+    for w in WAYS:
+        for w2 in WAYS:
+            pairs[w, w2].wait_recv()
+
+    @pl.loop(0, 4)
     def _(n):
-        rebuild(plane_at(z, y, n // 3 - 1, lax.rem(n, 3) - 1))
-
-    for e in (0, -1, 1, 2):
+        rebuild(plane_at(z, y, 2 * (n // 2) - 1, 2 * lax.rem(n, 2) - 1))
+
+    def last_hop(e):
         for j in (0, 1):
             for h in (0, 1):
                 tail[h, j, e].wait_recv()
         to_pair(2, e)
         if e != 2:
             to_pair(e, 2)
-    for e in FAR[:2] + (0,):
+
+    for e in (0, -1, 1):
+        last_hop(e)
+    for e in (0, -1, 1):
         pairs[e, 2].wait_recv()
         pairs[2, e].wait_recv()
 
@@ -159,12 +175,14 @@
     def _(n):
         rebuild(plane_at(z, y, n - 1, 2))
 
-    pairs[2, 2].wait_recv()
-
-    @pl.loop(0, 4)
+    last_hop(2)
+
+    @pl.loop(0, 3)
     def _(n):
         rebuild(plane_at(z, y, 2, n - 1))
 
+    pairs[2, 2].wait_recv()
+    rebuild(plane_at(z, y, 2, 2))
     for copy in started:
         copy.wait_send()
 
@@ -188,6 +206,7 @@
         self.peers = [(n, tp) for side in self.near for n in side]
         self.count = 0
         self.started = []
+        self.direct = {}
 
     def move(self, src, dst, target):
         i = self.count
@@ -197,15 +216,14 @@
         self.started.append(copy)
         return copy
 
-    def start(self):
-        self.direct = {}
-        for s, (e, col, width) in enumerate(self.spans):
-            for i, w in enumerate(WAYS):
-                for h in (0, 1):
-                    rows = pl.ds(h * self.half, self.half)
-                    block = lax.rem(self.here[h] + e + SIDE, SIDE)
-                    src = self.sources[h].at[block, rows, pl.ds(col, width)]
-                    self.direct[s, i, h] = self.move(src, self.slot(h, s, e, -w, w, 0, self.half), self.near[h][i])
+    def start(self, s):
+        e, col, width = self.spans[s]
+        for i, w in enumerate(WAYS):
+            for h in (0, 1):
+                rows = pl.ds(h * self.half, self.half)
+                block = lax.rem(self.here[h] + e + SIDE, SIDE)
+                src = self.sources[h].at[block, rows, pl.ds(col, width)]
+                self.direct[s, i, h] = self.move(src, self.slot(h, s, e, -w, w, 0, self.half), self.near[h][i])
 
     def relay(self, s):
         e = self.spans[s][0]
@@ -225,8 +243,8 @@
 
 
 def opening_kernel(
-    block, row_y, col_z, out, rest_a, lh, ll, rh, rl, part, pair, total, far, near, hold,
-    send, recv, own, pair_send, pair_recv, sum_send, sum_recv, rest_send, rest_recv,
+    turned_in, mix, row_y, col_z, out, block, lh, ll, rh, rl, part, pair, total, far, near, hold,
+    send, recv, own, pair_send, pair_recv, sum_send, sum_recv,
 ):
     fs, tp, z, y, x, core = places()
     right = 2 * lax.rem(x + 1, SIDE) + core
@@ -384,11 +402,10 @@
                 for c in (0, 1):
                     hold_copy(m, side, c).wait_send()
 
-    def slot(h, s, e, f, to, row, count):
-        return rest_a.at[h, FAR.index(f), pl.ds(row, count)]
-
-    rest = Rest(row_y, col_z, EARLY, slot, rest_send, rest_recv)
-    greet([(fs, right), (fs, left), (fs, other)] + rest.peers)
+    for i in range(2 * FFB // LANE):
+        block[:, pl.ds(LANE * i, LANE)] = turned_in[pl.ds(LANE * i, LANE), :].T
+    block[:, pl.ds(2 * FFB, MIX)] = mix[...]
+    greet([(fs, right), (fs, left), (fs, other)] + [(n, tp) for side in near_by for n in side])
     set_off(0)
     keeps = [pltpu.make_async_copy(block, outs[d].at[here[d]], own.at[d]) for d in (0, 1)]
     for copy in keeps:
@@ -416,10 +433,8 @@
     to_pair(2).start()
     sums(1)
     sums(2)
-    rest.start()
     pass_on(1)
     pass_on(2)
-    rest.relay(0)
 
     @pl.when(x == SIDE - 1)
     def _():
@@ -431,12 +446,11 @@
         sent(m)
     for copy in started:
         copy.wait_send()
-    rest.finish()
-
-
-def opening(block, cid):
+
+
+def opening(turned_in, mix, cid):
     f32, bf16 = jnp.float32, jnp.bfloat16
-    rows, cols = block.shape
+    rows, cols = LANE, PACKED
     size = SIDE * rows
     quad = (SIDE, rows // 2, size)
     duo = (2,) + quad[1:]
@@ -449,11 +463,11 @@
             jax.ShapeDtypeStruct((SIDE, rows, cols), f32),
             jax.ShapeDtypeStruct((SIDE, rows, cols), f32),
             jax.ShapeDtypeStruct((rows // 2, TURN * LANE), f32),
-            jax.ShapeDtypeStruct((2, len(FAR), rows // 2, PACKED), f32),
         ],
-        in_specs=[vmem],
-        out_specs=[vmem, vmem, vmem, ANY],
+        in_specs=[vmem] * 2,
+        out_specs=[vmem] * 3,
         scratch_shapes=[
+            pltpu.VMEM((rows, cols), f32),
             pltpu.VMEM((size, WIDTH_LEFT), bf16),
             pltpu.VMEM((size, WIDTH_LEFT), bf16),
             pltpu.VMEM((size, cols), bf16),
@@ -471,128 +485,10 @@
             dma((3,)),
             dma((3, 10)),
             dma((3, 10)),
-            dma((8 * len(EARLY),)),
-            dma((8 * len(EARLY),)),
         ],
         compiler_params=pltpu.CompilerParams(collective_id=cid, has_side_effects=True, vmem_limit_bytes=36 << 20),
         name="opening",
-    )(block)
-
-
-def last_kernel(
-    block, row_y, col_z, rest_a, rest_m, y_out, out, full, high, low, pair, send, recv, own, pair_send, pair_recv, rest_send, rest_recv
-):
-    fs, tp, z, y, x, core = places()
-    right = 2 * lax.rem(x + 1, SIDE) + core
-    left = 2 * lax.rem(x + SIDE - 1, SIDE) + core
-    other = tp + 1 - 2 * core
-    ahead, back, across = lax.rem(x + 1, SIDE), lax.rem(x + SIDE - 1, SIDE), lax.rem(x + 2, SIDE)
-
-    def origin(h, e, f):
-        return plane_at(z, y, f, e) if h == 0 else plane_at(z, y, e, f)
-
-    def slot(h, s, e, f, to, row, rows):
-        _, col, width = LATE[s]
-        return full.at[origin(h, e, f + to), pl.ds(h * rest.half + row, rows), pl.ds(col, width)]
-
-    rest = Rest(row_y, col_z, LATE, slot, rest_send, rest_recv)
-    greet([(fs, right), (fs, left), (fs, other)] + rest.peers)
-    half = block.shape[0] // 2
-    parts = [pl.ds(0, half), pl.ds(half, half)]
-    go_right = [put(block.at[parts[h]], out.at[x, core, parts[h]], send.at[h], recv.at[h], fs, right) for h in (0, 1)]
-    go_left = [put(block.at[parts[1 - h]], out.at[x, core, parts[1 - h]], send.at[2 + h], recv.at[2 + h], fs, left) for h in (0, 1)]
-    for h in (0, 1):
-        go_right[h].start()
-        go_left[h].start()
-    rest.start()
-    moves = [(block, out.at[x, core])]
-    moves += [(row_y.at[lax.rem(y + e + SIDE, SIDE)], full.at[plane_at(z, y, 0, e)]) for e in (0,) + FAR]
-    moves += [(col_z.at[lax.rem(z + e + SIDE, SIDE)], full.at[plane_at(z, y, e, 0)]) for e in FAR]
-    for buf, (e, col, width) in ((rest_a, EARLY[0]), (rest_m.at[0], AMID[0]), (rest_m.at[1], AMID[1])):
-        for h in (0, 1):
-            for i, f in enumerate(FAR):
-                dst = full.at[origin(h, e, f), pl.ds(h * rest.half, rest.half), pl.ds(col, width)]
-                moves.append((buf.at[h, i, :, pl.ds(0, width)], dst))
-    keeps = [pltpu.make_async_copy(src, dst, own.at[i]) for i, (src, dst) in enumerate(moves)]
-    for keep in keeps:
-        keep.start()
-    put(block, out.at[x, core], pair_send, pair_recv, fs, other).start()
-    go_right[0].wait_recv()
-    first = out.at[back, core, parts[0]]
-    relay_right = put(first, first, send.at[4], recv.at[4], fs, right)
-    relay_right.start()
-    go_left[0].wait_recv()
-    second = out.at[ahead, core, parts[1]]
-    relay_left = put(second, second, send.at[5], recv.at[5], fs, left)
-    relay_left.start()
-    rest.relay(0)
-    go_right[1].wait_recv()
-    put(out.at[back, core], out.at[back, core], pair_send, pair_recv, fs, other).start()
-    go_left[1].wait_recv()
-    put(out.at[ahead, core], out.at[ahead, core], pair_send, pair_recv, fs, other).start()
-    for keep in keeps:
-        keep.wait()
-    rest.finish()
-
-    @pl.loop(0, PLANE)
-    def _(i):
-        for k in (0, 1):
-            rows = pl.ds(pl.multiple_of(LANE * i + 64 * k, 64), 64)
-            high[rows, :], low[rows, :] = split(full[i, pl.ds(64 * k, 64), :])
-
-    relay_right.wait_recv()
-    relay_left.wait_recv()
-    put(out.at[across, core], out.at[across, core], pair_send, pair_recv, fs, other).start()
-    for c in go_right + go_left + [relay_right, relay_left]:
-        c.wait_send()
-    whole = put(out.at[:, core], out.at[:, 1 - core], pair_send, pair_recv, fs, other)
-    whole.wait_send()
-    whole.wait_recv()
-    for m, (start, tiles) in enumerate(((0, 3), (WIDE, 3), (2 * FFB, 1))):
-        for c in (0, 1):
-            pair[pl.ds(64 * c, 64), :], pair[pl.ds(LANE + 64 * c, 64), :] = split(out[m, c])
-        scale = math.sqrt(D) if m == 2 else math.sqrt(max(D, FF))
-        for t in range(tiles):
-            cols = pl.ds(start + 256 * t, 256)
-            main = jnp.dot(pair[...], high[:, cols], preferred_element_type=jnp.float32)
-            side = jnp.dot(pair[:LANE, :], low[:, cols], preferred_element_type=jnp.float32)
-            value = scale * (main[:LANE] + (main[LANE:] + side))
-            if m == 1 and t == 0:
-                shared = pl.ds(start, LANE)
-                lane = lax.broadcasted_iota(jnp.int32, (LANE, LANE), 1)
-                y_out[:, shared] = jnp.where(lane < ODD, y_out[:, shared], value[:, :LANE])
-                y_out[:, pl.ds(start + LANE, LANE)] = value[:, LANE:]
-            else:
-                y_out[:, cols] = value
-
-
-def last_product(block, row_y, col_z, rest_a, rest_m, cid):
-    rows, cols = block.shape
-    f32, bf16 = jnp.float32, jnp.bfloat16
-    vmem = pl.BlockSpec(memory_space=pltpu.VMEM)
-    lanes = 8 * len(LATE)
-    return pl.pallas_call(
-        last_kernel,
-        out_shape=jax.ShapeDtypeStruct((LANE, PACKED), f32),
-        in_specs=[vmem] + [ANY] * 4,
-        out_specs=vmem,
-        scratch_shapes=[
-            pltpu.VMEM((SIDE, 2, rows, cols), f32),
-            pltpu.VMEM((PLANE,) + row_y.shape[1:], f32),
-            pltpu.VMEM((D, PACKED), bf16),
-            pltpu.VMEM((D, PACKED), bf16),
-            pltpu.VMEM((2 * LANE, D), bf16),
-            pltpu.SemaphoreType.DMA((6,)),
-            pltpu.SemaphoreType.DMA((6,)),
-            pltpu.SemaphoreType.DMA((8 + 18,)),
-            pltpu.SemaphoreType.DMA,
-            pltpu.SemaphoreType.DMA,
-            pltpu.SemaphoreType.DMA((lanes,)),
-            pltpu.SemaphoreType.DMA((lanes,)),
-        ],
-        compiler_params=pltpu.CompilerParams(collective_id=cid, has_side_effects=True, vmem_limit_bytes=36 << 20),
-        name="last_product",
-    )(block, row_y, col_z, rest_a, rest_m)
+    )(turned_in, mix)
 
 
 def turned(rows, dst):
@@ -655,16 +551,30 @@
     turned(w, next_rows)
 
 
-def second_chain_kernel(
-    sent, coef, row_y, col_z, out, rest_m, buf, high, low, pair, v, p, q, send, recv, own_sem, pair_send, pair_recv, rest_send, rest_recv
+def closing_kernel(
+    sent, coef, row_y, col_z, turned_out, mix_out, buf, high, low, pair, v, p, q, send, recv, own_sem, pair_send, pair_recv,
+    full, poly, rows, left_side, rest_send, rest_recv, moved, go_send, go_recv, poly_own, poly_send, poly_recv,
 ):
-    def slot(h, s, e, f, to, row, rows):
-        return rest_m.at[s, h, FAR.index(f), pl.ds(row, rows), pl.ds(0, AMID[s][2])]
-
-    greet(plane_peers())
+    fs, tp, z, y, x, core = places()
+    right = 2 * lax.rem(x + 1, SIDE) + core
+    left = 2 * lax.rem(x + SIDE - 1, SIDE) + core
+    other = tp + 1 - 2 * core
+    ahead, back, across = lax.rem(x + 1, SIDE), lax.rem(x + SIDE - 1, SIDE), lax.rem(x + 2, SIDE)
+
+    def slot(h, s, e, f, to, row, count):
+        origin = plane_at(z, y, f + to, e) if h == 0 else plane_at(z, y, e, f + to)
+        return full.at[origin, pl.ds(h * rest.half + row, count)]
+
+    rest = Rest(row_y, col_z, SPANS, slot, rest_send, rest_recv)
+    greet(plane_peers() + [(fs, right), (fs, left)])
     plane_gather(sent, buf, high, low, False, send, recv, own_sem, pair_send, pair_recv)
-    rest = Rest(row_y, col_z, AMID, slot, rest_send, rest_recv)
-    rest.start()
+    rest.start(0)
+    rest.start(1)
+    moves = [(row_y.at[lax.rem(y + e + SIDE, SIDE)], full.at[plane_at(z, y, 0, e)]) for e in (0,) + FAR]
+    moves += [(col_z.at[lax.rem(z + e + SIDE, SIDE)], full.at[plane_at(z, y, e, 0)]) for e in FAR]
+    copies = [pltpu.make_async_copy(src, dst, moved.at[i]) for i, (src, dst) in enumerate(moves)]
+    for copy in copies:
+        copy.start()
 
     def by_a1(src, dst):
         times(src, p, pair, high, low)
@@ -680,17 +590,98 @@
             by_a1(v, v)
 
     by_a1(coef, v)
-    out[...] = A_COEF * v[...]
+    poly[...] = A_COEF * v[...]
     by_t2()
-    out[...] += B_COEF * v[...]
-    for s in range(len(AMID)):
-        rest.relay(s)
+    poly[...] += B_COEF * v[...]
+    rest.relay(0)
+    rest.start(2)
     by_t2()
-    out[...] += C_COEF * v[...]
+    poly[...] += C_COEF * v[...]
+
+    half = poly.shape[0] // 2
+    parts = [pl.ds(0, half), pl.ds(half, half)]
+
+    def go(i, src, slot_x, part, target):
+        return put(src, rows.at[slot_x, core, part], go_send.at[i], go_recv.at[i], fs, target)
+
+    go_right = [go(h, poly.at[parts[h]], x, parts[h], right) for h in (0, 1)]
+    go_left = [go(2 + h, poly.at[parts[1 - h]], x, parts[1 - h], left) for h in (0, 1)]
+    for h in (0, 1):
+        go_right[h].start()
+        go_left[h].start()
+    mine = pltpu.make_async_copy(poly, rows.at[x, core], poly_own)
+    mine.start()
+
+    def to_pair(i, slot_x, src=None):
+        at = rows.at[slot_x, core]
+        copy = put(at if src is None else src, at, poly_send.at[i], poly_recv.at[i], fs, other)
+        copy.start()
+        return copy
+
+    pairs = [to_pair(0, x, poly)]
+    rest.relay(1)
+    go_right[0].wait_recv()
+    relay_right = go(4, rows.at[back, core, parts[0]], back, parts[0], right)
+    relay_right.start()
+    go_left[0].wait_recv()
+    relay_left = go(5, rows.at[ahead, core, parts[1]], ahead, parts[1], left)
+    relay_left.start()
+    rest.relay(2)
+    go_right[1].wait_recv()
+    pairs.append(to_pair(1, back))
+    go_left[1].wait_recv()
+    pairs.append(to_pair(2, ahead))
+    for copy in copies:
+        copy.wait()
     rest.finish()
 
-
-def chain_call(kernel, args, outs, cid, extra_sems, name):
+    @pl.loop(0, 2 * PLANE)
+    def _(n):
+        at = pl.ds(pl.multiple_of(64 * n, 64), 64)
+        src = pl.ds(pl.multiple_of(64 * lax.rem(n, 2), 64), 64)
+        high[at, pl.ds(0, PACKED)], low[at, pl.ds(0, PACKED)] = split(full[n // 2, src, :])
+
+    def product(m):
+        for c in (0, 1):
+            left_side[pl.ds(64 * c, 64), :], left_side[pl.ds(LANE + 64 * c, 64), :] = split(rows[m, c])
+        first, tiles = ((0, 3), (WIDE, 3), (2 * FFB, 1))[m]
+        for t in range(tiles):
+            start = first + 256 * t
+            cols = pl.ds(start, 256)
+            main = jnp.dot(left_side[...], high[:, cols], preferred_element_type=jnp.float32)
+            side = jnp.dot(left_side[:LANE, :], low[:, cols], preferred_element_type=jnp.float32)
+            value = main[:LANE] + (main[LANE:] + side)
+            if m == 2:
+                mix_out[...] = value
+                continue
+            value = value.T
+            low_cut, high_cut = max(start, FFB * m), min(start + 256, FFB * (m + 1))
+            turned_out[pl.ds(low_cut, high_cut - low_cut), :] = value[low_cut - start : high_cut - start]
+
+    mine.wait()
+    for copy in pairs:
+        copy.wait_recv()
+    for m in range(3):
+
+        @pl.when(across != m)
+        def _():
+            product(m)
+
+    relay_right.wait_recv()
+    relay_left.wait_recv()
+    pairs.append(to_pair(3, across))
+    pairs[3].wait_recv()
+    for m in range(3):
+
+        @pl.when(across == m)
+        def _():
+            product(m)
+
+    for copy in go_right + go_left + [relay_right, relay_left] + pairs:
+        copy.wait_send()
+
+
+def chain_call(kernel, args, outs, cid, extra, limit, name):
     size, rows = D, 64
     f32, bf16 = jnp.float32, jnp.bfloat16
     vmem = pl.BlockSpec(memory_space=pltpu.VMEM)
@@ -699,36 +690,50 @@
         kernel,
         out_shape=[jax.ShapeDtypeStruct(shape, f32) for shape in outs],
         in_specs=[vmem if a.ndim == 2 else ANY for a in args],
-        out_specs=[vmem if len(shape) == 2 else ANY for shape in outs],
+        out_specs=[vmem] * len(outs),
         scratch_shapes=[pltpu.VMEM((PLANE, 2, rows, TURN * LANE), f32)]
         + [pltpu.VMEM((size, size), bf16)] * 2
         + [pltpu.VMEM((2 * rows, size), bf16)]
         + [pltpu.VMEM((rows, size), f32)] * 3
         + [dma((40,)), dma((40,)), dma, dma((PLANE,)), dma((PLANE,))]
-        + [dma((extra_sems,))] * (2 if extra_sems else 0),
-        compiler_params=pltpu.CompilerParams(collective_id=cid, has_side_effects=True, vmem_limit_bytes=40 << 20),
+        + extra,
+        compiler_params=pltpu.CompilerParams(collective_id=cid, has_side_effects=True, vmem_limit_bytes=limit << 20),
         name=name,
     )(*args)
 
 
 def local(weights_in, weights_mix, momentum_in, momentum_mix, grads_in, grads_mix):
-    moment_in = MOMENTUM_DECAY * momentum_in + grads_in
+    f32, dma = jnp.float32, pltpu.SemaphoreType.DMA
+    turned_in = MOMENTUM_DECAY * jnp.swapaxes(momentum_in, 1, 2) + jnp.swapaxes(grads_in, 1, 2)
     moment_mix = MOMENTUM_DECAY * momentum_mix + grads_mix
-    packed = jnp.concatenate([moment_in[0], moment_in[1], moment_mix], axis=1)
-    row_y, col_z, sent, rest_a = opening(packed, 0)
+    row_y, col_z, sent = opening(turned_in.reshape(2 * FFB, LANE), moment_mix, 0)
     turn = (64, TURN * LANE)
-    sent, coef = chain_call(first_chain_kernel, (sent,), (turn, (64, D)), 2, 0, "first_chain")
-    mid = (len(AMID), 2, len(FAR), 64, PACKED)
-    poly, rest_m = chain_call(second_chain_kernel, (sent, coef, row_y, col_z), ((64, D), mid), 3, 8 * len(AMID), "second_chain")
-    steps = last_product(poly, row_y, col_z, rest_a, rest_m, 4)
-    step_in = jnp.stack([steps[:, :FFB], steps[:, FFB : 2 * FFB]])
-    step_mix = steps[:, 2 * FFB :]
+    sent, coef = chain_call(first_chain_kernel, (sent,), (turn, (64, D)), 1, [], 30, "first_chain")
+    extra = [
+        pltpu.VMEM((PLANE, LANE, PACKED), f32),
+        pltpu.VMEM((64, D), f32),
+        pltpu.VMEM((SIDE, 2, 64, D), f32),
+        pltpu.VMEM((2 * LANE, D), jnp.bfloat16),
+        dma((8 * len(SPANS),)),
+        dma((8 * len(SPANS),)),
+        dma((7,)),
+        dma((6,)),
+        dma((6,)),
+        dma,
+        dma((4,)),
+        dma((4,)),
+    ]
+    outs = ((2 * FFB, LANE), (LANE, MIX))
+    turned_step, step_mix = chain_call(closing_kernel, (sent, coef, row_y, col_z), outs, 2, extra, 47, "closing")
+    turned_step = math.sqrt(max(D, FF)) * turned_step.reshape(2, FFB, LANE)
+    step_mix = math.sqrt(D) * step_mix
+    turned_weights = jnp.swapaxes(weights_in, 1, 2) - STEP_RATE * turned_step
     return (
-        moment_in,
+        jnp.swapaxes(turned_in, 1, 2),
         moment_mix,
-        weights_in - STEP_RATE * step_in,
+        jnp.swapaxes(turned_weights, 1, 2),
         weights_mix - STEP_RATE * step_mix,
-        step_in,
+        jnp.swapaxes(turned_step, 1, 2),
         step_mix,
     )
 

time: 215 us -> 203 us (0.944)
  local copies, waits for them, and re-layouts: 12.4 us -> 1.73 us
  Pallas kernels: 199 us -> 195 us
  other arithmetic: 2.08 us -> 5.07 us
    pallas_call x2, Pallas kernels: 111 us -> 140 us  [chain_call(): pl.pallas_call(kernel, out_shape=[jax.ShapeDtypeStruct(shape, f32) for sh...]
    pallas_call x1 -> x0, Pallas kernels: 27 us -> none  [last_product(): pl.pallas_call(last_kernel, out_shape=jax.ShapeDtypeStruct((LANE, PACKED)...]
    unnamed x20 -> x10, local copies, waits for them, and re-layouts: 11.2 us -> 1.73 us
    pallas_call x1, Pallas kernels: 60.7 us -> 54.9 us  [opening(): pl.pallas_call(opening_kernel, out_shape=[jax.ShapeDtypeStruct((SIDE, row...]
where the time goes in v6:
time: 203 us
  Pallas kernels  195 us (96%)
  other arithmetic  5.07 us (2%)
    pallas_call x2, Pallas kernels, chain_call(): pl.pallas_call(kernel, out_shape=[jax.ShapeDtypeStruct(shape, f32) for sh...  140 us
    pallas_call x1, Pallas kernels, opening(): pl.pallas_call(opening_kernel, out_shape=[jax.ShapeDtypeStruct((SIDE, row...  54.9 us

profile of v6, /device:TPU:1, one launch (start us, length us, event | category | flops | bytes accessed | tf_op | source)
XLA Modules:
  0.0 202.5 jit_solution(7382977918692566792)
XLA Ops:
  0.6 1.0 multiply_add_fusion.1.mix
  1.6 0.0 copy-start.2
  1.6 1.5 multiply_add_fusion
  3.1 0.0 copy-start.1
  3.1 54.9 %opening.1 = (f32[4,128,1664]{2,1,0:T(8,128)S(1)}, f32[4,128,1664]{2,1,0:T(8,128)S(1)}, f32[64,1152]{1,0:T(8,128)S(1)}) custom-call(f32[1408,128]{1,0:T(8,128)S(1)} %bitcast.13, f32[128,256]{1,0:T(8,128)S(1)} %multiply_add_fusion.1.mix), custom_call_target="tpu_custom_call" | custom-call | tf_op jit(solution)/shard_map/opening/pallas_call | solution.py:460
  58.1 0.0 copy-start
  58.1 1.7 copy-done
  59.8 46.3 %first_chain.1 = (f32[64,1152]{1,0:T(8,128)S(1)}, f32[64,2048]{1,0:T(8,128)S(1)}) custom-call(f32[64,1152]{1,0:T(8,128)S(1)} %get-tuple-element.13.sent), custom_call_target="tpu_custom_call" | custom-call | tf_op jit(solution)/shard_map/first_chain/pallas_call | solution.py:689
  106.0 0.0 copy-start.4
  106.1 0.0 copy-start.3
  106.1 93.8 %closing.1 = (f32[1408,128]{1,0:T(8,128)S(1)}, f32[128,256]{1,0:T(8,128)S(1)}) custom-call(f32[64,1152]{1,0:T(8,128)S(1)} %get-tuple-element.14.sent, f32[64,2048]{1,0:T(8,128)S(1)} %get-tuple-element.15.coef, f32[4,128,1664]{2,1,0:T(8,128)S(1)} %get-tuple-element.16.row_y, f32[4,128,1664]{2,1,0:T(8,128)} %copy-done), custom_call_target="tpu_custom_call" | custom-call | tf_op jit(solution)/shard_map/closing/pallas_call | solution.py:689
  199.9 0.0 copy-done.2
  199.9 0.0 copy-done.1
  199.9 0.0 copy-done.4
  199.9 0.7 broadcast_multiply_fusion.2
  200.6 1.0 broadcast_multiply_fusion
  201.6 0.0 copy-done.3
  201.6 0.9 fusion
Async XLA Ops:
  1.6 198.3 %copy-start.2 = (f32[128,256]{1,0:T(8,128)}, f32[128,256]{1,0:T(8,128)S(1)}, u32[]{:S(2)}) copy-start(f32[128,256]{1,0:T(8,128)S(1)} %multiply_add_fusion.1.mix) | copy-start | bytes 393220
  3.1 196.8 %copy-start.1 = (f32[2,128,704]{1,2,0:T(8,128)}, f32[2,128,704]{1,2,0:T(8,128)S(1)}, u32[]{:S(2)}) copy-start(f32[2,128,704]{1,2,0:T(8,128)S(1)} %multiply_add_fusion) | copy-start | bytes 2162692
  58.1 1.7 copy-start
  106.0 93.9 %copy-start.4 = (f32[128,256]{1,0:T(8,128)S(1)}, f32[128,256]{1,0:T(8,128)}, u32[]{:S(2)}) copy-start(f32[128,256]{1,0:T(8,128)} %param.7) | copy-start | bytes 393220
  106.1 95.6 %copy-start.3 = (f32[2,128,704]{1,2,0:T(8,128)S(1)}, f32[2,128,704]{1,2,0:T(8,128)}, u32[]{:S(2)}) copy-start(f32[2,128,704]{1,2,0:T(8,128)} %param.6) | copy-start | bytes 2162692

commit v7 on v6

--- a/solution.py
+++ b/solution.py
@@ -18,7 +18,6 @@
 MOMENTUM_DECAY = 0.95
 STEP_RATE = 0.02
 MESH = pl.DeviceIdType.MESH
-ANY = pl.BlockSpec(memory_space=pl.ANY)
 
 SIDE = 4
 PLANE = SIDE * SIDE
@@ -36,6 +35,7 @@
 LEFT = ((0, WIDE + LANE), (WIDE + LANE, WIDE + LANE), (2 * (WIDE + LANE), MIX))
 RIGHT = (0, WIDE, 2 * FFB)
 WIDTH_LEFT = 2 * (WIDE + LANE) + MIX
+OWNER = (1, 0, 2)
 
 
 def put(src, dst, send, recv, fs, tp):
@@ -197,62 +197,50 @@
 
 
 class Rest:
-    def __init__(self, row_y, col_z, spans, slot, send, recv):
+    def __init__(self, full, spans, send, recv):
         fs, tp, z, y, x, core = places()
-        self.tp, self.spans, self.slot, self.send, self.recv = tp, spans, slot, send, recv
-        self.sources, self.here = (row_y, col_z), (y, z)
-        self.half = row_y.shape[1] // 2
-        self.near = [[plane_at(z, y, w, 0) for w in WAYS], [plane_at(z, y, 0, w) for w in WAYS]]
-        self.peers = [(n, tp) for side in self.near for n in side]
-        self.count = 0
-        self.started = []
-        self.direct = {}
-
-    def move(self, src, dst, target):
-        i = self.count
-        self.count += 1
-        copy = put(src, dst, self.send.at[i], self.recv.at[i], target, self.tp)
-        copy.start()
-        self.started.append(copy)
-        return copy
+        self.z, self.y, self.tp, self.full, self.spans, self.send, self.recv = z, y, tp, full, spans, send, recv
+        self.half = full.shape[1] // 2
+
+    def part(self, s, h, f, row, count):
+        e, col, width = self.spans[s]
+        origin = plane_at(self.z, self.y, f, e) if h == 0 else plane_at(self.z, self.y, e, f)
+        return self.full.at[origin, pl.ds(h * self.half + row, count), pl.ds(col, width)]
+
+    def copy(self, s, i, h, again):
+        w, quarter = WAYS[i], self.half // 2
+        part = self.part(s, h, -w, quarter * i, quarter) if again else self.part(s, h, 0, 0, self.half)
+        target = plane_at(self.z, self.y, w, 0) if h == 0 else plane_at(self.z, self.y, 0, w)
+        lane = 8 * s + 4 * again + 2 * i + h
+        return put(part, part, self.send.at[lane], self.recv.at[lane], target, self.tp)
 
     def start(self, s):
-        e, col, width = self.spans[s]
-        for i, w in enumerate(WAYS):
+        for i in (0, 1):
             for h in (0, 1):
-                rows = pl.ds(h * self.half, self.half)
-                block = lax.rem(self.here[h] + e + SIDE, SIDE)
-                src = self.sources[h].at[block, rows, pl.ds(col, width)]
-                self.direct[s, i, h] = self.move(src, self.slot(h, s, e, -w, w, 0, self.half), self.near[h][i])
+                self.copy(s, i, h, 0).start()
 
     def relay(self, s):
-        e = self.spans[s][0]
-        part = self.half // 2
-        for i, w in enumerate(WAYS):
+        for i in (0, 1):
             for h in (0, 1):
-                self.direct[s, i, h].wait_recv()
-                src = self.slot(h, s, e, -w, 0, part * i, part)
-                self.direct[s, i, h, 2] = self.move(src, self.slot(h, s, e, 2, w, part * i, part), self.near[h][i])
+                self.copy(s, i, h, 0).wait_recv()
+                self.copy(s, i, h, 1).start()
 
     def finish(self):
-        for key, copy in self.direct.items():
-            if len(key) == 4:
-                copy.wait_recv()
-        for copy in self.started:
-            copy.wait_send()
-
-
-def opening_kernel(
-    turned_in, mix, row_y, col_z, out, block, lh, ll, rh, rl, part, pair, total, far, near, hold,
-    send, recv, own, pair_send, pair_recv, sum_send, sum_recv,
-):
+        for s in range(len(self.spans)):
+            for i in (0, 1):
+                for h in (0, 1):
+                    self.copy(s, i, h, 1).wait_recv()
+                    for again in (0, 1):
+                        self.copy(s, i, h, again).wait_send()
+
+
+def opening(full, out, lh, ll, rh, rl, part, pair, total, far, near, hold, send, recv, pair_send, pair_recv, sum_send, sum_recv):
     fs, tp, z, y, x, core = places()
     right = 2 * lax.rem(x + 1, SIDE) + core
     left = 2 * lax.rem(x + SIDE - 1, SIDE) + core
     other = tp + 1 - 2 * core
     near_by = [[plane_at(z, y, 0, w) for w in WAYS], [plane_at(z, y, w, 0) for w in WAYS]]
-    outs, here = (row_y, col_z), (y, z)
-    rows = block.shape[0] // 2
+    rows = full.shape[1] // 2
     parts = [pl.ds(0, rows), pl.ds(rows, rows)]
     lane = iter(range(12 * len(GROUPS)))
     direct, relays, started = {}, {}, []
@@ -270,14 +258,15 @@
             for i in (0, 1):
                 for d in (0, 1):
                     half = parts[(i + k) % 2]
-                    direct[g, i, d, k] = move(block.at[half, cols], outs[d].at[here[d], half, cols], near_by[d][i])
+                    mine = full.at[fs, half, cols]
+                    direct[g, i, d, k] = move(mine, mine, near_by[d][i])
 
     def relay(g):
         cols = pl.ds(*GROUPS[g])
         for i, w in enumerate(WAYS):
             for d in (0, 1):
                 direct[g, i, d, 0].wait_recv()
-                half = outs[d].at[lax.rem(here[d] - w + SIDE, SIDE), parts[i], cols]
+                half = full.at[near_by[d][1 - i], parts[i], cols]
                 relays[g, i, d] = move(half, half, near_by[d][i])
 
     def arrived(g):
@@ -295,18 +284,18 @@
             at = pl.ds(pl.multiple_of(64 * n, 64), 64)
             src = pl.ds(pl.multiple_of(64 * lax.rem(n, 2), 64), 64)
             cols = pl.ds(first, width)
-            rh[at, cols], rl[at, cols] = split(col_z[n // 2, src, cols])
+            rh[at, cols], rl[at, cols] = split(full[SIDE * (n // 2) + y, src, cols])
             if g == 0:
                 plain, shared = pl.ds(0, WIDE), pl.ds(WIDE, LANE)
-                lh[at, plain], ll[at, plain] = split(row_y[n // 2, src, plain])
-                value = row_y[n // 2, src, shared]
+                lh[at, plain], ll[at, plain] = split(full[SIDE * z + n // 2, src, plain])
+                value = full[SIDE * z + n // 2, src, shared]
                 low_lane = lax.broadcasted_iota(jnp.int32, value.shape, 1) < ODD
                 lh[at, shared], ll[at, shared] = split(jnp.where(low_lane, value, 0.0))
                 next_to = pl.ds(WIDE + LANE, LANE)
                 lh[at, next_to], ll[at, next_to] = split(jnp.where(low_lane, 0.0, value))
             else:
                 to = pl.ds(first + LANE, width)
-                lh[at, to], ll[at, to] = split(row_y[n // 2, src, cols])
+                lh[at, to], ll[at, to] = split(full[SIDE * z + n // 2, src, cols])
 
     def gram(m):
         lc = pl.ds(*LEFT[m])
@@ -338,13 +327,13 @@
         return put(hold.at[m, side, c], near.at[2 + side, c], sum_send.at[m, i], sum_recv.at[m, i], fs, (right, left)[side])
 
     def before(m):
-        return x == (m + SIDE - 1) % SIDE
+        return x == (OWNER[m] + SIDE - 1) % SIDE
 
     def after(m):
-        return x == (m + 1) % SIDE
+        return x == (OWNER[m] + 1) % SIDE
 
     def beyond(m):
-        return x == (m + 2) % SIDE
+        return x == (OWNER[m] + 2) % SIDE
 
     def sums(m):
         to_pair(m).wait()
@@ -373,7 +362,7 @@
                     hold_copy(m, side, c).start()
 
     def keep_sum(m):
-        @pl.when(x == m)
+        @pl.when(x == OWNER[m])
         def _():
             near_copy(m, 0).wait_recv()
             near_copy(m, 1).wait_recv()
@@ -402,18 +391,9 @@
                 for c in (0, 1):
                     hold_copy(m, side, c).wait_send()
 
-    for i in range(2 * FFB // LANE):
-        block[:, pl.ds(LANE * i, LANE)] = turned_in[pl.ds(LANE * i, LANE), :].T
-    block[:, pl.ds(2 * FFB, MIX)] = mix[...]
-    greet([(fs, right), (fs, left), (fs, other)] + [(n, tp) for side in near_by for n in side])
     set_off(0)
-    keeps = [pltpu.make_async_copy(block, outs[d].at[here[d]], own.at[d]) for d in (0, 1)]
-    for copy in keeps:
-        copy.start()
     relay(0)
     set_off(1)
-    for copy in keeps:
-        copy.wait()
     arrived(0)
     prepare(0)
     gram(0)
@@ -448,49 +428,6 @@
         copy.wait_send()
 
 
-def opening(turned_in, mix, cid):
-    f32, bf16 = jnp.float32, jnp.bfloat16
-    rows, cols = LANE, PACKED
-    size = SIDE * rows
-    quad = (SIDE, rows // 2, size)
-    duo = (2,) + quad[1:]
-    vmem = pl.BlockSpec(memory_space=pltpu.VMEM)
-    dma = pltpu.SemaphoreType.DMA
-    moves = 12 * len(GROUPS)
-    return pl.pallas_call(
-        opening_kernel,
-        out_shape=[
-            jax.ShapeDtypeStruct((SIDE, rows, cols), f32),
-            jax.ShapeDtypeStruct((SIDE, rows, cols), f32),
-            jax.ShapeDtypeStruct((rows // 2, TURN * LANE), f32),
-        ],
-        in_specs=[vmem] * 2,
-        out_specs=[vmem] * 3,
-        scratch_shapes=[
-            pltpu.VMEM((rows, cols), f32),
-            pltpu.VMEM((size, WIDTH_LEFT), bf16),
-            pltpu.VMEM((size, WIDTH_LEFT), bf16),
-            pltpu.VMEM((size, cols), bf16),
-            pltpu.VMEM((size, cols), bf16),
-            pltpu.VMEM((3, SIDE, 2, rows // 2, size), f32),
-            pltpu.VMEM((3,) + quad, f32),
-            pltpu.VMEM((3,) + quad, f32),
-            pltpu.VMEM((3, 2) + duo, f32),
-            pltpu.VMEM((4,) + duo, f32),
-            pltpu.VMEM((3, 2) + duo, f32),
-            dma((moves,)),
-            dma((moves,)),
-            dma((2,)),
-            dma((3,)),
-            dma((3,)),
-            dma((3, 10)),
-            dma((3, 10)),
-        ],
-        compiler_params=pltpu.CompilerParams(collective_id=cid, has_side_effects=True, vmem_limit_bytes=36 << 20),
-        name="opening",
-    )(turned_in, mix)
-
-
 def turned(rows, dst):
     fs = lax.axis_index("fs")
     for b in range(TURN):
@@ -504,17 +441,12 @@
 
 
 def times(src, dst, pair, high, low, scale=None):
-    rows, size = src.shape
+    rows = src.shape[0]
     pair[:rows, :], pair[rows:, :] = split(src[...])
-    width = 1024
-
-    @pl.loop(0, size // width)
-    def _(j):
-        cols = pl.ds(pl.multiple_of(j * width, width), width)
-        main = jnp.dot(pair[...], high[:, cols], preferred_element_type=jnp.float32)
-        rest = jnp.dot(pair[...], low[:, cols], preferred_element_type=jnp.float32)
-        value = main[:rows] + (main[rows:] + (rest[:rows] + rest[rows:]))
-        dst[:, cols] = value if scale is None else scale * value
+    main = jnp.dot(pair[...], high[...], preferred_element_type=jnp.float32)
+    rest = jnp.dot(pair[...], low[...], preferred_element_type=jnp.float32)
+    value = main[:rows] + (main[rows:] + (rest[:rows] + rest[rows:]))
+    dst[...] = value if scale is None else scale * value
 
 
 def plane_peers():
@@ -522,10 +454,7 @@
     return [(plane_at(z, y, 0, w), tp) for w in WAYS] + [(plane_at(z, y, w, 0), tp) for w in WAYS] + [(fs, tp + 1 - 2 * core)]
 
 
-def first_chain_kernel(sent, next_rows, coef_rows, buf, high, low, pair, v, p, w, *sems):
-    greet(plane_peers())
-    plane_gather(sent, buf, high, low, True, *sems)
-
+def first_chain(buf, high, low, pair, v, p, q, sent, coef, release):
     def diag(i, total):
         block = buf[i, :, :, pl.ds(0, LANE)].reshape(LANE, LANE)
         eye = lax.broadcasted_iota(jnp.int32, block.shape, 0) == lax.broadcasted_iota(jnp.int32, block.shape, 1)
@@ -535,25 +464,31 @@
     ssq = jnp.sum(jnp.sum(acc, axis=0, keepdims=True), axis=1, keepdims=True)
     s = 0.5 * lax.rsqrt(jnp.maximum(ssq / D, 1.0))
     s2 = s * s
+    release()
     fs, tp = lax.axis_index("fs"), lax.axis_index("tp")
     shape = v.shape
     start = pl.multiple_of(128 * fs + 64 * lax.rem(tp, 2), 64)
     on_diag = lax.broadcasted_iota(jnp.int32, shape, 1) == start + lax.broadcasted_iota(jnp.int32, shape, 0)
     mine = pl.ds(start, shape[0])
     v[...] = s2 * (high[mine, :].astype(jnp.float32) + low[mine, :].astype(jnp.float32))
-    times(v, p, pair, high, low, s2)
-    coef_rows[...] = s * (jnp.where(on_diag, A_COEF, 0.0) + B_COEF * v[...] + C_COEF * p[...])
-    times(p, w, pair, high, low, s2)
-    w[...] = A_COEF * v[...] + B_COEF * p[...] + C_COEF * w[...]
-    times(w, v, pair, high, low, s2)
-    times(v, p, pair, high, low, s2)
-    w[...] = A_COEF * w[...] + B_COEF * v[...] + C_COEF * p[...]
-    turned(w, next_rows)
-
-
-def closing_kernel(
-    sent, coef, row_y, col_z, turned_out, mix_out, buf, high, low, pair, v, p, q, send, recv, own_sem, pair_send, pair_recv,
-    full, poly, rows, left_side, rest_send, rest_recv, moved, go_send, go_recv, poly_own, poly_send, poly_recv,
+
+    @pl.loop(0, 2)
+    def _(n):
+        times(v, p, pair, high, low, s2)
+
+        @pl.when(n == 0)
+        def _():
+            coef[...] = s * (jnp.where(on_diag, A_COEF, 0.0) + B_COEF * v[...] + C_COEF * p[...])
+
+        times(p, q, pair, high, low, s2)
+        v[...] = A_COEF * v[...] + B_COEF * p[...] + C_COEF * q[...]
+
+    turned(v, sent)
+
+
+def closing(
+    poly, turned_out, mix_out, high, low, pair, v, p, q, full, rows, left_side, rest_send, rest_recv, go_send, go_recv, poly_own,
+    poly_send, poly_recv,
 ):
     fs, tp, z, y, x, core = places()
     right = 2 * lax.rem(x + 1, SIDE) + core
@@ -561,42 +496,35 @@
     other = tp + 1 - 2 * core
     ahead, back, across = lax.rem(x + 1, SIDE), lax.rem(x + SIDE - 1, SIDE), lax.rem(x + 2, SIDE)
 
-    def slot(h, s, e, f, to, row, count):
-        origin = plane_at(z, y, f + to, e) if h == 0 else plane_at(z, y, e, f + to)
-        return full.at[origin, pl.ds(h * rest.half + row, count)]
-
-    rest = Rest(row_y, col_z, SPANS, slot, rest_send, rest_recv)
-    greet(plane_peers() + [(fs, right), (fs, left)])
-    plane_gather(sent, buf, high, low, False, send, recv, own_sem, pair_send, pair_recv)
+    rest = Rest(full, SPANS, rest_send, rest_recv)
     rest.start(0)
     rest.start(1)
-    moves = [(row_y.at[lax.rem(y + e + SIDE, SIDE)], full.at[plane_at(z, y, 0, e)]) for e in (0,) + FAR]
-    moves += [(col_z.at[lax.rem(z + e + SIDE, SIDE)], full.at[plane_at(z, y, e, 0)]) for e in FAR]
-    copies = [pltpu.make_async_copy(src, dst, moved.at[i]) for i, (src, dst) in enumerate(moves)]
-    for copy in copies:
-        copy.start()
-
-    def by_a1(src, dst):
-        times(src, p, pair, high, low)
+    v[...] = poly[...]
+
+    @pl.loop(0, 5)
+    def _(n):
+        @pl.when(lax.rem(n, 2) == 1)
+        def _():
+            times(v, q, pair, high, low)
+            v[...] = q[...]
+
+        times(v, p, pair, high, low)
         times(p, q, pair, high, low)
-        dst[...] = A_COEF * src[...] + B_COEF * p[...] + C_COEF * q[...]
-
-    def by_t2():
-        times(v, q, pair, high, low)
-        v[...] = q[...]
-
-        @pl.loop(0, 2)
-        def _(_):
-            by_a1(v, v)
-
-    by_a1(coef, v)
-    poly[...] = A_COEF * v[...]
-    by_t2()
-    poly[...] += B_COEF * v[...]
-    rest.relay(0)
-    rest.start(2)
-    by_t2()
-    poly[...] += C_COEF * v[...]
+        v[...] = A_COEF * v[...] + B_COEF * p[...] + C_COEF * q[...]
+
+        @pl.when(n == 0)
+        def _():
+            poly[...] = A_COEF * v[...]
+
+        @pl.when(n == 2)
+        def _():
+            poly[...] += B_COEF * v[...]
+            rest.relay(0)
+            rest.start(2)
+
+        @pl.when(n == 4)
+        def _():
+            poly[...] += C_COEF * v[...]
 
     half = poly.shape[0] // 2
     parts = [pl.ds(0, half), pl.ds(half, half)]
@@ -631,8 +559,6 @@
     pairs.append(to_pair(1, back))
     go_left[1].wait_recv()
     pairs.append(to_pair(2, ahead))
-    for copy in copies:
-        copy.wait()
     rest.finish()
 
     @pl.loop(0, 2 * PLANE)
@@ -643,7 +569,7 @@
 
     def product(m):
         for c in (0, 1):
-            left_side[pl.ds(64 * c, 64), :], left_side[pl.ds(LANE + 64 * c, 64), :] = split(rows[m, c])
+            left_side[pl.ds(64 * c, 64), :], left_side[pl.ds(LANE + 64 * c, 64), :] = split(rows[OWNER[m], c])
         first, tiles = ((0, 3), (WIDE, 3), (2 * FFB, 1))[m]
         for t in range(tiles):
             start = first + 256 * t
@@ -663,7 +589,7 @@
         copy.wait_recv()
     for m in range(3):
 
-        @pl.when(across != m)
+        @pl.when(across != OWNER[m])
         def _():
             product(m)
 
@@ -673,7 +599,7 @@
     pairs[3].wait_recv()
     for m in range(3):
 
-        @pl.when(across == m)
+        @pl.when(across == OWNER[m])
         def _():
             product(m)
 
@@ -681,50 +607,90 @@
         copy.wait_send()
 
 
-def chain_call(kernel, args, outs, cid, extra, limit, name):
-    size, rows = D, 64
-    f32, bf16 = jnp.float32, jnp.bfloat16
+def whole_kernel(
+    turned_in, mix, turned_out, mix_out, full, part, twin, total, far, near, hold, buf, high, low, left_side, v, p, q, coef, sent, rows,
+    free, cross_send, cross_recv, twin_send, twin_recv, sum_send, sum_recv, first_send, first_recv, first_own, first_pair_send,
+    first_pair_recv, next_send, next_recv, next_own, next_pair_send, next_pair_recv, rest_send, rest_recv, go_send, go_recv,
+    poly_own, poly_send, poly_recv,
+):
+    fs, tp, z, y, x, core = places()
+    for i in range(2 * FFB // LANE):
+        full[fs, :, pl.ds(LANE * i, LANE)] = turned_in[pl.ds(LANE * i, LANE), :].T
+    full[fs, :, pl.ds(2 * FFB, MIX)] = mix[...]
+    peers = plane_peers()
+    greet(peers + [(fs, 2 * lax.rem(x + w + SIDE, SIDE) + core) for w in WAYS])
+    size = SIDE * LANE
+    top, under = pl.ds(0, size), pl.ds(size, size)
+    lh, ll = (ref.at[top, pl.ds(0, WIDTH_LEFT)] for ref in (high, low))
+    rh, rl = (ref.at[under, pl.ds(0, PACKED)] for ref in (high, low))
+    opening(full, sent, lh, ll, rh, rl, part, twin, total, far, near, hold, cross_send, cross_recv, twin_send, twin_recv, sum_send, sum_recv)
+    plane_gather(sent, buf, high, low, True, first_send, first_recv, first_own, first_pair_send, first_pair_recv)
+    pair = left_side.at[pl.ds(0, LANE)]
+
+    def release():
+        for to_fs, to_tp in peers:
+            pl.semaphore_signal(free, inc=1, device_id=(to_fs, to_tp), device_id_type=MESH)
+
+    first_chain(buf, high, low, pair, v, p, q, sent, coef, release)
+    pl.semaphore_wait(free, len(peers))
+    plane_gather(sent, buf, high, low, False, next_send, next_recv, next_own, next_pair_send, next_pair_recv)
+    closing(
+        coef, turned_out, mix_out, high, low, pair, v, p, q, full, rows, left_side, rest_send, rest_recv, go_send, go_recv, poly_own,
+        poly_send, poly_recv,
+    )
+
+
+def whole(turned_in, mix):
+    f32, bf16, dma = jnp.float32, jnp.bfloat16, pltpu.SemaphoreType.DMA
     vmem = pl.BlockSpec(memory_space=pltpu.VMEM)
-    dma = pltpu.SemaphoreType.DMA
+    half = 64
+    quad = (SIDE, half, SIDE * LANE)
+    duo = (2,) + quad[1:]
+    gather = [dma((40,)), dma((40,)), dma, dma((PLANE,)), dma((PLANE,))]
+    moves = 12 * len(GROUPS)
     return pl.pallas_call(
-        kernel,
-        out_shape=[jax.ShapeDtypeStruct(shape, f32) for shape in outs],
-        in_specs=[vmem if a.ndim == 2 else ANY for a in args],
-        out_specs=[vmem] * len(outs),
-        scratch_shapes=[pltpu.VMEM((PLANE, 2, rows, TURN * LANE), f32)]
-        + [pltpu.VMEM((size, size), bf16)] * 2
-        + [pltpu.VMEM((2 * rows, size), bf16)]
-        + [pltpu.VMEM((rows, size), f32)] * 3
-        + [dma((40,)), dma((40,)), dma, dma((PLANE,)), dma((PLANE,))]
-        + extra,
-        compiler_params=pltpu.CompilerParams(collective_id=cid, has_side_effects=True, vmem_limit_bytes=limit << 20),
-        name=name,
-    )(*args)
+        whole_kernel,
+        out_shape=[jax.ShapeDtypeStruct((2 * FFB, LANE), f32), jax.ShapeDtypeStruct((LANE, MIX), f32)],
+        in_specs=[vmem] * 2,
+        out_specs=[vmem] * 2,
+        scratch_shapes=[
+            pltpu.VMEM((PLANE, LANE, PACKED), f32),
+            pltpu.VMEM((3, SIDE, 2) + quad[1:], f32),
+            pltpu.VMEM((3,) + quad, f32),
+            pltpu.VMEM((3,) + quad, f32),
+            pltpu.VMEM((3, 2) + duo, f32),
+            pltpu.VMEM((4,) + duo, f32),
+            pltpu.VMEM((3, 2) + duo, f32),
+            pltpu.VMEM((PLANE, 2, half, TURN * LANE), f32),
+            pltpu.VMEM((D, D), bf16),
+            pltpu.VMEM((D, D), bf16),
+            pltpu.VMEM((2 * LANE, D), bf16),
+        ]
+        + [pltpu.VMEM((half, D), f32)] * 4
+        + [
+            pltpu.VMEM((half, TURN * LANE), f32),
+            pltpu.VMEM((SIDE, 2, half, D), f32),
+            pltpu.SemaphoreType.REGULAR,
+            dma((moves,)),
+            dma((moves,)),
+            dma((3,)),
+            dma((3,)),
+            dma((3, 10)),
+            dma((3, 10)),
+        ]
+        + gather
+        + gather
+        + [dma((8 * len(SPANS),))] * 2
+        + [dma((6,)), dma((6,)), dma, dma((4,)), dma((4,))],
+        compiler_params=pltpu.CompilerParams(collective_id=0, has_side_effects=True, vmem_limit_bytes=64000000),
+        name="whole",
+    )(turned_in, mix)
 
 
 def local(weights_in, weights_mix, momentum_in, momentum_mix, grads_in, grads_mix):
-    f32, dma = jnp.float32, pltpu.SemaphoreType.DMA
     turned_in = MOMENTUM_DECAY * jnp.swapaxes(momentum_in, 1, 2) + jnp.swapaxes(grads_in, 1, 2)
     moment_mix = MOMENTUM_DECAY * momentum_mix + grads_mix
-    row_y, col_z, sent = opening(turned_in.reshape(2 * FFB, LANE), moment_mix, 0)
-    turn = (64, TURN * LANE)
-    sent, coef = chain_call(first_chain_kernel, (sent,), (turn, (64, D)), 1, [], 30, "first_chain")
-    extra = [
-        pltpu.VMEM((PLANE, LANE, PACKED), f32),
-        pltpu.VMEM((64, D), f32),
-        pltpu.VMEM((SIDE, 2, 64, D), f32),
-        pltpu.VMEM((2 * LANE, D), jnp.bfloat16),
-        dma((8 * len(SPANS),)),
-        dma((8 * len(SPANS),)),
-        dma((7,)),
-        dma((6,)),
-        dma((6,)),
-        dma,
-        dma((4,)),
-        dma((4,)),
-    ]
-    outs = ((2 * FFB, LANE), (LANE, MIX))
-    turned_step, step_mix = chain_call(closing_kernel, (sent, coef, row_y, col_z), outs, 2, extra, 47, "closing")
+    turned_step, step_mix = whole(turned_in.reshape(2 * FFB, LANE), moment_mix)
     turned_step = math.sqrt(max(D, FF)) * turned_step.reshape(2, FFB, LANE)
     step_mix = math.sqrt(D) * step_mix
     turned_weights = jnp.swapaxes(weights_in, 1, 2) - STEP_RATE * turned_step

time: 203 us -> 192 us (0.946)
  Pallas kernels: 195 us -> 183 us
    pallas_call x3 -> x1, Pallas kernels: 195 us -> 183 us  [whole(): pl.pallas_call(whole_kernel, out_shape=[jax.ShapeDtypeStruct((2 * FFB, LA...]
where the time goes in v7:
time: 192 us; the launch traced here: 191 us
  Pallas kernels  183 us (95%)
  other arithmetic  6.78 us (4%)
    pallas_call x1, Pallas kernels, whole(): pl.pallas_call(whole_kernel, out_shape=[jax.ShapeDtypeStruct((2 * FFB, LA...  183 us

profile of v7, /device:TPU:1, one launch (start us, length us, event | category | flops | bytes accessed | tf_op | source)
XLA Modules:
  0.0 191.0 jit_solution(10794847549584949059)
XLA Ops:
  0.6 0.0 copy-start.1
  0.6 0.0 copy-start.2
  0.7 2.3 %multiply_add_fusion = f32[2,128,704]{1,2,0:T(8,128)} fusion(f32[2,128,704]{1,2,0:T(8,128)} %param.10, f32[2,128,704]{1,2,0:T(8,128)} %param.8), kind=kLoop, calls=%fused_computation.2 | loop fusion | flops 360448 | bytes 2162688 | tf_op jit(solution)/shard_map/add | solution.py:691
  3.0 0.0 copy-done.1
  3.0 0.0 copy-done.2
  3.0 0.7 multiply_add_fusion.1.mix
  3.6 183.4 %whole.1 = (f32[1408,128]{1,0:T(8,128)}, f32[128,256]{1,0:T(8,128)}) custom-call(f32[1408,128]{1,0:T(8,128)} %bitcast.13, f32[128,256]{1,0:T(8,128)} %multiply_add_fusion.1.mix), custom_call_target="tpu_custom_call" | custom-call | tf_op jit(solution)/shard_map/whole/pallas_call | solution.py:651
  187.1 0.0 copy-start
  187.1 2.1 %broadcast_multiply_fusion = (f32[1408,128]{1,0:T(8,128)}, f32[1408,128]{1,0:T(8,128)S(1)}) fusion(f32[1408,128]{1,0:T(8,128)} %get-tuple-element.8), kind=kLoop, calls=%fused_computation.3 | loop fusion | flops 360448 | bytes 2162688 | tf_op jit(solution)/shard_map/mul | solution.py:694
  189.2 0.0 copy-done
  189.2 0.0 copy-start.3
  189.2 0.0 copy-start.4
  189.2 0.9 fusion
  190.2 0.0 copy-done.3
  190.2 0.1 copy-done.4
  190.3 0.7 broadcast_multiply_fusion.2
Async XLA Ops:
  0.6 2.3 %copy-start.1 = (f32[128,256]{1,0:T(8,128)S(1)}, f32[128,256]{1,0:T(8,128)}, u32[]{:S(2)}) copy-start(f32[128,256]{1,0:T(8,128)} %param.11) | copy-start | bytes 393220
  0.6 2.3 %copy-start.2 = (f32[128,256]{1,0:T(8,128)S(1)}, f32[128,256]{1,0:T(8,128)}, u32[]{:S(2)}) copy-start(f32[128,256]{1,0:T(8,128)} %param.9) | copy-start | bytes 393220
  187.1 2.2 %copy-start = (f32[2,128,704]{1,2,0:T(8,128)S(1)}, f32[2,128,704]{1,2,0:T(8,128)}, u32[]{:S(2)}) copy-start(f32[2,128,704]{1,2,0:T(8,128)} %param.6) | copy-start | bytes 2162692
  189.2 0.9 copy-start.3
  189.2 1.0 copy-start.4

commit v8 on v7

--- a/solution.py
+++ b/solution.py
@@ -234,7 +234,7 @@
                         self.copy(s, i, h, again).wait_send()
 
 
-def opening(full, out, lh, ll, rh, rl, part, pair, total, far, near, hold, send, recv, pair_send, pair_recv, sum_send, sum_recv):
+def opening(full, rest, out, lh, ll, rh, rl, whole_gram, part, pair, total, far, near, hold, send, recv, pair_send, pair_recv, sum_send, sum_recv):
     fs, tp, z, y, x, core = places()
     right = 2 * lax.rem(x + 1, SIDE) + core
     left = 2 * lax.rem(x + SIDE - 1, SIDE) + core
@@ -306,10 +306,16 @@
         for r in (0, 1):
             at = pl.ds(256 * r, 256)
             value = dot(lh[at, lc], rh[:, rc]) + (dot(lh[at, lc], rl[:, rc]) + dot(ll[at, lc], rh[:, rc]))
-            part[m, pl.ds(2 * r, 2)] = value.reshape((2,) + part.shape[2:])
+            whole_gram[at, :] = value
+        for d in range(TURN):
+            chip = lax.rem(fs + d, PLANE)
+            cols = pl.ds(pl.multiple_of(LANE * (chip // SIDE), LANE), LANE)
+            for c in (0, 1):
+                at = pl.ds(pl.multiple_of(LANE * lax.rem(chip, SIDE) + 64 * c, 64), 64)
+                part[m, c, :, :, pl.ds(LANE * d, LANE)] = whole_gram[at, cols].reshape(part.shape[2:4] + (LANE,))
 
     def to_pair(m):
-        return put(part.at[m, :, 1 - core], pair.at[m], pair_send.at[m], pair_recv.at[m], fs, other)
+        return put(part.at[m, 1 - core], pair.at[m], pair_send.at[m], pair_recv.at[m], fs, other)
 
     up, down = pl.ds(0, 2), pl.ds(2, 2)
 
@@ -337,7 +343,7 @@
 
     def sums(m):
         to_pair(m).wait()
-        total[m] = part[m, :, core] + pair[m]
+        total[m] = part[m, core] + pair[m]
 
         @pl.when(beyond(m))
         def _():
@@ -369,12 +375,9 @@
             for c in (0, 1):
                 for side in (0, 1):
                     hold_copy(m, side, c).wait_recv()
-            pair[m, up] = total[m, up] + near[2] + near[1]
-            pair[m, down] = total[m, down] + near[3] + near[0]
-            for b in range(TURN):
-                chip = lax.rem(fs + b, PLANE)
-                col = pl.multiple_of(LANE * (chip // SIDE), LANE)
-                out[:, pl.ds(LANE * b, LANE)] = pair[m, lax.rem(chip, SIDE), :, pl.ds(col, LANE)]
+            rows_up, rows_down = pl.ds(0, 32), pl.ds(32, 32)
+            out[rows_up, :] = (total[m, up] + near[2] + near[1]).reshape(32, TURN * LANE)
+            out[rows_down, :] = (total[m, down] + near[3] + near[0]).reshape(32, TURN * LANE)
 
     def sent(m):
         @pl.when(beyond(m))
@@ -408,6 +411,7 @@
     gram(1)
     to_pair(1).start()
     arrived(2)
+    rest.start(0)
     prepare(2)
     gram(2)
     to_pair(2).start()
@@ -487,8 +491,7 @@
 
 
 def closing(
-    poly, turned_out, mix_out, high, low, pair, v, p, q, full, rows, left_side, rest_send, rest_recv, go_send, go_recv, poly_own,
-    poly_send, poly_recv,
+    poly, turned_out, mix_out, high, low, pair, v, p, q, full, rest, rows, left_side, go_send, go_recv, poly_own, poly_send, poly_recv
 ):
     fs, tp, z, y, x, core = places()
     right = 2 * lax.rem(x + 1, SIDE) + core
@@ -496,9 +499,8 @@
     other = tp + 1 - 2 * core
     ahead, back, across = lax.rem(x + 1, SIDE), lax.rem(x + SIDE - 1, SIDE), lax.rem(x + 2, SIDE)
 
-    rest = Rest(full, SPANS, rest_send, rest_recv)
-    rest.start(0)
     rest.start(1)
+    rest.start(2)
     v[...] = poly[...]
 
     @pl.loop(0, 5)
@@ -519,8 +521,11 @@
         @pl.when(n == 2)
         def _():
             poly[...] += B_COEF * v[...]
-            rest.relay(0)
-            rest.start(2)
+            rest.relay(1)
+
+        @pl.when(n == 3)
+        def _():
+            rest.relay(2)
 
         @pl.when(n == 4)
         def _():
@@ -547,25 +552,24 @@
         return copy
 
     pairs = [to_pair(0, x, poly)]
-    rest.relay(1)
+    rest.finish()
+
+    @pl.loop(0, 2 * PLANE)
+    def _(n):
+        at = pl.ds(pl.multiple_of(64 * n, 64), 64)
+        src = pl.ds(pl.multiple_of(64 * lax.rem(n, 2), 64), 64)
+        high[at, pl.ds(0, PACKED)], low[at, pl.ds(0, PACKED)] = split(full[n // 2, src, :])
+
     go_right[0].wait_recv()
     relay_right = go(4, rows.at[back, core, parts[0]], back, parts[0], right)
     relay_right.start()
     go_left[0].wait_recv()
     relay_left = go(5, rows.at[ahead, core, parts[1]], ahead, parts[1], left)
     relay_left.start()
-    rest.relay(2)
     go_right[1].wait_recv()
     pairs.append(to_pair(1, back))
     go_left[1].wait_recv()
     pairs.append(to_pair(2, ahead))
-    rest.finish()
-
-    @pl.loop(0, 2 * PLANE)
-    def _(n):
-        at = pl.ds(pl.multiple_of(64 * n, 64), 64)
-        src = pl.ds(pl.multiple_of(64 * lax.rem(n, 2), 64), 64)
-        high[at, pl.ds(0, PACKED)], low[at, pl.ds(0, PACKED)] = split(full[n // 2, src, :])
 
     def product(m):
         for c in (0, 1):
@@ -608,7 +612,7 @@
 
 
 def whole_kernel(
-    turned_in, mix, turned_out, mix_out, full, part, twin, total, far, near, hold, buf, high, low, left_side, v, p, q, coef, sent, rows,
+    turned_in, mix, turned_out, mix_out, full, whole_gram, part, twin, total, far, near, hold, buf, high, low, left_side, v, p, q, coef, sent, rows,
     free, cross_send, cross_recv, twin_send, twin_recv, sum_send, sum_recv, first_send, first_recv, first_own, first_pair_send,
     first_pair_recv, next_send, next_recv, next_own, next_pair_send, next_pair_recv, rest_send, rest_recv, go_send, go_recv,
     poly_own, poly_send, poly_recv,
@@ -623,8 +627,10 @@
     top, under = pl.ds(0, size), pl.ds(size, size)
     lh, ll = (ref.at[top, pl.ds(0, WIDTH_LEFT)] for ref in (high, low))
     rh, rl = (ref.at[under, pl.ds(0, PACKED)] for ref in (high, low))
-    opening(full, sent, lh, ll, rh, rl, part, twin, total, far, near, hold, cross_send, cross_recv, twin_send, twin_recv, sum_send, sum_recv)
+    rest = Rest(full, SPANS, rest_send, rest_recv)
+    opening(full, rest, sent, lh, ll, rh, rl, whole_gram, part, twin, total, far, near, hold, cross_send, cross_recv, twin_send, twin_recv, sum_send, sum_recv)
     plane_gather(sent, buf, high, low, True, first_send, first_recv, first_own, first_pair_send, first_pair_recv)
+    rest.relay(0)
     pair = left_side.at[pl.ds(0, LANE)]
 
     def release():
@@ -635,8 +641,7 @@
     pl.semaphore_wait(free, len(peers))
     plane_gather(sent, buf, high, low, False, next_send, next_recv, next_own, next_pair_send, next_pair_recv)
     closing(
-        coef, turned_out, mix_out, high, low, pair, v, p, q, full, rows, left_side, rest_send, rest_recv, go_send, go_recv, poly_own,
-        poly_send, poly_recv,
+        coef, turned_out, mix_out, high, low, pair, v, p, q, full, rest, rows, left_side, go_send, go_recv, poly_own, poly_send, poly_recv
     )
 
 
@@ -644,7 +649,8 @@
     f32, bf16, dma = jnp.float32, jnp.bfloat16, pltpu.SemaphoreType.DMA
     vmem = pl.BlockSpec(memory_space=pltpu.VMEM)
     half = 64
-    quad = (SIDE, half, SIDE * LANE)
+    size = SIDE * LANE
+    quad = (4, half // 4, TURN * LANE)
     duo = (2,) + quad[1:]
     gather = [dma((40,)), dma((40,)), dma, dma((PLANE,)), dma((PLANE,))]
     moves = 12 * len(GROUPS)
@@ -655,7 +661,8 @@
         out_specs=[vmem] * 2,
         scratch_shapes=[
             pltpu.VMEM((PLANE, LANE, PACKED), f32),
-            pltpu.VMEM((3, SIDE, 2) + quad[1:], f32),
+            pltpu.VMEM((size, size), f32),
+            pltpu.VMEM((3, 2) + quad, f32),
             pltpu.VMEM((3,) + quad, f32),
             pltpu.VMEM((3,) + quad, f32),
             pltpu.VMEM((3, 2) + duo, f32),
@@ -691,9 +698,10 @@
     turned_in = MOMENTUM_DECAY * jnp.swapaxes(momentum_in, 1, 2) + jnp.swapaxes(grads_in, 1, 2)
     moment_mix = MOMENTUM_DECAY * momentum_mix + grads_mix
     turned_step, step_mix = whole(turned_in.reshape(2 * FFB, LANE), moment_mix)
-    turned_step = math.sqrt(max(D, FF)) * turned_step.reshape(2, FFB, LANE)
+    turned_step = math.sqrt(max(D, FF)) * turned_step
     step_mix = math.sqrt(D) * step_mix
-    turned_weights = jnp.swapaxes(weights_in, 1, 2) - STEP_RATE * turned_step
+    turned_weights = jnp.swapaxes(weights_in, 1, 2).reshape(2 * FFB, LANE) - STEP_RATE * turned_step
+    turned_step, turned_weights = (t.reshape(2, FFB, LANE) for t in (turned_step, turned_weights))
     return (
         jnp.swapaxes(turned_in, 1, 2),
         moment_mix,

time: 192 us -> 185 us (0.964)
  Pallas kernels: 183 us -> 178 us
    pallas_call x1, Pallas kernels: 183 us -> 178 us  [whole(): pl.pallas_call(whole_kernel, out_shape=[jax.ShapeDtypeStruct((2 * FFB, LA...]
where the time goes in v8:
time: 185 us; the launch traced here: 184 us
  Pallas kernels  178 us (96%)
  other arithmetic  6.07 us (3%)
    pallas_call x1, Pallas kernels, whole(): pl.pallas_call(whole_kernel, out_shape=[jax.ShapeDtypeStruct((2 * FFB, LA...  178 us

profile of v8, /device:TPU:1, one launch (start us, length us, event | category | flops | bytes accessed | tf_op | source)
XLA Modules:
  0.0 184.3 jit_solution(14306997705357371255)
XLA Ops:
  0.6 0.0 copy-start.1
  0.6 0.0 copy-start.2
  0.7 2.3 %multiply_add_fusion = f32[2,128,704]{1,2,0:T(8,128)} fusion(f32[2,128,704]{1,2,0:T(8,128)} %param.10, f32[2,128,704]{1,2,0:T(8,128)} %param.8), kind=kLoop, calls=%fused_computation.1 | loop fusion | flops 360448 | bytes 2162688 | tf_op jit(solution)/shard_map/add | solution.py:698
  3.0 0.0 copy-start
  3.0 0.0 copy-done.1
  3.0 0.0 copy-done.2
  3.0 0.7 multiply_add_fusion.1.mix
  3.6 177.6 %whole.1 = (f32[1408,128]{1,0:T(8,128)}, f32[128,256]{1,0:T(8,128)}) custom-call(f32[1408,128]{1,0:T(8,128)} %bitcast.13, f32[128,256]{1,0:T(8,128)} %multiply_add_fusion.1.mix), custom_call_target="tpu_custom_call" | custom-call | tf_op jit(solution)/shard_map/whole/pallas_call | solution.py:657
  181.2 0.0 copy-done
  181.2 0.0 copy-start.3
  181.2 0.0 copy-start.4
  181.2 2.4 %broadcast_multiply_fusion = (f32[1408,128]{1,0:T(8,128)}, f32[1408,128]{1,0:T(8,128)}) fusion(f32[1408,128]{1,0:T(8,128)} %get-tuple-element.8, f32[2,128,704]{1,2,0:T(8,128)S(1)} %copy-done), kind=kLoop, calls=%fused_computation.2 | loop fusion | flops 540672 | bytes 2883584 | tf_op jit(solution)/shard_map/mul | solution.py:701
  183.6 0.0 copy-done.3
  183.6 0.0 copy-done.4
  183.6 0.7 broadcast_multiply_fusion.1
Async XLA Ops:
  0.6 2.3 %copy-start.1 = (f32[128,256]{1,0:T(8,128)S(1)}, f32[128,256]{1,0:T(8,128)}, u32[]{:S(2)}) copy-start(f32[128,256]{1,0:T(8,128)} %param.11) | copy-start | bytes 393220
  0.6 2.3 %copy-start.2 = (f32[128,256]{1,0:T(8,128)S(1)}, f32[128,256]{1,0:T(8,128)}, u32[]{:S(2)}) copy-start(f32[128,256]{1,0:T(8,128)} %param.9) | copy-start | bytes 393220
  3.0 178.3 %copy-start = (f32[2,128,704]{1,2,0:T(8,128)S(1)}, f32[2,128,704]{1,2,0:T(8,128)}, u32[]{:S(2)}) copy-start(f32[2,128,704]{1,2,0:T(8,128)} %param.6) | copy-start | bytes 2162692
  181.2 2.4 %copy-start.3 = (f32[128,256]{1,0:T(8,128)S(1)}, f32[128,256]{1,0:T(8,128)}, u32[]{:S(2)}) copy-start(f32[128,256]{1,0:T(8,128)} %param.7) | copy-start | bytes 393220
  181.2 2.4 %copy-start.4 = (f32[128,256]{1,0:T(8,128)S(1)}, f32[128,256]{1,0:T(8,128)}, u32[]{:S(2)}) copy-start(f32[128,256]{1,0:T(8,128)} %get-tuple-element.9) | copy-start | bytes 393220

commit v9 on v8

--- a/solution.py
+++ b/solution.py
@@ -148,14 +148,13 @@
             for w in WAYS:
                 for w2 in WAYS:
                     to_pair(w, w2)
-
-    for w in WAYS:
-        for w2 in WAYS:
-            pairs[w, w2].wait_recv()
-
-    @pl.loop(0, 4)
-    def _(n):
-        rebuild(plane_at(z, y, 2 * (n // 2) - 1, 2 * lax.rem(n, 2) - 1))
+            for w in WAYS:
+                for w2 in WAYS:
+                    pairs[w, w2].wait_recv()
+
+            @pl.loop(0, 4)
+            def _(n):
+                rebuild(plane_at(z, y, 2 * (n // 2) - 1, 2 * lax.rem(n, 2) - 1))
 
     def last_hop(e):
         for j in (0, 1):
@@ -165,22 +164,21 @@
         if e != 2:
             to_pair(e, 2)
 
-    for e in (0, -1, 1):
-        last_hop(e)
-    for e in (0, -1, 1):
+    def across(e):
+        pairs[2, e].wait_recv()
         pairs[e, 2].wait_recv()
-        pairs[2, e].wait_recv()
-
-    @pl.loop(0, 3)
-    def _(n):
-        rebuild(plane_at(z, y, n - 1, 2))
-
+
+        @pl.loop(0, 2)
+        def _(n):
+            rebuild(plane_at(z, y, 2 + (e - 2) * n, e + (2 - e) * n))
+
+    last_hop(0)
+    last_hop(-1)
+    across(0)
+    last_hop(1)
+    across(-1)
     last_hop(2)
-
-    @pl.loop(0, 3)
-    def _(n):
-        rebuild(plane_at(z, y, 2, n - 1))
-
+    across(1)
     pairs[2, 2].wait_recv()
     rebuild(plane_at(z, y, 2, 2))
     for copy in started:
@@ -545,8 +543,8 @@
     mine = pltpu.make_async_copy(poly, rows.at[x, core], poly_own)
     mine.start()
 
-    def to_pair(i, slot_x, src=None):
-        at = rows.at[slot_x, core]
+    def to_pair(i, slot_x, src=None, part=slice(None)):
+        at = rows.at[slot_x, core, part]
         copy = put(at if src is None else src, at, poly_send.at[i], poly_recv.at[i], fs, other)
         copy.start()
         return copy
@@ -598,9 +596,11 @@
             product(m)
 
     relay_right.wait_recv()
+    pairs.append(to_pair(3, across, part=parts[0]))
     relay_left.wait_recv()
-    pairs.append(to_pair(3, across))
+    pairs.append(to_pair(4, across, part=parts[1]))
     pairs[3].wait_recv()
+    pairs[4].wait_recv()
     for m in range(3):
 
         @pl.when(across == OWNER[m])
@@ -688,8 +688,8 @@
         + gather
         + gather
         + [dma((8 * len(SPANS),))] * 2
-        + [dma((6,)), dma((6,)), dma, dma((4,)), dma((4,))],
-        compiler_params=pltpu.CompilerParams(collective_id=0, has_side_effects=True, vmem_limit_bytes=64000000),
+        + [dma((6,)), dma((6,)), dma, dma((5,)), dma((5,))],
+        compiler_params=pltpu.CompilerParams(collective_id=0, has_side_effects=True, vmem_limit_bytes=58000000),
         name="whole",
     )(turned_in, mix)
 

time: 185 us -> 185 us (level)
  no operation moved by 1% of the time
where the time goes in v9:
time: 185 us
  Pallas kernels  178 us (96%)
  other arithmetic  6.07 us (3%)
    pallas_call x1, Pallas kernels, whole(): pl.pallas_call(whole_kernel, out_shape=[jax.ShapeDtypeStruct((2 * FFB, LA...  178 us

profile of v9, /device:TPU:1, one launch (start us, length us, event | category | flops | bytes accessed | tf_op | source)
XLA Modules:
  0.0 185.1 jit_solution(237539071834791230)
XLA Ops:
  0.6 0.0 copy-start.1
  0.6 0.0 copy-start.2
  0.7 2.3 %multiply_add_fusion = f32[2,128,704]{1,2,0:T(8,128)} fusion(f32[2,128,704]{1,2,0:T(8,128)} %param.10, f32[2,128,704]{1,2,0:T(8,128)} %param.8), kind=kLoop, calls=%fused_computation.1 | loop fusion | flops 360448 | bytes 2162688 | tf_op jit(solution)/shard_map/add | solution.py:698
  3.0 0.0 copy-start
  3.0 0.0 copy-done.1
  3.0 0.0 copy-done.2
  3.0 0.7 multiply_add_fusion.1.mix
  3.6 178.3 %whole.1 = (f32[1408,128]{1,0:T(8,128)}, f32[128,256]{1,0:T(8,128)}) custom-call(f32[1408,128]{1,0:T(8,128)} %bitcast.13, f32[128,256]{1,0:T(8,128)} %multiply_add_fusion.1.mix), custom_call_target="tpu_custom_call" | custom-call | tf_op jit(solution)/shard_map/whole/pallas_call | solution.py:657
  182.0 0.0 copy-done
  182.0 0.0 copy-start.3
  182.0 0.0 copy-start.4
  182.0 2.4 %broadcast_multiply_fusion = (f32[1408,128]{1,0:T(8,128)}, f32[1408,128]{1,0:T(8,128)}) fusion(f32[1408,128]{1,0:T(8,128)} %get-tuple-element.8, f32[2,128,704]{1,2,0:T(8,128)S(1)} %copy-done), kind=kLoop, calls=%fused_computation.2 | loop fusion | flops 540672 | bytes 2883584 | tf_op jit(solution)/shard_map/mul | solution.py:701
  184.4 0.0 copy-done.3
  184.4 0.0 copy-done.4
  184.4 0.7 broadcast_multiply_fusion.1
Async XLA Ops:
  0.6 2.3 %copy-start.1 = (f32[128,256]{1,0:T(8,128)S(1)}, f32[128,256]{1,0:T(8,128)}, u32[]{:S(2)}) copy-start(f32[128,256]{1,0:T(8,128)} %param.11) | copy-start | bytes 393220
  0.6 2.3 %copy-start.2 = (f32[128,256]{1,0:T(8,128)S(1)}, f32[128,256]{1,0:T(8,128)}, u32[]{:S(2)}) copy-start(f32[128,256]{1,0:T(8,128)} %param.9) | copy-start | bytes 393220
  3.0 179.0 %copy-start = (f32[2,128,704]{1,2,0:T(8,128)S(1)}, f32[2,128,704]{1,2,0:T(8,128)}, u32[]{:S(2)}) copy-start(f32[2,128,704]{1,2,0:T(8,128)} %param.6) | copy-start | bytes 2162692
  182.0 2.4 %copy-start.3 = (f32[128,256]{1,0:T(8,128)S(1)}, f32[128,256]{1,0:T(8,128)}, u32[]{:S(2)}) copy-start(f32[128,256]{1,0:T(8,128)} %param.7) | copy-start | bytes 393220
  182.0 2.4 %copy-start.4 = (f32[128,256]{1,0:T(8,128)S(1)}, f32[128,256]{1,0:T(8,128)}, u32[]{:S(2)}) copy-start(f32[128,256]{1,0:T(8,128)} %get-tuple-element.9) | copy-start | bytes 393220

commit v10 on v8

--- a/solution.py
+++ b/solution.py
@@ -129,33 +129,18 @@
             for w in WAYS:
                 to_pair(0, w)
                 to_pair(w, 0)
-        if e == -1:
-            keep.wait()
-            for w in WAYS:
-                pairs[0, w].wait_recv()
-                pairs[w, 0].wait_recv()
-            pairs[0, 0].wait_recv()
-
-            @pl.loop(0, 3)
-            def _(n):
-                rebuild(plane_at(z, y, 0, n - 1))
-
-            @pl.loop(0, 2)
-            def _(n):
-                rebuild(plane_at(z, y, 2 * n - 1, 0))
-
         if e == 1:
             for w in WAYS:
                 for w2 in WAYS:
                     to_pair(w, w2)
 
-    for w in WAYS:
-        for w2 in WAYS:
-            pairs[w, w2].wait_recv()
-
-    @pl.loop(0, 4)
+    keep.wait()
+    for copy in pairs.values():
+        copy.wait_recv()
+
+    @pl.loop(0, 9)
     def _(n):
-        rebuild(plane_at(z, y, 2 * (n // 2) - 1, 2 * lax.rem(n, 2) - 1))
+        rebuild(plane_at(z, y, n // 3 - 1, lax.rem(n, 3) - 1))
 
     def last_hop(e):
         for j in (0, 1):

time: 185 us -> 187 us (1.011)
  Pallas kernels: 178 us -> 180 us
    pallas_call x1, Pallas kernels: 178 us -> 180 us  [whole(): pl.pallas_call(whole_kernel, out_shape=[jax.ShapeDtypeStruct((2 * FFB, LA...]
where the time goes in v10:
time: 187 us; the launch traced here: 186 us
  Pallas kernels  180 us (96%)
  other arithmetic  6.07 us (3%)
    pallas_call x1, Pallas kernels, whole(): pl.pallas_call(whole_kernel, out_shape=[jax.ShapeDtypeStruct((2 * FFB, LA...  180 us

profile of v10, /device:TPU:1, one launch (start us, length us, event | category | flops | bytes accessed | tf_op | source)
XLA Modules:
  0.0 186.4 jit_solution(1370635798594644580)
XLA Ops:
  0.6 0.0 copy-start.1
  0.6 0.0 copy-start.2
  0.7 2.3 %multiply_add_fusion = f32[2,128,704]{1,2,0:T(8,128)} fusion(f32[2,128,704]{1,2,0:T(8,128)} %param.10, f32[2,128,704]{1,2,0:T(8,128)} %param.8), kind=kLoop, calls=%fused_computation.1 | loop fusion | flops 360448 | bytes 2162688 | tf_op jit(solution)/shard_map/add | solution.py:683
  3.0 0.0 copy-start
  3.0 0.0 copy-done.1
  3.0 0.0 copy-done.2
  3.0 0.7 multiply_add_fusion.1.mix
  3.6 179.6 %whole.1 = (f32[1408,128]{1,0:T(8,128)}, f32[128,256]{1,0:T(8,128)}) custom-call(f32[1408,128]{1,0:T(8,128)} %bitcast.13, f32[128,256]{1,0:T(8,128)} %multiply_add_fusion.1.mix), custom_call_target="tpu_custom_call" | custom-call | tf_op jit(solution)/shard_map/whole/pallas_call | solution.py:642
  183.3 0.0 copy-done
  183.3 0.0 copy-start.3
  183.3 0.0 copy-start.4
  183.3 2.4 %broadcast_multiply_fusion = (f32[1408,128]{1,0:T(8,128)}, f32[1408,128]{1,0:T(8,128)}) fusion(f32[1408,128]{1,0:T(8,128)} %get-tuple-element.8, f32[2,128,704]{1,2,0:T(8,128)S(1)} %copy-done), kind=kLoop, calls=%fused_computation.2 | loop fusion | flops 540672 | bytes 2883584 | tf_op jit(solution)/shard_map/mul | solution.py:686
  185.7 0.0 copy-done.3
  185.7 0.0 copy-done.4
  185.7 0.7 broadcast_multiply_fusion.1
Async XLA Ops:
  0.6 2.3 %copy-start.1 = (f32[128,256]{1,0:T(8,128)S(1)}, f32[128,256]{1,0:T(8,128)}, u32[]{:S(2)}) copy-start(f32[128,256]{1,0:T(8,128)} %param.11) | copy-start | bytes 393220
  0.6 2.3 %copy-start.2 = (f32[128,256]{1,0:T(8,128)S(1)}, f32[128,256]{1,0:T(8,128)}, u32[]{:S(2)}) copy-start(f32[128,256]{1,0:T(8,128)} %param.9) | copy-start | bytes 393220
  3.0 180.3 %copy-start = (f32[2,128,704]{1,2,0:T(8,128)S(1)}, f32[2,128,704]{1,2,0:T(8,128)}, u32[]{:S(2)}) copy-start(f32[2,128,704]{1,2,0:T(8,128)} %param.6) | copy-start | bytes 2162692
  183.3 2.4 %copy-start.3 = (f32[128,256]{1,0:T(8,128)S(1)}, f32[128,256]{1,0:T(8,128)}, u32[]{:S(2)}) copy-start(f32[128,256]{1,0:T(8,128)} %param.7) | copy-start | bytes 393220
  183.3 2.4 %copy-start.4 = (f32[128,256]{1,0:T(8,128)S(1)}, f32[128,256]{1,0:T(8,128)}, u32[]{:S(2)}) copy-start(f32[128,256]{1,0:T(8,128)} %get-tuple-element.9) | copy-start | bytes 393220
